TPU v7x, 256 devices: a whole 4x4x8 slice. The times are simulated.
256 devices in a mesh: sp: 64 (over z, x, core), tp: 4 (over y).
Axes of the slice: x: 4, y: 4, z: 8, core: 2. Of those that a mesh axis runs over, the one named last changes fastest.
Arguments:
- residual: bfloat16 [8192, 2048], P(('sp', 'tp')), may hold values from -20 to 20
- query_small: bfloat16 [8192, 384], P('sp', 'tp'), may hold values from -12 to 12
- query_large: bfloat16 [8192, 640], P('sp', 'tp'), may hold values from -12 to 12
- latent: bfloat16 [8192, 512], P('sp'), may hold values from -30 to 30
- rotary_key: bfloat16 [8192, 32], P('sp'), may hold values from -16 to 16
- latent_gain: float32 [512], replicated, may hold values from 0.1 to 1.9
- small_keys: bfloat16 [512, 256], P(None, 'tp'), may hold values from -0.25 to 0.25
- small_values: bfloat16 [512, 256], P(None, 'tp'), may hold values from -0.25 to 0.25
- large_keys: bfloat16 [512, 512], P(None, 'tp'), may hold values from -0.25 to 0.25
- large_values: bfloat16 [512, 512], P(None, 'tp'), may hold values from -0.25 to 0.25
- small_output: bfloat16 [256, 2048], P('tp'), may hold values from -0.21875 to 0.21875
- large_output: bfloat16 [512, 2048], P('tp'), may hold values from -0.21875 to 0.21875
- ffn_gain: float32 [2048], replicated, may hold values from 0.1 to 1.9
- gate_weights: bfloat16 [64, 2048, 2048], P('sp', None, 'tp'), may hold values from -2 to 2
- up_weights: bfloat16 [64, 2048, 2048], P('sp', None, 'tp'), may hold values from -2 to 2
- down_weights: bfloat16 [64, 2048, 2048], P('sp', 'tp'), may hold values from -0.046875 to 0.046875
- routing: int32 [8192, 2], P(('sp', 'tp')), may hold values from 0 to 63, all different within a row; in each aligned block of 32 rows (0 to 31, 32 to 63, ...) at most 2 rows name the same one
- route_weight: float32 [8192, 2], P(('sp', 'tp')), may hold values from 0.2 to 1
Outputs:
- output: bfloat16 [8192, 2048], P(('sp', 'tp'))
Inputs may be any that keep to these rules, and one draw needn't show every extreme that they name: `routing`: each row names 2 different experts. Within the rows of one device (aligned blocks of 32 rows) no expert is named by more than 2 rows, and in every draw some block has an expert named by exactly 2 rows.
All inputs are finite; a program needn't handle non-finite values.
Results may differ from a plain program's by a relative error of at most 0.018.
Values may be sent and summed in bfloat16 or wider, within the bound.
No kernel may reach another device: no remote copies, remote signals or barrier semaphores. Data moves between devices by JAX's collectives and lax.ppermute only.
A program may use at most 128 MiB of HBM per device.

v0:
```python
import jax
import jax.numpy as jnp
from jax import lax
from jax.sharding import PartitionSpec as P

NOPE_S = 64
NOPE_L = 128
ROPE = 32
TOPK = 2


eps = 1e-06
clamp_limit = 7.0
glu_alpha = 1.702
rope_base = 10000.0
masked_score = -1e30


def sent_together(arrays, axis, dim, along):
    both = jnp.concatenate(arrays, axis=along)
    filled, at, gathered = (lax.all_gather(both, axis, axis=dim, tiled=True), 0, [])
    for a in arrays:
        gathered.append(lax.slice_in_dim(filled, at, at + a.shape[along], axis=along))
        at += a.shape[along]
    return tuple(gathered)


def in_blocks(array, dim, length):
    before, after = (array.shape[:dim], array.shape[dim + 1 :])
    return jnp.moveaxis(array.reshape(*before, length, -1, *after), dim, 0)


def sent_and_summed(array, axis, dim):
    length = lax.axis_size(axis)
    pieces = lax.all_to_all(in_blocks(array, dim, length), axis, 0, 0, tiled=True)
    return jnp.sum(pieces.astype(jnp.float32), axis=0)


def copy_for_each(array, axis):
    length = lax.axis_size(axis)
    return lax.all_to_all(
        jnp.broadcast_to(array[None], (length, *array.shape)), axis, 0, 0, tiled=True
    )


def laid_out(pieces, dim):
    pieces = jnp.moveaxis(pieces, 0, dim)
    dims = pieces.shape
    return pieces.reshape(*dims[:dim], dims[dim] * dims[dim + 1], *dims[dim + 2 :])


def gather_directly(array, axis, dim):
    pieces = copy_for_each(array, axis)
    return laid_out(pieces, dim)


def rope_tables(row_count, first_pos):
    half_size = ROPE // 2
    frequencies = jnp.power(rope_base, -jnp.arange(half_size, dtype=jnp.float32) * (2.0 / ROPE))
    places = (first_pos + jnp.arange(row_count, dtype=jnp.int32)).astype(jnp.float32)
    angles = places[:, None] * frequencies[None, :]
    return (jnp.cos(angles), jnp.sin(angles))


def rotate(values_in, cos_vals, sin_vals):
    front_half, back_half = jnp.split(values_in, 2, axis=-1)
    return jnp.concatenate(
        [
            front_half * cos_vals - back_half * sin_vals,
            back_half * cos_vals + front_half * sin_vals,
        ],
        axis=-1,
    )


def rms_scaled(values_in, gain):
    widened = values_in.astype(jnp.float32)
    return widened * lax.rsqrt(jnp.mean(widened * widened, axis=-1, keepdims=True) + eps) * gain


def turn_queries(query, nope, cos_vals, sin_vals):
    width = nope + ROPE
    shaped = query.reshape(query.shape[0], query.shape[1] // width, width)
    turned = rotate(
        shaped[:, :, nope:].astype(jnp.float32), cos_vals[:, None, :], sin_vals[:, None, :]
    )
    return jnp.concatenate([shaped[:, :, :nope], turned.astype(jnp.bfloat16)], axis=2)


def clamped(gate_pre, up_pre):
    limited = jnp.minimum(gate_pre, clamp_limit)
    linear = jnp.clip(up_pre, -clamp_limit, clamp_limit)
    return limited * jax.nn.sigmoid(glu_alpha * limited) * (linear + 1.0)


def make_keys(latent_rows, raw_rotary, first_pos, latent_gain, projections):
    normed_latent = rms_scaled(latent_rows, latent_gain).astype(jnp.bfloat16)
    projected = tuple(
        (
            jnp.dot(normed_latent, weight, preferred_element_type=jnp.float32).astype(jnp.bfloat16)
            for weight in projections
        )
    )
    cos_vals, sin_vals = rope_tables(latent_rows.shape[0], first_pos)
    turned = rotate(raw_rotary.astype(jnp.float32), cos_vals, sin_vals).astype(jnp.bfloat16)
    return projected + (turned,)


def empty_state(query, values_in):
    head_count = query.shape[1]
    row_count = query.shape[0]
    value_size = values_in.shape[1] // head_count
    return (
        jnp.full((head_count, row_count), masked_score, jnp.float32),
        jnp.zeros((head_count, row_count), jnp.float32),
        jnp.zeros((row_count, head_count, value_size), jnp.float32),
    )


def update(state_now, query, keys_in, values_in, rotary, nope, allowed):
    running_max, weight_sum, weighted = state_now
    head_count = query.shape[1]
    span_rows = rotary.shape[0]
    key_heads = keys_in.reshape(span_rows, head_count, nope)
    value_heads = values_in.reshape(span_rows, head_count, -1)
    scores = jnp.einsum(
        "rhd,khd->hrk", query[:, :, :nope], key_heads, preferred_element_type=jnp.float32
    )
    scores = scores + jnp.einsum(
        "rhd,kd->hrk", query[:, :, nope:], rotary, preferred_element_type=jnp.float32
    )
    scores = jnp.where(allowed[None], scores * (nope + ROPE) ** (-0.5), masked_score)
    new_max = jnp.maximum(running_max, jnp.max(scores, axis=2))
    weights = jnp.where(allowed[None], jnp.exp(scores - new_max[:, :, None]), 0.0)
    rescale = jnp.exp(running_max - new_max)
    weight_sum = jnp.sum(weights, axis=2)
    weighted = weighted * rescale.T[:, :, None] + jnp.einsum(
        "hrk,khd->rhd",
        weights.astype(jnp.bfloat16),
        value_heads,
        preferred_element_type=jnp.float32,
    )
    return (new_max, weight_sum, weighted)


def finish(state_end, row_count):
    running_max, weight_sum, weighted = state_end
    return (weighted / weight_sum.T[:, :, None]).reshape(row_count, -1).astype(jnp.bfloat16)


def on_device(
    residual,
    query_small,
    query_large,
    latent,
    rotary_key,
    latent_gain,
    small_keys,
    small_values,
    large_keys,
    large_values,
    small_output,
    large_output,
    ffn_gain,
    gate_weights,
    up_weights,
    down_weights,
    routing,
    route_weight,
):
    row_count = latent.shape[0]
    first_pos = lax.axis_index("sp") * row_count
    cos_vals, sin_vals = rope_tables(row_count, first_pos)
    small_query = turn_queries(query_small, NOPE_S, cos_vals, sin_vals)
    large_query = turn_queries(query_large, NOPE_L, cos_vals, sin_vals)
    query_pos = first_pos + jnp.arange(row_count, dtype=jnp.int32)
    last_pos = first_pos + row_count - 1
    projections = (small_keys, small_values, large_keys, large_values)
    initial = (empty_state(small_query, small_values), empty_state(large_query, large_values))
    own_keys = make_keys(latent, rotary_key, first_pos, latent_gain, projections)
    key_set = sent_together(
        (own_keys[0], own_keys[1], own_keys[2], own_keys[3], own_keys[4]), "sp", 0, 1
    )
    offset = jnp.int32(0)
    span_rows = key_set[0].shape[0]
    allowed = jnp.arange(span_rows, dtype=jnp.int32)[None, :] <= query_pos[:, None]

    def live(inner):
        return (
            update(inner[0], small_query, key_set[0], key_set[1], key_set[4], NOPE_S, allowed),
            update(inner[1], large_query, key_set[2], key_set[3], key_set[4], NOPE_L, allowed),
        )

    def keep_state(inner):
        return inner

    state_end = lax.cond(offset <= last_pos, live, keep_state, initial)
    small_heads = finish(state_end[0], row_count)
    large_heads = finish(state_end[1], row_count)
    tok_count = row_count // lax.axis_size("tp")
    summed = sent_and_summed(
        (
            jnp.dot(small_heads, small_output, preferred_element_type=jnp.float32)
            + jnp.dot(large_heads, large_output, preferred_element_type=jnp.float32)
        ).astype(jnp.bfloat16),
        "tp",
        0,
    )
    attention = lax.optimization_barrier(summed.astype(jnp.bfloat16)).astype(jnp.float32)
    middle = lax.optimization_barrier(
        (residual.astype(jnp.float32) + attention).astype(jnp.bfloat16)
    )
    normed = rms_scaled(middle, ffn_gain).astype(jnp.bfloat16)
    local_experts = gate_weights.shape[0]
    expert_count = local_experts * lax.axis_size("sp")
    capacity = max(2, 2 * TOPK * tok_count // expert_count)
    assigned = routing.reshape(-1)
    onehot = (assigned[:, None] == jnp.arange(expert_count, dtype=jnp.int32)[None, :]).astype(
        jnp.int32
    )
    slot_index = jnp.sum((jnp.cumsum(onehot, axis=0) - onehot) * onehot, axis=1)
    places = assigned * capacity + slot_index
    pick_table = (
        places[:, None] == jnp.arange(expert_count * capacity, dtype=jnp.int32)[None, :]
    ).astype(jnp.bfloat16)
    send_table = jnp.sum(pick_table.reshape(tok_count, TOPK, -1), axis=1)
    outgoing = lax.dot_general(
        send_table, normed, (((0,), (0,)), ((), ())), preferred_element_type=jnp.float32
    )
    outgoing = outgoing.astype(jnp.bfloat16).reshape(expert_count, capacity, -1)
    shard_piece = gather_directly(
        lax.all_to_all(outgoing, "sp", split_axis=0, concat_axis=0, tiled=True), "tp", 0
    )
    grouped = shard_piece.reshape(-1, local_experts, shard_piece.shape[1], shard_piece.shape[2])
    gate_pre = jnp.einsum(
        "secd,edf->secf", grouped, gate_weights, preferred_element_type=jnp.float32
    )
    up_pre = jnp.einsum("secd,edf->secf", grouped, up_weights, preferred_element_type=jnp.float32)
    hidden = clamped(gate_pre, up_pre).astype(jnp.bfloat16)
    result = jnp.einsum("secf,efd->secd", hidden, down_weights, preferred_element_type=jnp.float32)
    partials = result.reshape(shard_piece.shape[0], shard_piece.shape[1], -1)
    combined = lax.psum_scatter(
        partials.astype(jnp.bfloat16), "tp", scatter_dimension=0, tiled=True
    )
    returned = lax.all_to_all(combined, "sp", split_axis=0, concat_axis=0, tiled=True)
    picked = jnp.dot(
        pick_table,
        returned.reshape(expert_count * capacity, -1),
        preferred_element_type=jnp.float32,
    )
    mixed = jnp.sum(route_weight[:, :, None] * picked.reshape(tok_count, TOPK, -1), axis=1)
    return (middle.astype(jnp.float32) + mixed).astype(jnp.bfloat16)


def solution(mesh):
    return jax.shard_map(
        on_device,
        mesh=mesh,
        in_specs=(
            P(("sp", "tp"), None),
            P("sp", "tp"),
            P("sp", "tp"),
            P("sp", None),
            P("sp", None),
            P(),
            P(None, "tp"),
            P(None, "tp"),
            P(None, "tp"),
            P(None, "tp"),
            P("tp", None),
            P("tp", None),
            P(),
            P("sp", None, "tp"),
            P("sp", None, "tp"),
            P("sp", "tp", None),
            P(("sp", "tp"), None),
            P(("sp", "tp"), None),
        ),
        out_specs=P(("sp", "tp"), None),
        check_vma=False,
    )
```

profile of v0, /device:TPU:1, one launch (start us, length us, event | category | flops | bytes accessed | tf_op | source)
XLA Modules:
  0.0 278.2 jit_solution(9431828192114323149)
XLA Ops:
  6.6 1.2 fusion.104
  7.7 0.7 convert_element_type.125
  8.4 1.2 fusion.96
  9.6 1.2 fusion.95
  10.8 1.3 fusion.94
  12.1 1.3 fusion.93
  14.2 0.8 copy.66
  16.8 83.5 %all-gather.2.cloned.1.call-done = bf16[8192,416]{0,1:T(8,128)(2,1)} async-done(((bf16[128,416]{0,1:T(8,128)(2,1)}), bf16[8192,416]{0,1:T(8,128)(2,1)}) %all-gather.2.cloned.1.call-update) | async-done | bytes 6815760 | tf_op jit(solution)/shard_map/all_gather | solution.py:21
  100.4 2.4 le.22
  102.8 27.6 %conditional.1 = (f32[1,128]{1,0:T(1,128)}, f32[128,1,64]{0,2,1:T(8,128)S(1)}, f32[1,128]{1,0:T(1,128)}, f32[128,1,128]{2,0,1:T(8,128)S(1)}) conditional(s32[]{:T(128)} %convert_element_type.118, () %tuple.13, (s32[]{:T(128)}, s32[128,1]{0,1:T(1,128)S(1)}, s32[128,8192]{1,0:T(8,128)}, bf16[128,1,96]{0,2,1:T(8,128)(2,1)}, bf16[8192,416]{0,1:T(8,128)(2,1)}, ...), branch_computations={%region_1.0_spmd, %region_2.7_spmd} | conditional | flops 962617728 | bytes 124086408 | solution.py:197
  102.9 2.8 %broadcast_compare_fusion = pred[128,8192]{1,0:T(32,128)(4,1)S(1)} fusion(s32[128,8192]{1,0:T(8,128)} %get-tuple-element.37, s32[128]{0:T(128)S(1)} %add_bitcast_fusion), kind=kLoop, calls=%fused_computation.28 | loop fusion | flops 1048576 | bytes 5243392 | tf_op jit(solution)/shard_map/le | solution.py:186
  105.7 10.8 %copy.64 = bf16[8192,416]{1,0:T(8,128)(2,1)} copy(bf16[8192,416]{0,1:T(8,128)(2,1)} %get-tuple-element.89) | data formatting | bytes 13631488 | tf_op jit(solution)/shard_map
  116.5 2.5 convolution_bitcast_fusion
  119.0 3.0 %fusion.155 = (f32[128]{0:T(128)S(1)}, f32[1,128,8192]{2,1,0:T(8,128)S(1)}) fusion(f32[1,128,8192]{2,1,0:T(8,128)S(1)} %convolution_bitcast_fusion, bf16[8192,416]{1,0:T(8,128)(2,1)} %copy.64, bf16[128,1,160]{2,0,1:T(8,128)(2,1)S(1)} %copy.65, pred[128,8192]{1,0:T(32,128)(4,1)S(1)} %broadcast_compare_fusion), kind=kOutput, calls=%fused_computation.153 | convolution fusion | flops 272629632 | bytes 11567616 | tf_op jit(solution)/shard_map/cond/branch_1_fun/rhd,khd->hrk/dot_general | solution.py:126
  122.0 0.7 convolution_bitcast_fusion.2
  122.8 1.4 fusion.156
  124.3 0.7 copy-done.1
  125.0 2.4 fusion.9
  127.4 1.9 fusion.51
  129.3 1.1 fusion.36
  130.4 1.0 fusion.120
  131.4 2.2 fusion.62
  133.6 4.0 %all-to-all-start = ((bf16[4,32,2048]{2,1,0:T(8,128)(2,1)}), bf16[4,32,2048]{2,1,0:T(8,128)(2,1)S(1)}, u32[]{:S(2)}, u32[]{:S(2)}) async-start(bf16[4,32,2048]{2,1,0:T(8,128)(2,1)} %bitcast.28), calls=%async_computation | async-start | bytes 1048576 | tf_op jit(solution)/shard_map/all_to_all | solution.py:35
  138.1 8.6 %all-to-all-done = bf16[4,32,2048]{2,1,0:T(8,128)(2,1)S(1)} async-done(((bf16[4,32,2048]{2,1,0:T(8,128)(2,1)}), bf16[4,32,2048]{2,1,0:T(8,128)(2,1)S(1)}, u32[]{:S(2)}, u32[]{:S(2)}) %all-to-all-start) | async-done | bytes 524320 | tf_op jit(solution)/shard_map/all_to_all | solution.py:35
  147.6 27.4 %all_to_all.20 = bf16[64,2,2048]{2,1,0:T(2,128)(2,1)S(1)} all-to-all(bf16[64,2,2048]{2,1,0:T(2,128)(2,1)S(1)} %reshape.355), channel_id=1, replica_groups=mesh['sp'=64,'tp'=4] {'sp'}, dimensions={0} | all-to-all | bytes 1048576 | tf_op jit(solution)/shard_map/all_to_all | solution.py:232
  175.5 28.6 %all_to_all.21 = bf16[4,64,2,2048]{3,1,2,0:T(8,128)(2,1)S(1)} all-to-all(bf16[4,64,2,2048]{3,1,2,0:T(8,128)(2,1)S(1)} %broadcast_in_dim.21), channel_id=1, replica_groups=mesh['sp'=64,'tp'=4] {'tp'}, dimensions={0} | all-to-all | bytes 4194304 | tf_op jit(solution)/shard_map/all_to_all | solution.py:41
  204.4 1.3 copy-done.2
  205.7 1.2 fusion.71
  206.9 6.1 %convolution_convert_fusion = bf16[256,2,2048]{2,0,1:T(8,128)(2,1)} fusion(bf16[1,512,2048]{2,1,0:T(8,128)(2,1)S(1)} %copy-done, bf16[256,2,2048]{2,0,1:T(8,128)(2,1)} %bitcast.195, bf16[1,2048,512]{2,1,0:T(8,128)(2,1)} %param.34, f32[256,1,2,512]{3,0,2,1:T(8,128)S(1)} %fusion.71), kind=kOutput, calls=%fused_computation.49 | convolution fusion | flops 2150891520 | bytes 9437184 | tf_op jit(solution)/shard_map/secf,efd->secd/dot_general | solution.py:240
  213.0 27.4 %reduce-scatter.2.cloned.1.call-done = bf16[64,2,2048]{2,0,1:T(8,128)(2,1)} async-done(((bf16[256,2,2048]{2,0,1:T(8,128)(2,1)}), bf16[64,2,2048]{2,0,1:T(8,128)(2,1)}) %reduce-scatter.2.cloned.1.call-update) | async-done | bytes 524304 | tf_op jit(solution)/shard_map/reduce_scatter | solution.py:242
  240.4 1.6 copy.70
  242.0 28.2 %all_to_all.22 = bf16[64,2,2048]{2,1,0:T(2,128)(2,1)S(1)} all-to-all(bf16[64,2,2048]{2,1,0:T(2,128)(2,1)S(1)} %copy.70), channel_id=1, replica_groups=mesh['sp'=64,'tp'=4] {'sp'}, dimensions={0} | all-to-all | bytes 1048576 | tf_op jit(solution)/shard_map/all_to_all | solution.py:245
  (68 shorter events, 6.1 us)
Async XLA Ops:
  6.5 200.4 %copy-start = (bf16[1,512,2048]{2,1,0:T(8,128)(2,1)S(1)}, bf16[1,512,2048]{2,1,0:T(8,128)(2,1)}, u32[]{:S(2)}) copy-start(bf16[1,512,2048]{2,1,0:T(8,128)(2,1)} %param.35) | copy-start | bytes 6291460
  6.5 96.2 %copy-start.6 = (bf16[128,160]{0,1:T(8,128)(2,1)S(1)}, bf16[128,160]{0,1:T(8,128)(2,1)}, u32[]{:S(2)}) copy-start(bf16[128,160]{0,1:T(8,128)(2,1)} %param.22) | copy-start | bytes 122884
  6.5 93.8 %all-gather.2.cloned.1.call-start = ((), (), s32[]{:S(2)}) async-start(), calls=%async_computation.5 | async-start | bytes 6922240 | tf_op jit(solution)/shard_map/all_gather | solution.py:21
  13.6 0.6 copy-start.5
  15.1 87.6 %copy-start.9 = (s32[64]{0:T(128)}, s32[64]{0:T(128)S(1)}, u32[]{:S(2)}) copy-start(s32[64]{0:T(128)S(1)} %eq.51) | copy-start | bytes 772
  102.7 27.6 %copy-start.3 = (bf16[64,2048]{1,0:T(8,128)(2,1)S(1)}, bf16[64,2048]{1,0:T(8,128)(2,1)}, u32[]{:S(2)}) copy-start(bf16[64,2048]{1,0:T(8,128)(2,1)} %param.30) | copy-start | bytes 786436
  116.5 5.5 %slice-start = ((s8[8388608]{0:T(1024)(128)(4,1)}), s8[4194304]{0:T(1024)(128)(4,1)S(1)}, s32[]{:S(2)}) async-start(s8[8388608]{0:T(1024)(128)(4,1)} %bitcast.192), calls=%async_computation.7 | async-start | bytes 8388608 | tf_op jit(solution)/shard_map/cond
  119.0 3.0 %slice-start.1 = ((s8[8388608]{0:T(1024)(128)(4,1)}), s8[4194304]{0:T(1024)(128)(4,1)S(1)}, s32[]{:S(2)}) async-start(s8[8388608]{0:T(1024)(128)(4,1)} %bitcast.192), calls=%async_computation.8 | async-start | bytes 8388608 | tf_op jit(solution)/shard_map/cond
  122.0 0.8 copy-start.7
  122.8 2.2 copy-start.1
  130.3 7.3 %copy-start.10 = (s32[64]{0:T(128)S(1)}, s32[64]{0:T(128)}, u32[]{:S(2)}) copy-start(s32[64]{0:T(128)} %copy-done.9) | copy-start | bytes 772
  130.3 7.6 %copy-start.11 = (s32[32,2]{0,1:T(2,128)S(1)}, s32[32,2]{0,1:T(2,128)}, u32[]{:S(2)}) copy-start(s32[32,2]{0,1:T(2,128)} %param.36) | copy-start | bytes 772
  130.4 16.4 %copy-start.4 = (bf16[32,2048]{1,0:T(8,128)(2,1)S(1)}, bf16[32,2048]{1,0:T(8,128)(2,1)}, u32[]{:S(2)}) copy-start(bf16[32,2048]{1,0:T(8,128)(2,1)} %param.20) | copy-start | bytes 393220
  130.4 16.6 %copy-start.8 = (f32[2048]{0:T(1024)S(1)}, f32[2048]{0:T(1024)}, u32[]{:S(2)}) copy-start(f32[2048]{0:T(1024)} %param.32) | copy-start | bytes 24580
  133.6 13.0 %all-to-all-start = ((bf16[4,32,2048]{2,1,0:T(8,128)(2,1)}), bf16[4,32,2048]{2,1,0:T(8,128)(2,1)S(1)}, u32[]{:S(2)}, u32[]{:S(2)}) async-start(bf16[4,32,2048]{2,1,0:T(8,128)(2,1)} %bitcast.28), calls=%async_computation | async-start | bytes 1048576 | tf_op jit(solution)/shard_map/all_to_all | solution.py:35
  137.6 102.8 %reduce-scatter.2.cloned.1.call-start = ((), (), s32[]{:S(2)}) async-start(), calls=%async_computation.6 | async-start | bytes 2621440 | tf_op jit(solution)/shard_map/reduce_scatter | solution.py:242
  175.5 30.2 %copy-start.13 = (bf16[1,2048,512]{2,1,0:T(8,128)(2,1)S(1)}, bf16[1,2048,512]{2,1,0:T(8,128)(2,1)}, u32[]{:S(2)}) copy-start(bf16[1,2048,512]{2,1,0:T(8,128)(2,1)} %param.33) | copy-start | bytes 6291460
  204.4 1.3 copy-start.2
  213.0 57.4 %copy-start.12 = (f32[32,2]{0,1:T(2,128)S(1)}, f32[32,2]{0,1:T(2,128)}, u32[]{:S(2)}) copy-start(f32[32,2]{0,1:T(2,128)} %param.37) | copy-start | bytes 772
Sparse Core Ops, SparseCore 0:
  14.4 85.9 all-gather.1
  213.1 27.1 reduce-scatter.1
where the time goes:
time: 279 us; the launch traced here: 278 us
  waiting for transfers between devices  119 us (43%)
  blocking collectives  84.3 us (30%)
  matrix products  26.6 us (10%)
  local copies, waits for them, and re-layouts  19.9 us (7%)
  between operations  13.6 us (5%)
  other arithmetic  10.2 us (4%)
  starting transfers between devices  4 us (1%)
    all_gather x1, waiting for transfers between devices, sent_together(): lax.all_gather(both, axis, axis=dim, tiled=True)  83.5 us
    all_to_all x1, blocking collectives, copy_for_each(): lax.all_to_all(jnp.broadcast_to(array[None], (length, *array.shape)), axi...  28.6 us
    all_to_all x1, blocking collectives, on_device(): lax.all_to_all(combined, 'sp', split_axis=0, concat_axis=0, tiled=True)  28.2 us
    all_to_all x1, blocking collectives, on_device(): lax.all_to_all(outgoing, 'sp', split_axis=0, concat_axis=0, tiled=True)  27.4 us
    reduce_scatter x1, waiting for transfers between devices, on_device(): lax.psum_scatter(partials.astype(jnp.bfloat16), 'tp', scatter_dimension=0...  27.4 us
    another operation x2, local copies, waits for them, and re-layouts  10.9 us
    all_to_all x1, waiting for transfers between devices, sent_and_summed(): lax.all_to_all(in_blocks(array, dim, length), axis, 0, 0, tiled=True)  8.57 us
    dot_general x1, matrix products, on_device(): jnp.einsum('secf,efd->secd', hidden, down_weights, preferred_element_type...  6.05 us
  transfers between devices with their start and end apart: 3, of which 3 were waited for; matrix products, arithmetic and copies ran while one was open for 1% of the time, Pallas kernels for 0%

commit v1 on v0

v1 whole, which is shorter than its diff:
```python
import functools

import jax
import jax.numpy as jnp
import numpy as np
from jax import lax
from jax.experimental import pallas as pl
from jax.experimental.pallas import tpu as pltpu
from jax.sharding import Mesh
from jax.sharding import PartitionSpec as P

NZ, NX, NC, NY = 8, 4, 2, 4
NXC = NX * NC
ROWS = 128
TOK = 32
D = 2048
NOPE_S = 64
NOPE_L = 128
ROPE = 32
EXPERTS = 64
CAP = 2
SLOTS = EXPERTS * CAP
FF_LOCAL = 512
EPS = 1e-6
LIMIT = 7.0
ALPHA = 1.702
ROPE_BASE = 10000.0
MASKED = -float(2**99)
LOG2E = 1.4426950408889634
SCALE_S = (NOPE_S + ROPE) ** -0.5 * LOG2E
SCALE_L = (NOPE_L + ROPE) ** -0.5 * LOG2E

f32 = jnp.float32
bf16 = jnp.bfloat16


def rope_parts():
    freq = ROPE_BASE ** (-np.arange(ROPE // 2, dtype=np.float64) * (2.0 / ROPE))

    def table(places):
        angles = places[:, None].astype(np.float64) * freq[None, :]
        c, s = np.cos(angles), np.sin(angles)
        return np.concatenate([c, c, s, s], axis=1).astype(np.float32)

    return table(np.arange(64) * ROWS), table(np.arange(ROWS))


def vmem(n):
    return [pl.BlockSpec(memory_space=pltpu.VMEM) for _ in range(n)]


def smem():
    return pl.BlockSpec(memory_space=pltpu.SMEM)


def pre_kernel(
    place_ref, lat_ref, gain_ref, rk_ref, qs_ref, ql_ref, ks_w, vs_w, kl_w, vl_w,
    base_ref, row_ref, kv_ref, q_ref,
):
    block = (place_ref[0] * NX + place_ref[1]) * NC + place_ref[2]
    base = base_ref[pl.ds(block, 1), :]
    row = row_ref[...]
    cb, sb = base[:, :ROPE], base[:, ROPE:]
    cr, sr = row[:, :ROPE], row[:, ROPE:]
    cos = cr * cb - sr * sb
    sin = sr * cb + cr * sb
    lane = lax.broadcasted_iota(jnp.int32, (ROWS, ROPE), 1)
    sin = jnp.where(lane < ROPE // 2, -sin, sin)

    def turned(v):
        v = v.astype(f32)
        swapped = jnp.concatenate([v[:, ROPE // 2 :], v[:, : ROPE // 2]], axis=1)
        return (v * cos + swapped * sin).astype(bf16)

    lat = lat_ref[...].astype(f32)
    scale = lax.rsqrt(jnp.mean(lat * lat, axis=1, keepdims=True) + EPS)
    normed = (lat * scale * gain_ref[...]).astype(bf16)

    def proj(w_ref):
        return jnp.dot(normed, w_ref[...], preferred_element_type=f32).astype(bf16)

    kv_ref[0:128, :] = proj(kl_w)
    kv_ref[128:256, :] = proj(vl_w)
    kv_ref[256:384, :] = jnp.concatenate([proj(ks_w), proj(vs_w)], axis=1)
    rot = turned(rk_ref[...])
    kv_ref[384:416, :] = jnp.concatenate([rot[32 * i : 32 * i + 32] for i in range(4)], axis=1)
    ql = ql_ref[...]
    qs = qs_ref[...]
    q_ref[0:128, :] = ql[:, :NOPE_L]
    q_ref[128:256, :] = jnp.concatenate(
        [qs[:, :NOPE_S], turned(ql[:, NOPE_L:]), turned(qs[:, NOPE_S:])], axis=1
    )


def attn_kernel(
    place_ref, k0, k1, k2, k3, k4, k5, k6, k7a, k7b, q0, q1, q2, q3, r_ref, out_ref,
    kl, ks, vl, vs,
):
    z, x, c = place_ref[0], place_ref[1], place_ref[2]
    ones = jnp.ones((ROWS, 128), bf16)
    zero32 = jnp.zeros((ROWS, 32), bf16)
    zero64 = jnp.zeros((ROWS, 64), bf16)
    blocks = [(k, k, 256) for k in (k0, k1, k2, k3, k4, k5, k6)] + [(k7a, k7b, 0)]
    for j, (front, back, at) in enumerate(blocks):
        lo, hi = j * ROWS, (j + 1) * ROWS
        small = back[at : at + 128, :]
        packed = back[at + 128 : at + 160, :]
        rot = jnp.concatenate([packed[:, 32 * i : 32 * i + 32] for i in range(4)], axis=0)
        kl[lo:hi, 0:128] = front[0:128, :]
        kl[lo:hi, 128:256] = jnp.concatenate([zero64, rot, zero32], axis=1)
        ks[lo:hi, :] = jnp.concatenate([small[:, :64], zero32, rot], axis=1)
        vl[lo:hi, 0:128] = front[128:256, :]
        vl[lo:hi, 128:256] = ones
        vs[lo:hi, 0:128] = small
        vs[lo:hi, 128:256] = ones
    shifts = (0, 1, 7, 2, 6, 3, 5, 4)
    lane = lax.broadcasted_iota(jnp.int32, (1, 128), 1)
    own = (x * NC + c) * ROWS
    kpos = jnp.concatenate(
        [lax.rem(z + (NZ - s), NZ) * (NXC * ROWS) + own + lane for s in shifts], axis=1
    )
    row = lax.broadcasted_iota(jnp.int32, (2 * ROWS, 1), 0)
    lanes = lax.broadcasted_iota(jnp.int32, (2 * ROWS, 128), 1)
    for d, (shift, mine) in enumerate(((0, q0), (1, q1), (3, q2), (2, q3))):
        xq = lax.rem(x + (NX - shift), NX)
        b_mine = xq * NC + c
        b_other = xq * NC + (1 - c)
        q = jnp.concatenate(
            [
                jnp.concatenate([mine[0:128, :], mine[128:256, :]], axis=1),
                jnp.concatenate([r_ref[d, 0:128, :], r_ref[d, 128:256, :]], axis=1),
            ],
            axis=0,
        )
        qpos = z * (NXC * ROWS) + jnp.where(
            row < ROWS, b_mine * ROWS + row, b_other * ROWS + row - ROWS
        )
        allowed = kpos <= qpos

        def attend(query, keys, values, scale):
            s = lax.dot_general(
                query, keys[...], (((1,), (1,)), ((), ())), preferred_element_type=f32
            )
            s = jnp.where(allowed, s, MASKED)
            top = jnp.max(s, axis=1, keepdims=True).astype(bf16).astype(f32)
            w = jnp.exp2((s - top) * scale).astype(bf16)
            o = jnp.dot(w, values[...], preferred_element_type=f32)
            total = o[:, 128:129]
            return o[:, :128] / total, top, total

        o_l, m_l, t_l = attend(q, kl, vl, SCALE_L)
        o_s, m_s, t_s = attend(q[:, 128:256], ks, vs, SCALE_S)
        h_l = t_l.astype(bf16).astype(f32)
        h_s = t_s.astype(bf16).astype(f32)
        for i, v in enumerate((m_l, h_l, t_l - h_l, m_s, h_s, t_s - h_s)):
            o_s = jnp.where(lanes == i, v, o_s)
        o_l = o_l.astype(bf16)
        o_s = o_s.astype(bf16)
        for half, b in ((0, b_mine), (1, b_other)):
            for y in range(NY):
                lo = half * ROWS + y * TOK
                out_ref[b, y, 0:TOK, :] = o_l[lo : lo + TOK]
                out_ref[b, y, TOK : 2 * TOK, :] = o_s[lo : lo + TOK]


def mid_kernel(
    place_ref, parts_ref, w0, w1, w3, w2a, w2b, res_ref, gain_ref, routing_ref,
    disp_ref, mid_ref, pick_ref,
):
    y = place_ref[3]
    total = jnp.zeros((TOK, D), f32)
    for shift, weights in ((0, (w0, w0, 96)), (1, (w1, w1, 96)), (3, (w3, w3, 96)), (2, (w2a, w2b, 0))):
        ya = lax.rem(y + (NY - shift), NY)
        larges = [parts_ref[i, ya, 0:TOK, :].astype(f32) for i in range(NXC)]
        smalls = [parts_ref[i, ya, TOK : 2 * TOK, :].astype(f32) for i in range(NXC)]

        def mixed(values, at, scale):
            tops = [s[:, at : at + 1] for s in smalls]
            top = functools.reduce(jnp.maximum, tops)
            ws = [
                (s[:, at + 1 : at + 2] + s[:, at + 2 : at + 3]) * jnp.exp2((t - top) * scale)
                for s, t in zip(smalls, tops)
            ]
            inv = 1.0 / functools.reduce(jnp.add, ws)
            return functools.reduce(jnp.add, [v * (w * inv) for v, w in zip(values, ws)])

        large = mixed(larges, 0, SCALE_L).astype(bf16)
        small = mixed(smalls, 3, SCALE_S)[:, 64:128].astype(bf16)
        heads = jnp.concatenate([large, small], axis=1)
        first, second, at = weights
        partial = jnp.dot(heads[:, :96], first[0:96, :], preferred_element_type=f32)
        partial = partial + jnp.dot(
            heads[:, 96:192], second[at : at + 96, :], preferred_element_type=f32
        )
        total = total + partial.astype(bf16).astype(f32)
    attention = total.astype(bf16).astype(f32)
    middle = (res_ref[...].astype(f32) + attention).astype(bf16)
    mid_ref[...] = middle
    wide = middle.astype(f32)
    scale = lax.rsqrt(jnp.mean(wide * wide, axis=1, keepdims=True) + EPS)
    normed = (wide * scale * gain_ref[...]).astype(bf16)

    lane = lax.broadcasted_iota(jnp.int32, (TOK, SLOTS), 1)
    r = [routing_ref[:, k : k + 1] for k in range(2)]
    hit = [lane == rk for rk in r]
    named = jnp.where(hit[0] | hit[1], 1.0, 0.0)
    tri = jnp.where(
        lax.broadcasted_iota(jnp.int32, (TOK, TOK), 1)
        < lax.broadcasted_iota(jnp.int32, (TOK, TOK), 0),
        1.0,
        0.0,
    )
    earlier = jnp.dot(tri.astype(bf16), named.astype(bf16), preferred_element_type=f32)
    send = jnp.zeros((TOK, SLOTS), f32)
    for k in range(2):
        slot = jnp.sum(jnp.where(hit[k], earlier, 0.0), axis=1, keepdims=True)
        pick = jnp.where(lane == r[k] * CAP + slot.astype(jnp.int32), 1.0, 0.0)
        pick_ref[k] = pick.astype(bf16)
        send = send + pick
    disp_ref[...] = lax.dot_general(
        send.astype(bf16), normed, (((0,), (0,)), ((), ())), preferred_element_type=f32
    ).astype(bf16)


def ffn_kernel(*refs):
    count = (len(refs) - 3) // 2
    xs, (wg, wu, wd), outs = refs[:count], refs[count : count + 3], refs[count + 3 :]
    rows = jnp.concatenate([x[...] for x in xs], axis=0) if count > 1 else xs[0][...]
    gate = jnp.dot(rows, wg[...], preferred_element_type=f32)
    up = jnp.dot(rows, wu[...], preferred_element_type=f32)
    m = jnp.minimum(gate, LIMIT)
    linear = jnp.clip(up, -LIMIT, LIMIT) + 1.0
    hidden = (m * jax.nn.sigmoid(ALPHA * m) * linear).astype(bf16)
    out = jnp.dot(hidden, wd[...], preferred_element_type=f32).astype(bf16)
    at = 0
    for x, o in zip(xs, outs):
        o[...] = out[at : at + x.shape[0]]
        at += x.shape[0]


def end_kernel(mid_ref, pick_ref, ret_ref, weight_ref, out_ref):
    total = mid_ref[...].astype(f32)
    ret = ret_ref[...]
    mixed = weight_ref[:, 0:1] * jnp.dot(pick_ref[0], ret, preferred_element_type=f32)
    mixed = mixed + weight_ref[:, 1:2] * jnp.dot(pick_ref[1], ret, preferred_element_type=f32)
    out_ref[...] = (total + mixed).astype(bf16)


def call(kernel, in_specs, shapes, scratch=(), flops=0):
    many = len(shapes) > 1
    outs = [jax.ShapeDtypeStruct(s, d) for s, d in shapes]
    return pl.pallas_call(
        kernel,
        in_specs=in_specs,
        out_specs=vmem(len(outs)) if many else vmem(1)[0],
        out_shape=outs if many else outs[0],
        scratch_shapes=list(scratch),
        compiler_params=pltpu.CompilerParams(vmem_limit_bytes=56 * 2**20),
        cost_estimate=pl.CostEstimate(flops=flops, transcendentals=0, bytes_accessed=0)
        if flops
        else None,
    )


def shifted(a, axis, size, by):
    return lax.ppermute(a, axis, [(i, (i + by) % size) for i in range(size)])


def on_device(
    residual, query_small, query_large, latent, rotary_key, latent_gain,
    small_keys, small_values, large_keys, large_values, small_output, large_output,
    ffn_gain, gate_weights, up_weights, down_weights, routing, route_weight,
):
    place = jnp.stack([lax.axis_index(a) for a in ("z", "x", "c", "y")]).astype(jnp.int32)
    base, row = rope_parts()
    kv, q = call(
        pre_kernel, [smem()] + vmem(11), [((416, 128), bf16), ((256, 128), bf16)]
    )(
        place, latent, latent_gain[None, :], rotary_key, query_small, query_large,
        small_keys, small_values, large_keys, large_values, base, row,
    )

    plus = minus = kv
    blocks = [kv]
    for _ in range(3):
        plus = shifted(plus, "z", NZ, 1)
        minus = shifted(minus, "z", NZ, -1)
        blocks += [plus, minus]
    blocks += [shifted(plus[:256], "z", NZ, 1), shifted(minus[256:], "z", NZ, -1)]

    qx = [q] + [shifted(q, "x", NX, s) for s in (1, -1, 2)]
    qc = shifted(jnp.stack(qx), "c", NC, 1)

    wo = jnp.concatenate([large_output, small_output], axis=0)
    wo_p = shifted(wo, "y", NY, 1)
    wo_m = shifted(wo, "y", NY, -1)
    wo_a = shifted(wo_p[:96], "y", NY, 1)
    wo_b = shifted(wo_m[96:], "y", NY, -1)

    parts = call(
        attn_kernel,
        [smem()] + vmem(14),
        [((NXC, NY, 2 * TOK, 128), bf16)],
        scratch=[
            pltpu.VMEM((1024, 256), bf16),
            pltpu.VMEM((1024, 128), bf16),
            pltpu.VMEM((1024, 256), bf16),
            pltpu.VMEM((1024, 256), bf16),
        ],
    )(place, *blocks, *qx, qc)
    parts = lax.all_to_all(
        parts.reshape(NXC * NY * 2 * TOK, 128), ("x", "c", "y"), 0, 0, tiled=True
    ).reshape(NXC, NY, 2 * TOK, 128)

    disp, middle, pick = call(
        mid_kernel,
        [smem()] + vmem(9),
        [((SLOTS, D), bf16), ((TOK, D), bf16), ((2, TOK, SLOTS), bf16)],
    )(place, parts, wo, wo_p, wo_m, wo_a, wo_b, residual, ffn_gain[None, :], routing)

    sp = ("z", "x", "c")
    mine = lax.all_to_all(disp.reshape(EXPERTS, CAP, D), sp, 0, 0, tiled=True)
    mine = mine.reshape(SLOTS, D)

    half = SLOTS // 2
    x_a, x_b = mine[:half], mine[half:]
    weights = (gate_weights[0], up_weights[0], down_weights[0])

    def ffn(*pieces):
        return call(
            ffn_kernel,
            vmem(len(pieces) + 3),
            [(p.shape, bf16) for p in pieces],
        )(*pieces, *weights)

    p_a = shifted(x_a, "y", NY, 1)
    m_b = shifted(x_b, "y", NY, -1)
    p_b = shifted(x_b, "y", NY, 1)
    m_a = shifted(x_a, "y", NY, -1)
    o_a = shifted(p_a, "y", NY, 1)
    o_b = shifted(m_b, "y", NY, -1)
    r0_a, r0_b = ffn(x_a, x_b)
    r1_a, r1_b, r3_a, r3_b = ffn(p_a, p_b, m_a, m_b)
    r2_a, r2_b = ffn(o_a, o_b)

    from_m_b = shifted(r3_b, "y", NY, 1)
    from_p_a = shifted(r1_a, "y", NY, -1)
    t_a = shifted(r2_a, "y", NY, 1)
    t_b = shifted(r2_b, "y", NY, -1)
    r3_a = (r3_a.astype(f32) + t_a.astype(f32)).astype(bf16)
    r1_b = (r1_b.astype(f32) + t_b.astype(f32)).astype(bf16)
    from_m_a = shifted(r3_a, "y", NY, 1)
    from_p_b = shifted(r1_b, "y", NY, -1)
    done = jnp.concatenate(
        [
            r0_a.astype(f32) + from_m_a.astype(f32) + from_p_a.astype(f32),
            r0_b.astype(f32) + from_m_b.astype(f32) + from_p_b.astype(f32),
        ],
        axis=0,
    ).astype(bf16)
    ret = lax.all_to_all(done.reshape(EXPERTS, CAP, D), sp, 0, 0, tiled=True)
    return call(end_kernel, vmem(4), [((TOK, D), bf16)])(
        middle, pick, ret.reshape(SLOTS, D), route_weight
    )


def solution(mesh):
    fine = Mesh(mesh.devices.reshape(NZ, NX, NC, NY), ("z", "x", "c", "y"))
    sp = ("z", "x", "c")
    every = ("z", "x", "c", "y")
    return jax.shard_map(
        on_device,
        mesh=fine,
        in_specs=(
            P(every, None),
            P(sp, "y"),
            P(sp, "y"),
            P(sp, None),
            P(sp, None),
            P(),
            P(None, "y"),
            P(None, "y"),
            P(None, "y"),
            P(None, "y"),
            P("y", None),
            P("y", None),
            P(),
            P(sp, None, "y"),
            P(sp, None, "y"),
            P(sp, "y", None),
            P(every, None),
            P(every, None),
        ),
        out_specs=P(every, None),
        check_vma=False,
    )
```

time: 279 us -> 200 us (0.72)
  waiting for transfers between devices: 119 us -> 50.8 us
  starting transfers between devices: 4 us -> 67.7 us
  blocking collectives: 84.3 us -> 27.4 us
  Pallas kernels: 0 us -> 31 us
  matrix products: 26.6 us -> 0 us
  between operations: 13.6 us -> 0.37 us
  other arithmetic: 10.2 us -> 3.75 us
    all_gather x1 -> x0, waiting for transfers between devices: 83.5 us -> none  [sent_together(): lax.all_gather(both, axis, axis=dim, tiled=True)]
    all_to_all x3 -> x1, blocking collectives: 84.3 us -> 27.4 us  [on_device(): mine = lax.all_to_all(disp.reshape(EXPERTS, CAP, D), sp, 0, 0, tiled=True)]
    ppermute x0 -> x28, starting transfers between devices: none -> 47.8 us  [shifted(): return lax.ppermute(a, axis, [(i, (i + by) % size) for i in range(size)])]
    pallas_call x0 -> x7, Pallas kernels: none -> 31 us  [the longest x3 15.9 us: ffn(): call(ffn_kernel, vmem(len(pieces) + 3), [(p.shape, bf16) for p in pieces])]
    reduce_scatter x1 -> x0, waiting for transfers between devices: 27.4 us -> none  [on_device(): lax.psum_scatter(partials.astype(jnp.bfloat16), 'tp', scatter_dimension=0...]
    ppermute x0 -> x28, waiting for transfers between devices: none -> 27 us  [shifted(): return lax.ppermute(a, axis, [(i, (i + by) % size) for i in range(size)])]
    dot_general x16 -> x0, matrix products: 26.6 us -> none  [the longest x1 6.05 us: on_device(): jnp.einsum('secf,efd->secd', hidden, down_weights, preferred_element_type...]
    all_to_all x1 -> x2, starting transfers between devices: 4 us -> 19.8 us  [the longest x1 11.2 us: on_device(): ret = lax.all_to_all(done.reshape(EXPERTS, CAP, D), sp, 0, 0, tiled=True)]
  transfers between devices with their start and end apart: 3 -> 30, of which waited for: 3 -> 13; matrix products, arithmetic and copies ran while one was open for 1% -> 6% of each run, Pallas kernels for 0% -> 12%
where the time goes in v1:
time: 200 us
  starting transfers between devices  67.7 us (34%)
  waiting for transfers between devices  50.8 us (25%)
  Pallas kernels  31 us (16%)
  blocking collectives  27.4 us (14%)
  local copies, waits for them, and re-layouts  18.8 us (9%)
  other arithmetic  3.75 us (2%)
    ppermute x28, starting transfers between devices, shifted(): return lax.ppermute(a, axis, [(i, (i + by) % size) for i in range(size)])  47.8 us
    all_to_all x1, blocking collectives, on_device(): mine = lax.all_to_all(disp.reshape(EXPERTS, CAP, D), sp, 0, 0, tiled=True)  27.4 us
    ppermute x28, waiting for transfers between devices, shifted(): return lax.ppermute(a, axis, [(i, (i + by) % size) for i in range(size)])  27 us
    all_to_all x1, waiting for transfers between devices, on_device(): ret = lax.all_to_all(done.reshape(EXPERTS, CAP, D), sp, 0, 0, tiled=True)  17 us
    pallas_call x3, Pallas kernels, ffn(): call(ffn_kernel, vmem(len(pieces) + 3), [(p.shape, bf16) for p in pieces])  15.9 us
    unnamed x74, local copies, waits for them, and re-layouts  12.9 us
    all_to_all x1, starting transfers between devices, on_device(): ret = lax.all_to_all(done.reshape(EXPERTS, CAP, D), sp, 0, 0, tiled=True)  11.2 us
    all_to_all x1, starting transfers between devices, on_device(): lax.all_to_all(parts.reshape(NXC * NY * 2 * TOK, 128), ('x', 'c', 'y'), 0...  8.69 us
  transfers between devices with their start and end apart: 30, of which 13 were waited for; matrix products, arithmetic and copies ran while one was open for 6% of the time, Pallas kernels for 12%

profile of v1, /device:TPU:1, one launch (start us, length us, event | category | flops | bytes accessed | tf_op | source)
XLA Modules:
  0.0 199.7 jit_solution(6154675892977187812)
XLA Ops:
  2.1 2.2 %collective-permute-start.12 = (bf16[192,2048]{1,0:T(8,128)(2,1)S(1)}, bf16[192,2048]{1,0:T(8,128)(2,1)S(1)}, u32[]{:S(2)}, u32[]{:S(2)}) collective-permute-start(bf16[192,2048]{1,0:T(8,128)(2,1)S(1)} %constant_dynamic-update-slice_fusion.w0), channel_id=1, source_target_pairs={{0,1},{1,2},{2,3},{3,0},{4,5},{5,6},{6,7},{7,4},{8,9},{9,10},{10,1... | collective-permute-start | bytes 2359304 | tf_op jit(solution)/shard_map/ppermute | solution.py:266
  7.4 1.6 copy.25.vs_w
  12.5 2.4 %shard_map.190 = (bf16[416,128]{1,0:T(8,128)(2,1)}, bf16[256,128]{1,0:T(8,128)(2,1)}) custom-call(s32[4]{0:T(128)} %pad_add_fusion.place_ref, bf16[128,512]{1,0:T(8,128)(2,1)} %lat_ref.1, f32[1,512]{1,0:T(1,128)} %bitcast.31, bf16[128,32]{1,0:T(8,128)(2,1)} %copy.21.rk_ref, bf16[128,96]{1,0:T(8,128)(2,1)} %copy.22.qs_ref, bf16[128,160]{1,0:T(8,128)(2,1)} %copy.23.ql_ref, ...), custom_call_target="tpu_custom_call" | custom-call | tf_op jit(solution)/shard_map/pallas_call | solution.py:276
  16.1 1.6 collective-permute-start
  21.4 5.5 %collective-permute-start.1 = (bf16[416,128]{1,0:T(8,128)(2,1)}, bf16[416,128]{1,0:T(8,128)(2,1)S(1)}, u32[]{:S(2)}, u32[]{:S(2)}) collective-permute-start(bf16[416,128]{1,0:T(8,128)(2,1)} %get-tuple-element.18.k0), channel_id=1, source_target_pairs={{0,224},{32,0},{64,32},{96,64},{128,96},{160,128},{192,160},{224,1... | collective-permute-start | bytes 319496 | tf_op jit(solution)/shard_map/ppermute | solution.py:266
  27.8 2.6 %collective-permute-start.11 = (bf16[4,256,128]{2,1,0:T(8,128)(2,1)S(1)}, bf16[4,256,128]{2,1,0:T(8,128)(2,1)S(1)}, u32[]{:S(2)}, u32[]{:S(2)}) collective-permute-start(bf16[4,256,128]{2,1,0:T(8,128)(2,1)S(1)} %pad_maximum_fusion.1), channel_id=1, source_target_pairs={{0,4},{4,0},{1,5},{5,1},{2,6},{6,2},{3,7},{7,3},{8,12},{12,8},{9,1... | collective-permute-start | bytes 786440 | tf_op jit(solution)/shard_map/ppermute | solution.py:266
  30.4 3.8 %collective-permute-start.3 = (bf16[416,128]{1,0:T(8,128)(2,1)S(1)}, bf16[416,128]{1,0:T(8,128)(2,1)S(1)}, u32[]{:S(2)}, u32[]{:S(2)}) collective-permute-start(bf16[416,128]{1,0:T(8,128)(2,1)S(1)} %collective-permute-done.1.k2), channel_id=1, source_target_pairs={{0,224},{32,0},{64,32},{96,64},{128,96},{160,128},{192,160},{224,1... | collective-permute-start | bytes 319496 | tf_op jit(solution)/shard_map/ppermute | solution.py:266
  34.3 1.7 collective-permute-done.3.k4
  36.0 3.0 %collective-permute-start.5 = (bf16[416,128]{1,0:T(8,128)(2,1)S(1)}, bf16[416,128]{1,0:T(8,128)(2,1)S(1)}, u32[]{:S(2)}, u32[]{:S(2)}) collective-permute-start(bf16[416,128]{1,0:T(8,128)(2,1)S(1)} %collective-permute-done.3.k4), channel_id=1, source_target_pairs={{0,224},{32,0},{64,32},{96,64},{128,96},{160,128},{192,160},{224,1... | collective-permute-start | bytes 319496 | tf_op jit(solution)/shard_map/ppermute | solution.py:266
  40.7 3.3 %collective-permute-start.7 = (bf16[160,128]{1,0:T(8,128)(2,1)S(1)}, bf16[160,128]{1,0:T(8,128)(2,1)S(1)}, u32[]{:S(2)}, u32[]{:S(2)}) collective-permute-start(bf16[160,128]{1,0:T(8,128)(2,1)S(1)} %slice.33), channel_id=1, source_target_pairs={{0,224},{32,0},{64,32},{96,64},{128,96},{160,128},{192,160},{224,1... | collective-permute-start | bytes 122888 | tf_op jit(solution)/shard_map/ppermute | solution.py:266
  46.4 5.9 %shard_map.191 = bf16[8,4,64,128]{3,2,1,0:T(8,128)(2,1)} custom-call(s32[4]{0:T(128)} %pad_add_fusion.place_ref, bf16[416,128]{1,0:T(8,128)(2,1)} %get-tuple-element.18.k0, bf16[416,128]{1,0:T(8,128)(2,1)} %copy-done.22, bf16[416,128]{1,0:T(8,128)(2,1)} %copy-done.23, bf16[416,128]{1,0:T(8,128)(2,1)} %copy-done.24, bf16[416,128]{1,0:T(8,128)(2,1)} %copy-done.25, ...), custom_call_target="tpu_custom_call" | custom-call | tf_op jit(solution)/shard_map/pallas_call | solution.py:300
  52.2 8.7 %all-to-all-start = ((bf16[32,64,128]{2,1,0:T(8,128)(2,1)}), bf16[32,64,128]{2,1,0:T(8,128)(2,1)S(1)}, u32[]{:S(2)}, u32[]{:S(2)}) async-start(bf16[32,64,128]{2,1,0:T(8,128)(2,1)} %bitcast.25), calls=%async_computation | async-start | bytes 1048576 | tf_op jit(solution)/shard_map/all_to_all | solution.py:311
  65.3 6.8 %all-to-all-done = bf16[32,64,128]{2,1,0:T(8,128)(2,1)S(1)} async-done(((bf16[32,64,128]{2,1,0:T(8,128)(2,1)}), bf16[32,64,128]{2,1,0:T(8,128)(2,1)S(1)}, u32[]{:S(2)}, u32[]{:S(2)}) %all-to-all-start) | async-done | bytes 524320 | tf_op jit(solution)/shard_map/all_to_all | solution.py:311
  72.1 6.9 %collective-permute-done.14.w2a = bf16[96,2048]{1,0:T(8,128)(2,1)S(1)} collective-permute-done((bf16[96,2048]{1,0:T(8,128)(2,1)}, bf16[96,2048]{1,0:T(8,128)(2,1)S(1)}, u32[]{:S(2)}, u32[]{:S(2)}) %collective-permute-start.14) | collective-permute-done | bytes 393248 | tf_op jit(solution)/shard_map/ppermute | solution.py:266
  79.8 4.8 %shard_map.192 = (bf16[128,2048]{1,0:T(8,128)(2,1)}, bf16[32,2048]{1,0:T(8,128)(2,1)}, bf16[2,32,128]{2,1,0:T(8,128)(2,1)}) custom-call(s32[4]{0:T(128)} %pad_add_fusion.place_ref, bf16[8,4,64,128]{3,2,1,0:T(8,128)(2,1)} %bitcast.24, bf16[192,2048]{1,0:T(8,128)(2,1)} %copy-done, bf16[192,2048]{1,0:T(8,128)(2,1)} %copy-done.2, bf16[192,2048]{1,0:T(8,128)(2,1)} %copy-done.3, ...), custom_call_target="tpu_custom_call" | custom-call | tf_op jit(solution)/shard_map/pallas_call | solution.py:315
  86.0 27.4 %all_to_all.19 = bf16[64,2,2048]{2,1,0:T(2,128)(2,1)S(1)} all-to-all(bf16[64,2,2048]{2,1,0:T(2,128)(2,1)S(1)} %reshape.21), channel_id=1, replica_groups=mesh['z'=8,'x'=4,'c'=2,'y'=4] {'z','x','c'}, dimensions={0} | all-to-all | bytes 1048576 | tf_op jit(solution)/shard_map/all_to_all | solution.py:322
  114.1 2.7 %collective-permute-start.19 = (bf16[64,2048]{1,0:T(8,128)(2,1)S(1)}, bf16[64,2048]{1,0:T(8,128)(2,1)S(1)}, u32[]{:S(2)}, u32[]{:S(2)}) collective-permute-start(bf16[64,2048]{1,0:T(8,128)(2,1)S(1)} %slice.31.refs_1_), channel_id=1, source_target_pairs={{0,3},{1,0},{2,1},{3,2},{4,7},{5,4},{6,5},{7,6},{8,11},{9,8},{10,9... | collective-permute-start | bytes 786440 | tf_op jit(solution)/shard_map/ppermute | solution.py:266
  116.8 5.8 %collective-permute-done.16.refs_0_ = bf16[64,2048]{1,0:T(8,128)(2,1)S(1)} collective-permute-done((bf16[64,2048]{1,0:T(8,128)(2,1)S(1)}, bf16[64,2048]{1,0:T(8,128)(2,1)S(1)}, u32[]{:S(2)}, u32[]{:S(2)}) %collective-permute-start.16) | collective-permute-done | bytes 262176 | tf_op jit(solution)/shard_map/ppermute | solution.py:266
  122.7 2.7 %collective-permute-start.21 = (bf16[64,2048]{1,0:T(8,128)(2,1)S(1)}, bf16[64,2048]{1,0:T(8,128)(2,1)S(1)}, u32[]{:S(2)}, u32[]{:S(2)}) collective-permute-start(bf16[64,2048]{1,0:T(8,128)(2,1)S(1)} %collective-permute-done.19.refs_3_), channel_id=1, source_target_pairs={{0,3},{1,0},{2,1},{3,2},{4,7},{5,4},{6,5},{7,6},{8,11},{9,8},{10,9... | collective-permute-start | bytes 786440 | tf_op jit(solution)/shard_map/ppermute | solution.py:266
  125.3 2.7 %collective-permute-start.18 = (bf16[64,2048]{1,0:T(8,128)(2,1)S(1)}, bf16[64,2048]{1,0:T(8,128)(2,1)S(1)}, u32[]{:S(2)}, u32[]{:S(2)}) collective-permute-start(bf16[64,2048]{1,0:T(8,128)(2,1)S(1)} %slice.29.refs_0_), channel_id=1, source_target_pairs={{0,3},{1,0},{2,1},{3,2},{4,7},{5,4},{6,5},{7,6},{8,11},{9,8},{10,9... | collective-permute-start | bytes 786440 | tf_op jit(solution)/shard_map/ppermute | solution.py:266
  128.0 2.5 %collective-permute-done.20.refs_0_ = bf16[64,2048]{1,0:T(8,128)(2,1)S(1)} collective-permute-done((bf16[64,2048]{1,0:T(8,128)(2,1)S(1)}, bf16[64,2048]{1,0:T(8,128)(2,1)S(1)}, u32[]{:S(2)}, u32[]{:S(2)}) %collective-permute-start.20) | collective-permute-done | bytes 262176 | tf_op jit(solution)/shard_map/ppermute | solution.py:266
  131.3 4.9 %shard_map.195 = (bf16[64,2048]{1,0:T(8,128)(2,1)}, bf16[64,2048]{1,0:T(8,128)(2,1)}) custom-call(bf16[64,2048]{1,0:T(8,128)(2,1)} %copy-done.19, bf16[64,2048]{1,0:T(8,128)(2,1)} %copy-done.20, bf16[2048,512]{1,0:T(8,128)(2,1)} %bitcast.15, bf16[2048,512]{1,0:T(8,128)(2,1)} %bitcast.18, bf16[512,2048]{1,0:T(8,128)(2,1)} %bitcast.21), custom_call_target="tpu_custom_call" | custom-call | tf_op jit(solution)/shard_map/pallas_call | solution.py:330
  136.3 4.9 %shard_map.193 = (bf16[64,2048]{1,0:T(8,128)(2,1)}, bf16[64,2048]{1,0:T(8,128)(2,1)}) custom-call(bf16[64,2048]{1,0:T(8,128)(2,1)} %copy-done.4, bf16[64,2048]{1,0:T(8,128)(2,1)} %copy-done.5, bf16[2048,512]{1,0:T(8,128)(2,1)} %bitcast.16, bf16[2048,512]{1,0:T(8,128)(2,1)} %bitcast.19, bf16[512,2048]{1,0:T(8,128)(2,1)} %bitcast.22), custom_call_target="tpu_custom_call" | custom-call | tf_op jit(solution)/shard_map/pallas_call | solution.py:330
  142.6 6.0 %shard_map.194 = (bf16[64,2048]{1,0:T(8,128)(2,1)}, bf16[64,2048]{1,0:T(8,128)(2,1)}, bf16[64,2048]{1,0:T(8,128)(2,1)}, bf16[64,2048]{1,0:T(8,128)(2,1)}) custom-call(bf16[64,2048]{1,0:T(8,128)(2,1)} %copy-done.9, bf16[64,2048]{1,0:T(8,128)(2,1)} %copy-done.11, bf16[64,2048]{1,0:T(8,128)(2,1)} %copy-done.12, bf16[64,2048]{1,0:T(8,128)(2,1)} %copy-done.10, ...), custom_call_target="tpu_custom_call" | custom-call | tf_op jit(solution)/shard_map/pallas_call | solution.py:330
  148.6 2.7 %collective-permute-start.24 = (bf16[64,2048]{1,0:T(8,128)(2,1)}, bf16[64,2048]{1,0:T(8,128)(2,1)S(1)}, u32[]{:S(2)}, u32[]{:S(2)}) collective-permute-start(bf16[64,2048]{1,0:T(8,128)(2,1)} %get-tuple-element.26), channel_id=1, source_target_pairs={{0,3},{1,0},{2,1},{3,2},{4,7},{5,4},{6,5},{7,6},{8,11},{9,8},{10,9... | collective-permute-start | bytes 786440 | tf_op jit(solution)/shard_map/ppermute | solution.py:266
  151.3 2.7 %collective-permute-start.26 = (bf16[64,2048]{1,0:T(8,128)(2,1)S(1)}, bf16[64,2048]{1,0:T(8,128)(2,1)S(1)}, u32[]{:S(2)}, u32[]{:S(2)}) collective-permute-start(bf16[64,2048]{1,0:T(8,128)(2,1)S(1)} %copy-done.32), channel_id=1, source_target_pairs={{0,3},{1,0},{2,1},{3,2},{4,7},{5,4},{6,5},{7,6},{8,11},{9,8},{10,9... | collective-permute-start | bytes 786440 | tf_op jit(solution)/shard_map/ppermute | solution.py:266
  155.1 3.6 %collective-permute-done.26 = bf16[64,2048]{1,0:T(8,128)(2,1)S(1)} collective-permute-done((bf16[64,2048]{1,0:T(8,128)(2,1)S(1)}, bf16[64,2048]{1,0:T(8,128)(2,1)S(1)}, u32[]{:S(2)}, u32[]{:S(2)}) %collective-permute-start.26) | collective-permute-done | bytes 262176 | tf_op jit(solution)/shard_map/ppermute | solution.py:266
  159.7 3.5 %collective-permute-start.27 = (bf16[64,2048]{1,0:T(8,128)(2,1)S(1)}, bf16[64,2048]{1,0:T(8,128)(2,1)S(1)}, u32[]{:S(2)}, u32[]{:S(2)}) collective-permute-start(bf16[64,2048]{1,0:T(8,128)(2,1)S(1)} %add_convert_fusion.1), channel_id=1, source_target_pairs={{0,3},{1,0},{2,1},{3,2},{4,7},{5,4},{6,5},{7,6},{8,11},{9,8},{10,9... | collective-permute-start | bytes 786440 | tf_op jit(solution)/shard_map/ppermute | solution.py:266
  163.5 3.1 %collective-permute-done.27 = bf16[64,2048]{1,0:T(8,128)(2,1)S(1)} collective-permute-done((bf16[64,2048]{1,0:T(8,128)(2,1)S(1)}, bf16[64,2048]{1,0:T(8,128)(2,1)S(1)}, u32[]{:S(2)}, u32[]{:S(2)}) %collective-permute-start.27) | collective-permute-done | bytes 262176 | tf_op jit(solution)/shard_map/ppermute | solution.py:266
  167.8 11.2 %all-to-all-start.2 = ((bf16[64,2,2048]{2,1,0:T(2,128)(2,1)}), bf16[64,2,2048]{2,1,0:T(2,128)(2,1)S(1)}, u32[]{:S(2)}, u32[]{:S(2)}) async-start(bf16[64,2,2048]{2,1,0:T(2,128)(2,1)} %convert_element_type.53), calls=%async_computation.2 | async-start | bytes 1048576 | tf_op jit(solution)/shard_map/all_to_all | solution.py:361
  179.7 17.0 %all-to-all-done.2 = bf16[64,2,2048]{2,1,0:T(2,128)(2,1)S(1)} async-done(((bf16[64,2,2048]{2,1,0:T(2,128)(2,1)}), bf16[64,2,2048]{2,1,0:T(2,128)(2,1)S(1)}, u32[]{:S(2)}, u32[]{:S(2)}) %all-to-all-start.2) | async-done | bytes 524320 | tf_op jit(solution)/shard_map/all_to_all | solution.py:361
  197.7 2.1 %shard_map.196 = bf16[32,2048]{1,0:T(8,128)(2,1)} custom-call(bf16[32,2048]{1,0:T(8,128)(2,1)} %get-tuple-element.20.mid_ref, bf16[2,32,128]{2,1,0:T(8,128)(2,1)} %get-tuple-element.21.pick_ref, bf16[128,2048]{1,0:T(8,128)(2,1)} %reshape.22.ret_ref, f32[32,2]{1,0:T(8,128)} %copy.27.weight_ref), custom_call_target="tpu_custom_call" | custom-call | tf_op jit(solution)/shard_map/pallas_call | solution.py:362
  (128 shorter events, 33.3 us)
Async XLA Ops:
  2.1 50.2 %copy-start = (bf16[192,2048]{1,0:T(8,128)(2,1)}, bf16[192,2048]{1,0:T(8,128)(2,1)S(1)}, u32[]{:S(2)}) copy-start(bf16[192,2048]{1,0:T(8,128)(2,1)S(1)} %constant_dynamic-update-slice_fusion.w0) | copy-start | bytes 2359300
  2.1 58.9 %collective-permute-start.12 = (bf16[192,2048]{1,0:T(8,128)(2,1)S(1)}, bf16[192,2048]{1,0:T(8,128)(2,1)S(1)}, u32[]{:S(2)}, u32[]{:S(2)}) collective-permute-start(bf16[192,2048]{1,0:T(8,128)(2,1)S(1)} %constant_dynamic-update-slice_fusion.w0), channel_id=1, source_target_pairs={{0,1},{1,2},{2,3},{3,0},{4,5},{5,6},{6,7},{7,4},{8,9},{9,10},{10,1... | collective-permute-start | bytes 2359304 | tf_op jit(solution)/shard_map/ppermute | solution.py:266
  4.3 58.9 %collective-permute-start.13 = (bf16[192,2048]{1,0:T(8,128)(2,1)S(1)}, bf16[192,2048]{1,0:T(8,128)(2,1)S(1)}, u32[]{:S(2)}, u32[]{:S(2)}) collective-permute-start(bf16[192,2048]{1,0:T(8,128)(2,1)S(1)} %constant_dynamic-update-slice_fusion.w0), channel_id=1, source_target_pairs={{0,3},{1,0},{2,1},{3,2},{4,7},{5,4},{6,5},{7,6},{8,11},{9,8},{10,9... | collective-permute-start | bytes 2359304 | tf_op jit(solution)/shard_map/ppermute | solution.py:266
  14.9 4.8 %collective-permute-start.8 = (bf16[256,128]{1,0:T(8,128)(2,1)}, bf16[256,128]{1,0:T(8,128)(2,1)S(1)}, u32[]{:S(2)}, u32[]{:S(2)}) collective-permute-start(bf16[256,128]{1,0:T(8,128)(2,1)} %get-tuple-element.19.q0), channel_id=1, source_target_pairs={{0,8},{8,16},{16,24},{24,0},{1,9},{9,17},{17,25},{25,1},{2,10},{10... | collective-permute-start | bytes 196616 | tf_op jit(solution)/shard_map/ppermute | solution.py:266
  16.1 10.7 %collective-permute-start = (bf16[416,128]{1,0:T(8,128)(2,1)}, bf16[416,128]{1,0:T(8,128)(2,1)S(1)}, u32[]{:S(2)}, u32[]{:S(2)}) collective-permute-start(bf16[416,128]{1,0:T(8,128)(2,1)} %get-tuple-element.18.k0), channel_id=1, source_target_pairs={{0,32},{32,64},{64,96},{96,128},{128,160},{160,192},{192,224},{224... | collective-permute-start | bytes 319496 | tf_op jit(solution)/shard_map/ppermute | solution.py:266
  17.8 3.6 %collective-permute-start.9 = (bf16[256,128]{1,0:T(8,128)(2,1)}, bf16[256,128]{1,0:T(8,128)(2,1)S(1)}, u32[]{:S(2)}, u32[]{:S(2)}) collective-permute-start(bf16[256,128]{1,0:T(8,128)(2,1)} %get-tuple-element.19.q0), channel_id=1, source_target_pairs={{0,24},{8,0},{16,8},{24,16},{1,25},{9,1},{17,9},{25,17},{2,26},{10... | collective-permute-start | bytes 196616 | tf_op jit(solution)/shard_map/ppermute | solution.py:266
  19.7 25.4 %copy-start.16 = (bf16[256,128]{1,0:T(8,128)(2,1)}, bf16[256,128]{1,0:T(8,128)(2,1)S(1)}, u32[]{:S(2)}) copy-start(bf16[256,128]{1,0:T(8,128)(2,1)S(1)} %collective-permute-done.8.q1) | copy-start | bytes 196612
  19.7 7.1 %collective-permute-start.10 = (bf16[256,128]{1,0:T(8,128)(2,1)}, bf16[256,128]{1,0:T(8,128)(2,1)S(1)}, u32[]{:S(2)}, u32[]{:S(2)}) collective-permute-start(bf16[256,128]{1,0:T(8,128)(2,1)} %get-tuple-element.19.q0), channel_id=1, source_target_pairs={{0,16},{8,24},{16,0},{24,8},{1,17},{9,25},{17,1},{25,9},{2,18},{10... | collective-permute-start | bytes 196616 | tf_op jit(solution)/shard_map/ppermute | solution.py:266
  21.4 9.0 %collective-permute-start.1 = (bf16[416,128]{1,0:T(8,128)(2,1)}, bf16[416,128]{1,0:T(8,128)(2,1)S(1)}, u32[]{:S(2)}, u32[]{:S(2)}) collective-permute-start(bf16[416,128]{1,0:T(8,128)(2,1)} %get-tuple-element.18.k0), channel_id=1, source_target_pairs={{0,224},{32,0},{64,32},{96,64},{128,96},{160,128},{192,160},{224,1... | collective-permute-start | bytes 319496 | tf_op jit(solution)/shard_map/ppermute | solution.py:266
  26.9 7.4 %collective-permute-start.2 = (bf16[416,128]{1,0:T(8,128)(2,1)S(1)}, bf16[416,128]{1,0:T(8,128)(2,1)S(1)}, u32[]{:S(2)}, u32[]{:S(2)}) collective-permute-start(bf16[416,128]{1,0:T(8,128)(2,1)S(1)} %collective-permute-done.k1), channel_id=1, source_target_pairs={{0,32},{32,64},{64,96},{96,128},{128,160},{160,192},{192,224},{224... | collective-permute-start | bytes 319496 | tf_op jit(solution)/shard_map/ppermute | solution.py:266
  27.8 16.2 %collective-permute-start.11 = (bf16[4,256,128]{2,1,0:T(8,128)(2,1)S(1)}, bf16[4,256,128]{2,1,0:T(8,128)(2,1)S(1)}, u32[]{:S(2)}, u32[]{:S(2)}) collective-permute-start(bf16[4,256,128]{2,1,0:T(8,128)(2,1)S(1)} %pad_maximum_fusion.1), channel_id=1, source_target_pairs={{0,4},{4,0},{1,5},{5,1},{2,6},{6,2},{3,7},{7,3},{8,12},{12,8},{9,1... | collective-permute-start | bytes 786440 | tf_op jit(solution)/shard_map/ppermute | solution.py:266
  30.4 5.5 %collective-permute-start.3 = (bf16[416,128]{1,0:T(8,128)(2,1)S(1)}, bf16[416,128]{1,0:T(8,128)(2,1)S(1)}, u32[]{:S(2)}, u32[]{:S(2)}) collective-permute-start(bf16[416,128]{1,0:T(8,128)(2,1)S(1)} %collective-permute-done.1.k2), channel_id=1, source_target_pairs={{0,224},{32,0},{64,32},{96,64},{128,96},{160,128},{192,160},{224,1... | collective-permute-start | bytes 319496 | tf_op jit(solution)/shard_map/ppermute | solution.py:266
  34.2 4.8 %collective-permute-start.4 = (bf16[416,128]{1,0:T(8,128)(2,1)S(1)}, bf16[416,128]{1,0:T(8,128)(2,1)S(1)}, u32[]{:S(2)}, u32[]{:S(2)}) collective-permute-start(bf16[416,128]{1,0:T(8,128)(2,1)S(1)} %collective-permute-done.2.k3), channel_id=1, source_target_pairs={{0,32},{32,64},{64,96},{96,128},{128,160},{160,192},{192,224},{224... | collective-permute-start | bytes 319496 | tf_op jit(solution)/shard_map/ppermute | solution.py:266
  36.0 4.8 %collective-permute-start.5 = (bf16[416,128]{1,0:T(8,128)(2,1)S(1)}, bf16[416,128]{1,0:T(8,128)(2,1)S(1)}, u32[]{:S(2)}, u32[]{:S(2)}) collective-permute-start(bf16[416,128]{1,0:T(8,128)(2,1)S(1)} %collective-permute-done.3.k4), channel_id=1, source_target_pairs={{0,224},{32,0},{64,32},{96,64},{128,96},{160,128},{192,160},{224,1... | collective-permute-start | bytes 319496 | tf_op jit(solution)/shard_map/ppermute | solution.py:266
  39.0 6.1 %collective-permute-start.6 = (bf16[256,128]{1,0:T(8,128)(2,1)S(1)}, bf16[256,128]{1,0:T(8,128)(2,1)S(1)}, u32[]{:S(2)}, u32[]{:S(2)}) collective-permute-start(bf16[256,128]{1,0:T(8,128)(2,1)S(1)} %slice.32), channel_id=1, source_target_pairs={{0,32},{32,64},{64,96},{96,128},{128,160},{160,192},{192,224},{224... | collective-permute-start | bytes 196616 | tf_op jit(solution)/shard_map/ppermute | solution.py:266
  40.7 4.4 %collective-permute-start.7 = (bf16[160,128]{1,0:T(8,128)(2,1)S(1)}, bf16[160,128]{1,0:T(8,128)(2,1)S(1)}, u32[]{:S(2)}, u32[]{:S(2)}) collective-permute-start(bf16[160,128]{1,0:T(8,128)(2,1)S(1)} %slice.33), channel_id=1, source_target_pairs={{0,224},{32,0},{64,32},{96,64},{128,96},{160,128},{192,160},{224,1... | collective-permute-start | bytes 122888 | tf_op jit(solution)/shard_map/ppermute | solution.py:266
  52.2 19.8 %all-to-all-start = ((bf16[32,64,128]{2,1,0:T(8,128)(2,1)}), bf16[32,64,128]{2,1,0:T(8,128)(2,1)S(1)}, u32[]{:S(2)}, u32[]{:S(2)}) async-start(bf16[32,64,128]{2,1,0:T(8,128)(2,1)} %bitcast.25), calls=%async_computation | async-start | bytes 1048576 | tf_op jit(solution)/shard_map/all_to_all | solution.py:311
  61.8 17.1 %collective-permute-start.14 = (bf16[96,2048]{1,0:T(8,128)(2,1)}, bf16[96,2048]{1,0:T(8,128)(2,1)S(1)}, u32[]{:S(2)}, u32[]{:S(2)}) collective-permute-start(bf16[96,2048]{1,0:T(8,128)(2,1)} %slice.34), channel_id=1, source_target_pairs={{0,1},{1,2},{2,3},{3,0},{4,5},{5,6},{6,7},{7,4},{8,9},{9,10},{10,1... | collective-permute-start | bytes 1179656 | tf_op jit(solution)/shard_map/ppermute | solution.py:266
  63.2 15.8 %collective-permute-start.15 = (bf16[96,2048]{1,0:T(8,128)(2,1)S(1)}, bf16[96,2048]{1,0:T(8,128)(2,1)S(1)}, u32[]{:S(2)}, u32[]{:S(2)}) collective-permute-start(bf16[96,2048]{1,0:T(8,128)(2,1)S(1)} %slice.35), channel_id=1, source_target_pairs={{0,3},{1,0},{2,1},{3,2},{4,7},{5,4},{6,5},{7,6},{8,11},{9,8},{10,9... | collective-permute-start | bytes 1179656 | tf_op jit(solution)/shard_map/ppermute | solution.py:266
  113.9 8.8 %collective-permute-start.16 = (bf16[64,2048]{1,0:T(8,128)(2,1)S(1)}, bf16[64,2048]{1,0:T(8,128)(2,1)S(1)}, u32[]{:S(2)}, u32[]{:S(2)}) collective-permute-start(bf16[64,2048]{1,0:T(8,128)(2,1)S(1)} %slice.29.refs_0_), channel_id=1, source_target_pairs={{0,1},{1,2},{2,3},{3,0},{4,5},{5,6},{6,7},{7,4},{8,9},{9,10},{10,1... | collective-permute-start | bytes 786440 | tf_op jit(solution)/shard_map/ppermute | solution.py:266
  114.1 8.6 %collective-permute-start.19 = (bf16[64,2048]{1,0:T(8,128)(2,1)S(1)}, bf16[64,2048]{1,0:T(8,128)(2,1)S(1)}, u32[]{:S(2)}, u32[]{:S(2)}) collective-permute-start(bf16[64,2048]{1,0:T(8,128)(2,1)S(1)} %slice.31.refs_1_), channel_id=1, source_target_pairs={{0,3},{1,0},{2,1},{3,2},{4,7},{5,4},{6,5},{7,6},{8,11},{9,8},{10,9... | collective-permute-start | bytes 786440 | tf_op jit(solution)/shard_map/ppermute | solution.py:266
  122.6 7.8 %collective-permute-start.20 = (bf16[64,2048]{1,0:T(8,128)(2,1)S(1)}, bf16[64,2048]{1,0:T(8,128)(2,1)S(1)}, u32[]{:S(2)}, u32[]{:S(2)}) collective-permute-start(bf16[64,2048]{1,0:T(8,128)(2,1)S(1)} %collective-permute-done.16.refs_0_), channel_id=1, source_target_pairs={{0,1},{1,2},{2,3},{3,0},{4,5},{5,6},{6,7},{7,4},{8,9},{9,10},{10,1... | collective-permute-start | bytes 786440 | tf_op jit(solution)/shard_map/ppermute | solution.py:266
  122.7 7.8 %collective-permute-start.21 = (bf16[64,2048]{1,0:T(8,128)(2,1)S(1)}, bf16[64,2048]{1,0:T(8,128)(2,1)S(1)}, u32[]{:S(2)}, u32[]{:S(2)}) collective-permute-start(bf16[64,2048]{1,0:T(8,128)(2,1)S(1)} %collective-permute-done.19.refs_3_), channel_id=1, source_target_pairs={{0,3},{1,0},{2,1},{3,2},{4,7},{5,4},{6,5},{7,6},{8,11},{9,8},{10,9... | collective-permute-start | bytes 786440 | tf_op jit(solution)/shard_map/ppermute | solution.py:266
  125.3 15.9 %collective-permute-start.17 = (bf16[64,2048]{1,0:T(8,128)(2,1)S(1)}, bf16[64,2048]{1,0:T(8,128)(2,1)S(1)}, u32[]{:S(2)}, u32[]{:S(2)}) collective-permute-start(bf16[64,2048]{1,0:T(8,128)(2,1)S(1)} %slice.31.refs_1_), channel_id=1, source_target_pairs={{0,1},{1,2},{2,3},{3,0},{4,5},{5,6},{6,7},{7,4},{8,9},{9,10},{10,1... | collective-permute-start | bytes 786440 | tf_op jit(solution)/shard_map/ppermute | solution.py:266
  125.3 15.9 %collective-permute-start.18 = (bf16[64,2048]{1,0:T(8,128)(2,1)S(1)}, bf16[64,2048]{1,0:T(8,128)(2,1)S(1)}, u32[]{:S(2)}, u32[]{:S(2)}) collective-permute-start(bf16[64,2048]{1,0:T(8,128)(2,1)S(1)} %slice.29.refs_0_), channel_id=1, source_target_pairs={{0,3},{1,0},{2,1},{3,2},{4,7},{5,4},{6,5},{7,6},{8,11},{9,8},{10,9... | collective-permute-start | bytes 786440 | tf_op jit(solution)/shard_map/ppermute | solution.py:266
  136.2 17.8 %collective-permute-start.22 = (bf16[64,2048]{1,0:T(8,128)(2,1)}, bf16[64,2048]{1,0:T(8,128)(2,1)S(1)}, u32[]{:S(2)}, u32[]{:S(2)}) collective-permute-start(bf16[64,2048]{1,0:T(8,128)(2,1)} %get-tuple-element.25), channel_id=1, source_target_pairs={{0,1},{1,2},{2,3},{3,0},{4,5},{5,6},{6,7},{7,4},{8,9},{9,10},{10,1... | collective-permute-start | bytes 786440 | tf_op jit(solution)/shard_map/ppermute | solution.py:266
  148.6 14.6 %collective-permute-start.24 = (bf16[64,2048]{1,0:T(8,128)(2,1)}, bf16[64,2048]{1,0:T(8,128)(2,1)S(1)}, u32[]{:S(2)}, u32[]{:S(2)}) collective-permute-start(bf16[64,2048]{1,0:T(8,128)(2,1)} %get-tuple-element.26), channel_id=1, source_target_pairs={{0,3},{1,0},{2,1},{3,2},{4,7},{5,4},{6,5},{7,6},{8,11},{9,8},{10,9... | collective-permute-start | bytes 786440 | tf_op jit(solution)/shard_map/ppermute | solution.py:266
  151.3 12.2 %collective-permute-start.25 = (bf16[64,2048]{1,0:T(8,128)(2,1)}, bf16[64,2048]{1,0:T(8,128)(2,1)S(1)}, u32[]{:S(2)}, u32[]{:S(2)}) collective-permute-start(bf16[64,2048]{1,0:T(8,128)(2,1)} %get-tuple-element.28), channel_id=1, source_target_pairs={{0,1},{1,2},{2,3},{3,0},{4,5},{5,6},{6,7},{7,4},{8,9},{9,10},{10,1... | collective-permute-start | bytes 786440 | tf_op jit(solution)/shard_map/ppermute | solution.py:266
  151.3 7.4 %collective-permute-start.26 = (bf16[64,2048]{1,0:T(8,128)(2,1)S(1)}, bf16[64,2048]{1,0:T(8,128)(2,1)S(1)}, u32[]{:S(2)}, u32[]{:S(2)}) collective-permute-start(bf16[64,2048]{1,0:T(8,128)(2,1)S(1)} %copy-done.32), channel_id=1, source_target_pairs={{0,3},{1,0},{2,1},{3,2},{4,7},{5,4},{6,5},{7,6},{8,11},{9,8},{10,9... | collective-permute-start | bytes 786440 | tf_op jit(solution)/shard_map/ppermute | solution.py:266
  155.0 8.3 %collective-permute-start.23 = (bf16[64,2048]{1,0:T(8,128)(2,1)S(1)}, bf16[64,2048]{1,0:T(8,128)(2,1)S(1)}, u32[]{:S(2)}, u32[]{:S(2)}) collective-permute-start(bf16[64,2048]{1,0:T(8,128)(2,1)S(1)} %add_convert_fusion.3), channel_id=1, source_target_pairs={{0,1},{1,2},{2,3},{3,0},{4,5},{5,6},{6,7},{7,4},{8,9},{9,10},{10,1... | collective-permute-start | bytes 786440 | tf_op jit(solution)/shard_map/ppermute | solution.py:266
  159.7 6.8 %collective-permute-start.27 = (bf16[64,2048]{1,0:T(8,128)(2,1)S(1)}, bf16[64,2048]{1,0:T(8,128)(2,1)S(1)}, u32[]{:S(2)}, u32[]{:S(2)}) collective-permute-start(bf16[64,2048]{1,0:T(8,128)(2,1)S(1)} %add_convert_fusion.1), channel_id=1, source_target_pairs={{0,3},{1,0},{2,1},{3,2},{4,7},{5,4},{6,5},{7,6},{8,11},{9,8},{10,9... | collective-permute-start | bytes 786440 | tf_op jit(solution)/shard_map/ppermute | solution.py:266
  167.8 28.9 %all-to-all-start.2 = ((bf16[64,2,2048]{2,1,0:T(2,128)(2,1)}), bf16[64,2,2048]{2,1,0:T(2,128)(2,1)S(1)}, u32[]{:S(2)}, u32[]{:S(2)}) async-start(bf16[64,2,2048]{2,1,0:T(2,128)(2,1)} %convert_element_type.53), calls=%async_computation.2 | async-start | bytes 1048576 | tf_op jit(solution)/shard_map/all_to_all | solution.py:361
  (31 other events, 333.4 us)

commit v2 on v1

--- a/solution.py
+++ b/solution.py
@@ -42,7 +42,7 @@
         c, s = np.cos(angles), np.sin(angles)
         return np.concatenate([c, c, s, s], axis=1).astype(np.float32)
 
-    return table(np.arange(64) * ROWS), table(np.arange(ROWS))
+    return table(np.arange(64) * ROWS), np.ascontiguousarray(table(np.arange(ROWS)).T)
 
 
 def vmem(n):
@@ -53,72 +53,76 @@
     return pl.BlockSpec(memory_space=pltpu.SMEM)
 
 
+def column(row):
+    n = row.shape[1]
+    same = lax.broadcasted_iota(jnp.int32, (n, n), 0) == lax.broadcasted_iota(
+        jnp.int32, (n, n), 1
+    )
+    return jnp.sum(jnp.where(same, row, 0.0), axis=1, keepdims=True)
+
+
 def pre_kernel(
     place_ref, lat_ref, gain_ref, rk_ref, qs_ref, ql_ref, ks_w, vs_w, kl_w, vl_w,
-    base_ref, row_ref, kv_ref, q_ref,
+    base_ref, row_ref, lo_ref, so_ref, kv_ref, q_ref, wo_ref,
 ):
     block = (place_ref[0] * NX + place_ref[1]) * NC + place_ref[2]
-    base = base_ref[pl.ds(block, 1), :]
-    row = row_ref[...]
-    cb, sb = base[:, :ROPE], base[:, ROPE:]
-    cr, sr = row[:, :ROPE], row[:, ROPE:]
+    base = column(base_ref[pl.ds(block, 1), :])
+    cb, sb = base[:ROPE], base[ROPE:]
+    cr, sr = row_ref[:ROPE], row_ref[ROPE:]
     cos = cr * cb - sr * sb
     sin = sr * cb + cr * sb
-    lane = lax.broadcasted_iota(jnp.int32, (ROWS, ROPE), 1)
-    sin = jnp.where(lane < ROPE // 2, -sin, sin)
+    at = lax.broadcasted_iota(jnp.int32, (ROPE, ROWS), 0)
+    sin = jnp.where(at < ROPE // 2, -sin, sin)
 
     def turned(v):
         v = v.astype(f32)
-        swapped = jnp.concatenate([v[:, ROPE // 2 :], v[:, : ROPE // 2]], axis=1)
-        return (v * cos + swapped * sin).astype(bf16)
+        swapped = jnp.concatenate([v[ROPE // 2 :], v[: ROPE // 2]], axis=0)
+        return v * cos + swapped * sin
 
     lat = lat_ref[...].astype(f32)
     scale = lax.rsqrt(jnp.mean(lat * lat, axis=1, keepdims=True) + EPS)
     normed = (lat * scale * gain_ref[...]).astype(bf16)
-
-    def proj(w_ref):
-        return jnp.dot(normed, w_ref[...], preferred_element_type=f32).astype(bf16)
-
-    kv_ref[0:128, :] = proj(kl_w)
-    kv_ref[128:256, :] = proj(vl_w)
-    kv_ref[256:384, :] = jnp.concatenate([proj(ks_w), proj(vs_w)], axis=1)
-    rot = turned(rk_ref[...])
-    kv_ref[384:416, :] = jnp.concatenate([rot[32 * i : 32 * i + 32] for i in range(4)], axis=1)
-    ql = ql_ref[...]
-    qs = qs_ref[...]
-    q_ref[0:128, :] = ql[:, :NOPE_L]
-    q_ref[128:256, :] = jnp.concatenate(
-        [qs[:, :NOPE_S], turned(ql[:, NOPE_L:]), turned(qs[:, NOPE_S:])], axis=1
-    )
-
-
-def attn_kernel(
-    place_ref, k0, k1, k2, k3, k4, k5, k6, k7a, k7b, q0, q1, q2, q3, r_ref, out_ref,
-    kl, ks, vl, vs,
-):
+    across = (((1,), (1,)), ((), ()))
+
+    kv_ref[0, 0:128, :] = jnp.dot(normed, kl_w[...], preferred_element_type=f32).T.astype(bf16)
+    kv_ref[0, 128:256, :] = jnp.dot(normed, vl_w[...], preferred_element_type=f32).astype(bf16)
+    kv_ref[0, 256:320, :] = lax.dot_general(
+        ks_w[...], normed, across, preferred_element_type=f32
+    ).astype(bf16)
+    kv_ref[0, 320:352, :] = turned(rk_ref[...]).astype(bf16)
+    kv_ref[0, 352:416, :] = lax.dot_general(
+        vs_w[...], normed, across, preferred_element_type=f32
+    ).astype(bf16)
+    for j in range(1, NZ):
+        kv_ref[j] = kv_ref[0]
+    q_ref[0:128, :] = ql_ref[0:NOPE_L, :].astype(f32).T.astype(bf16)
+    mixed = jnp.concatenate(
+        [qs_ref[0:NOPE_S, :].astype(f32), turned(ql_ref[NOPE_L:, :]), turned(qs_ref[NOPE_S:, :])],
+        axis=0,
+    )
+    q_ref[128:256, :] = mixed.T.astype(bf16)
+    wo_ref[0:128, :] = lo_ref[...]
+    wo_ref[128:192, :] = so_ref[...]
+
+
+def attn_kernel(place_ref, kv_ref, q0, q1, q2, q3, r_ref, out_ref, kl, ks, vl, vs):
     z, x, c = place_ref[0], place_ref[1], place_ref[2]
-    ones = jnp.ones((ROWS, 128), bf16)
-    zero32 = jnp.zeros((ROWS, 32), bf16)
-    zero64 = jnp.zeros((ROWS, 64), bf16)
-    blocks = [(k, k, 256) for k in (k0, k1, k2, k3, k4, k5, k6)] + [(k7a, k7b, 0)]
-    for j, (front, back, at) in enumerate(blocks):
+    kl[128:192, :] = jnp.zeros((64, 1024), bf16)
+    kl[224:256, :] = jnp.zeros((32, 1024), bf16)
+    ks[64:96, :] = jnp.zeros((32, 1024), bf16)
+    vl[:, 128:256] = jnp.ones((1024, 128), bf16)
+    vs[0:64, :] = jnp.ones((64, 1024), bf16)
+    for j in range(NZ):
         lo, hi = j * ROWS, (j + 1) * ROWS
-        small = back[at : at + 128, :]
-        packed = back[at + 128 : at + 160, :]
-        rot = jnp.concatenate([packed[:, 32 * i : 32 * i + 32] for i in range(4)], axis=0)
-        kl[lo:hi, 0:128] = front[0:128, :]
-        kl[lo:hi, 128:256] = jnp.concatenate([zero64, rot, zero32], axis=1)
-        ks[lo:hi, :] = jnp.concatenate([small[:, :64], zero32, rot], axis=1)
-        vl[lo:hi, 0:128] = front[128:256, :]
-        vl[lo:hi, 128:256] = ones
-        vs[lo:hi, 0:128] = small
-        vs[lo:hi, 128:256] = ones
-    shifts = (0, 1, 7, 2, 6, 3, 5, 4)
-    lane = lax.broadcasted_iota(jnp.int32, (1, 128), 1)
-    own = (x * NC + c) * ROWS
-    kpos = jnp.concatenate(
-        [lax.rem(z + (NZ - s), NZ) * (NXC * ROWS) + own + lane for s in shifts], axis=1
-    )
+        rot = kv_ref[j, 320:352, :]
+        kl[0:128, lo:hi] = kv_ref[j, 0:128, :]
+        kl[192:224, lo:hi] = rot
+        ks[0:64, lo:hi] = kv_ref[j, 256:320, :]
+        ks[96:128, lo:hi] = rot
+        vl[lo:hi, 0:128] = kv_ref[j, 128:256, :]
+        vs[64:128, lo:hi] = kv_ref[j, 352:416, :]
+    key = lax.broadcasted_iota(jnp.int32, (1, NZ * ROWS), 1)
+    kpos = (key // ROWS) * (NXC * ROWS) + (x * NC + c) * ROWS + lax.rem(key, ROWS)
     row = lax.broadcasted_iota(jnp.int32, (2 * ROWS, 1), 0)
     lanes = lax.broadcasted_iota(jnp.int32, (2 * ROWS, 128), 1)
     for d, (shift, mine) in enumerate(((0, q0), (1, q1), (3, q2), (2, q3))):
@@ -137,19 +141,19 @@
         )
         allowed = kpos <= qpos
 
-        def attend(query, keys, values, scale):
-            s = lax.dot_general(
-                query, keys[...], (((1,), (1,)), ((), ())), preferred_element_type=f32
-            )
+        def attend(query, keys, values, contract, scale, at):
+            s = jnp.dot(query, keys[...], preferred_element_type=f32)
             s = jnp.where(allowed, s, MASKED)
             top = jnp.max(s, axis=1, keepdims=True).astype(bf16).astype(f32)
             w = jnp.exp2((s - top) * scale).astype(bf16)
-            o = jnp.dot(w, values[...], preferred_element_type=f32)
-            total = o[:, 128:129]
+            o = lax.dot_general(
+                w, values[...], (((1,), (contract,)), ((), ())), preferred_element_type=f32
+            )
+            total = o[:, at : at + 1]
             return o[:, :128] / total, top, total
 
-        o_l, m_l, t_l = attend(q, kl, vl, SCALE_L)
-        o_s, m_s, t_s = attend(q[:, 128:256], ks, vs, SCALE_S)
+        o_l, m_l, t_l = attend(q, kl, vl, 0, SCALE_L, 128)
+        o_s, m_s, t_s = attend(q[:, 128:256], ks, vs, 1, SCALE_S, 0)
         h_l = t_l.astype(bf16).astype(f32)
         h_s = t_s.astype(bf16).astype(f32)
         for i, v in enumerate((m_l, h_l, t_l - h_l, m_s, h_s, t_s - h_s)):
@@ -201,7 +205,8 @@
     normed = (wide * scale * gain_ref[...]).astype(bf16)
 
     lane = lax.broadcasted_iota(jnp.int32, (TOK, SLOTS), 1)
-    r = [routing_ref[:, k : k + 1] for k in range(2)]
+    named_by = routing_ref[...].astype(f32)
+    r = [column(named_by[k : k + 1, :]).astype(jnp.int32) for k in range(2)]
     hit = [lane == rk for rk in r]
     named = jnp.where(hit[0] | hit[1], 1.0, 0.0)
     tri = jnp.where(
@@ -220,6 +225,17 @@
     disp_ref[...] = lax.dot_general(
         send.astype(bf16), normed, (((0,), (0,)), ((), ())), preferred_element_type=f32
     ).astype(bf16)
+
+
+def load_kernel(a, b, c, out_a, out_b, out_c, sems):
+    copies = [
+        pltpu.make_async_copy(src, dst, sems.at[i])
+        for i, (src, dst) in enumerate(((a, out_a), (b, out_b), (c, out_c)))
+    ]
+    for copy in copies:
+        copy.start()
+    for copy in copies:
+        copy.wait()
 
 
 def ffn_kernel(*refs):
@@ -241,12 +257,15 @@
 def end_kernel(mid_ref, pick_ref, ret_ref, weight_ref, out_ref):
     total = mid_ref[...].astype(f32)
     ret = ret_ref[...]
-    mixed = weight_ref[:, 0:1] * jnp.dot(pick_ref[0], ret, preferred_element_type=f32)
-    mixed = mixed + weight_ref[:, 1:2] * jnp.dot(pick_ref[1], ret, preferred_element_type=f32)
+    weight = weight_ref[...]
+    mixed = column(weight[0:1, :]) * jnp.dot(pick_ref[0], ret, preferred_element_type=f32)
+    mixed = mixed + column(weight[1:2, :]) * jnp.dot(
+        pick_ref[1], ret, preferred_element_type=f32
+    )
     out_ref[...] = (total + mixed).astype(bf16)
 
 
-def call(kernel, in_specs, shapes, scratch=(), flops=0):
+def call(kernel, in_specs, shapes, scratch=(), flops=0, mib=16):
     many = len(shapes) > 1
     outs = [jax.ShapeDtypeStruct(s, d) for s, d in shapes]
     return pl.pallas_call(
@@ -255,7 +274,7 @@
         out_specs=vmem(len(outs)) if many else vmem(1)[0],
         out_shape=outs if many else outs[0],
         scratch_shapes=list(scratch),
-        compiler_params=pltpu.CompilerParams(vmem_limit_bytes=56 * 2**20),
+        compiler_params=pltpu.CompilerParams(vmem_limit_bytes=mib * 2**20),
         cost_estimate=pl.CostEstimate(flops=flops, transcendentals=0, bytes_accessed=0)
         if flops
         else None,
@@ -266,48 +285,52 @@
     return lax.ppermute(a, axis, [(i, (i + by) % size) for i in range(size)])
 
 
-def on_device(
+def layer(
     residual, query_small, query_large, latent, rotary_key, latent_gain,
     small_keys, small_values, large_keys, large_values, small_output, large_output,
     ffn_gain, gate_weights, up_weights, down_weights, routing, route_weight,
 ):
     place = jnp.stack([lax.axis_index(a) for a in ("z", "x", "c", "y")]).astype(jnp.int32)
     base, row = rope_parts()
-    kv, q = call(
-        pre_kernel, [smem()] + vmem(11), [((416, 128), bf16), ((256, 128), bf16)]
+    kv, q, wo = call(
+        pre_kernel,
+        [smem()] + vmem(13),
+        [((NZ, 416, 128), bf16), ((256, 128), bf16), ((192, D), bf16)],
+        flops=10**9,
+        mib=63,
     )(
-        place, latent, latent_gain[None, :], rotary_key, query_small, query_large,
-        small_keys, small_values, large_keys, large_values, base, row,
-    )
-
-    plus = minus = kv
-    blocks = [kv]
-    for _ in range(3):
-        plus = shifted(plus, "z", NZ, 1)
-        minus = shifted(minus, "z", NZ, -1)
-        blocks += [plus, minus]
-    blocks += [shifted(plus[:256], "z", NZ, 1), shifted(minus[256:], "z", NZ, -1)]
-
-    qx = [q] + [shifted(q, "x", NX, s) for s in (1, -1, 2)]
+        place, latent, latent_gain[None, :], rotary_key.T, query_small.T, query_large.T,
+        small_keys.T, small_values.T, large_keys, large_values, base, row,
+        large_output, small_output,
+    )
+
+    kvs = lax.all_to_all(kv, "z", 0, 0, tiled=True)
+
+    qx = [q]
+    for by in (1, -1, 2):
+        qx.append(shifted(q, "x", NX, by))
     qc = shifted(jnp.stack(qx), "c", NC, 1)
 
-    wo = jnp.concatenate([large_output, small_output], axis=0)
     wo_p = shifted(wo, "y", NY, 1)
     wo_m = shifted(wo, "y", NY, -1)
+    kvs, wo_p, wo_m = lax.optimization_barrier((kvs, wo_p, wo_m))
     wo_a = shifted(wo_p[:96], "y", NY, 1)
     wo_b = shifted(wo_m[96:], "y", NY, -1)
 
-    parts = call(
+    attend = call(
         attn_kernel,
-        [smem()] + vmem(14),
+        [smem()] + vmem(6),
         [((NXC, NY, 2 * TOK, 128), bf16)],
         scratch=[
+            pltpu.VMEM((256, 1024), bf16),
+            pltpu.VMEM((128, 1024), bf16),
             pltpu.VMEM((1024, 256), bf16),
-            pltpu.VMEM((1024, 128), bf16),
-            pltpu.VMEM((1024, 256), bf16),
-            pltpu.VMEM((1024, 256), bf16),
+            pltpu.VMEM((128, 1024), bf16),
         ],
-    )(place, *blocks, *qx, qc)
+        flops=3 * 10**9,
+        mib=24,
+    )
+    parts = attend(place, kvs, *qx, qc)
     parts = lax.all_to_all(
         parts.reshape(NXC * NY * 2 * TOK, 128), ("x", "c", "y"), 0, 0, tiled=True
     ).reshape(NXC, NY, 2 * TOK, 128)
@@ -316,7 +339,9 @@
         mid_kernel,
         [smem()] + vmem(9),
         [((SLOTS, D), bf16), ((TOK, D), bf16), ((2, TOK, SLOTS), bf16)],
-    )(place, parts, wo, wo_p, wo_m, wo_a, wo_b, residual, ffn_gain[None, :], routing)
+        flops=2 * 10**9,
+        mib=63,
+    )(place, parts, wo, wo_p, wo_m, wo_a, wo_b, residual, ffn_gain[None, :], routing.T)
 
     sp = ("z", "x", "c")
     mine = lax.all_to_all(disp.reshape(EXPERTS, CAP, D), sp, 0, 0, tiled=True)
@@ -324,13 +349,22 @@
 
     half = SLOTS // 2
     x_a, x_b = mine[:half], mine[half:]
-    weights = (gate_weights[0], up_weights[0], down_weights[0])
+    weights = call(
+        load_kernel,
+        [pl.BlockSpec(memory_space=pltpu.HBM) for _ in range(3)],
+        [((D, FF_LOCAL), bf16), ((D, FF_LOCAL), bf16), ((FF_LOCAL, D), bf16)],
+        scratch=[pltpu.SemaphoreType.DMA((3,))],
+        flops=10**9,
+        mib=8,
+    )(gate_weights[0], up_weights[0], down_weights[0])
 
     def ffn(*pieces):
         return call(
             ffn_kernel,
             vmem(len(pieces) + 3),
             [(p.shape, bf16) for p in pieces],
+            flops=3 * 10**9,
+            mib=28,
         )(*pieces, *weights)
 
     p_a = shifted(x_a, "y", NY, 1)
@@ -339,8 +373,7 @@
     m_a = shifted(x_a, "y", NY, -1)
     o_a = shifted(p_a, "y", NY, 1)
     o_b = shifted(m_b, "y", NY, -1)
-    r0_a, r0_b = ffn(x_a, x_b)
-    r1_a, r1_b, r3_a, r3_b = ffn(p_a, p_b, m_a, m_b)
+    r0_a, r0_b, r1_a, r1_b, r3_a, r3_b = ffn(x_a, x_b, p_a, p_b, m_a, m_b)
     r2_a, r2_b = ffn(o_a, o_b)
 
     from_m_b = shifted(r3_b, "y", NY, 1)
@@ -360,7 +393,7 @@
     ).astype(bf16)
     ret = lax.all_to_all(done.reshape(EXPERTS, CAP, D), sp, 0, 0, tiled=True)
     return call(end_kernel, vmem(4), [((TOK, D), bf16)])(
-        middle, pick, ret.reshape(SLOTS, D), route_weight
+        middle, pick, ret.reshape(SLOTS, D), route_weight.T
     )
 
 
@@ -369,7 +402,7 @@
     sp = ("z", "x", "c")
     every = ("z", "x", "c", "y")
     return jax.shard_map(
-        on_device,
+        layer,
         mesh=fine,
         in_specs=(
             P(every, None),

time: 200 us -> 172 us (0.86)
  blocking collectives: 27.4 us -> 50.3 us
  starting transfers between devices: 67.7 us -> 44.9 us
  Pallas kernels: 31 us -> 17.6 us
  local copies, waits for them, and re-layouts: 18.8 us -> 8.82 us
  waiting for transfers between devices: 50.8 us -> 47.4 us
    all_to_all x1 -> x2, blocking collectives: 27.4 us -> 50.3 us  [the longest x1 26.7 us: layer(): ret = lax.all_to_all(done.reshape(EXPERTS, CAP, D), sp, 0, 0, tiled=True)]
    ppermute x28 -> x20, starting transfers between devices: 47.8 us -> 28.2 us  [shifted(): return lax.ppermute(a, axis, [(i, (i + by) % size) for i in range(size)])]
    all_to_all x2, waiting for transfers between devices: 23.8 us -> 5.27 us  [the longest x1 5.27 us: layer(): kvs = lax.all_to_all(kv, 'z', 0, 0, tiled=True)]
    ppermute x28 -> x20, waiting for transfers between devices: 27 us -> 42.1 us  [shifted(): return lax.ppermute(a, axis, [(i, (i + by) % size) for i in range(size)])]
    pallas_call x7, Pallas kernels: 31 us -> 17.6 us  [the longest x1 4.73 us: layer(): parts = attend(place, kvs, *qx, qc)]
    unnamed x74 -> x22, local copies, waits for them, and re-layouts: 12.9 us -> 4.14 us
    all_to_all x2, starting transfers between devices: 19.8 us -> 16.7 us  [the longest x1 9.14 us: layer(): kvs = lax.all_to_all(kv, 'z', 0, 0, tiled=True)]
  transfers between devices with their start and end apart: 30 -> 22, of which waited for: 13 -> 11; matrix products, arithmetic and copies ran while one was open for 6% -> 2% of each run, Pallas kernels for 12% -> 2%
where the time goes in v2:
time: 172 us; the launch traced here: 171 us
  blocking collectives  50.3 us (29%)
  waiting for transfers between devices  47.4 us (28%)
  starting transfers between devices  44.9 us (26%)
  Pallas kernels  17.6 us (10%)
  local copies, waits for them, and re-layouts  8.82 us (5%)
  other arithmetic  1.88 us (1%)
    ppermute x20, waiting for transfers between devices, shifted(): return lax.ppermute(a, axis, [(i, (i + by) % size) for i in range(size)])  42.1 us
    ppermute x20, starting transfers between devices, shifted(): return lax.ppermute(a, axis, [(i, (i + by) % size) for i in range(size)])  28.2 us
    all_to_all x1, blocking collectives, layer(): ret = lax.all_to_all(done.reshape(EXPERTS, CAP, D), sp, 0, 0, tiled=True)  26.7 us
    all_to_all x1, blocking collectives, layer(): mine = lax.all_to_all(disp.reshape(EXPERTS, CAP, D), sp, 0, 0, tiled=True)  23.6 us
    all_to_all x1, starting transfers between devices, layer(): kvs = lax.all_to_all(kv, 'z', 0, 0, tiled=True)  9.14 us
    all_to_all x1, starting transfers between devices, layer(): lax.all_to_all(parts.reshape(NXC * NY * 2 * TOK, 128), ('x', 'c', 'y'), 0...  7.57 us
    all_to_all x1, waiting for transfers between devices, layer(): kvs = lax.all_to_all(kv, 'z', 0, 0, tiled=True)  5.27 us
    pallas_call x1, Pallas kernels, layer(): parts = attend(place, kvs, *qx, qc)  4.73 us
  transfers between devices with their start and end apart: 22, of which 11 were waited for; matrix products, arithmetic and copies ran while one was open for 2% of the time, Pallas kernels for 2%

profile of v2, /device:TPU:1, one launch (start us, length us, event | category | flops | bytes accessed | tf_op | source)
XLA Modules:
  0.0 171.1 jit_solution(846439990780919335)
XLA Ops:
  0.6 3.0 %shard_map.190 = (bf16[8,416,128]{2,1,0:T(8,128)(2,1)}, bf16[256,128]{1,0:T(8,128)(2,1)}, bf16[192,2048]{1,0:T(8,128)(2,1)}) custom-call(s32[4]{0:T(128)} %pad_add_fusion.place_ref, bf16[128,512]{1,0:T(8,128)(2,1)} %lat_ref.1, f32[1,512]{1,0:T(1,128)} %bitcast.37, bf16[32,128]{1,0:T(8,128)(2,1)} %bitcast.35, bf16[96,128]{1,0:T(8,128)(2,1)} %bitcast.34, ...), custom_call_target="tpu_custom_call" | custom-call | flops 1000000000 | tf_op jit(solution)/shard_map/pallas_call | solution.py:295
  3.7 9.1 %all-to-all-start = ((bf16[8,416,128]{2,1,0:T(8,128)(2,1)}), bf16[8,416,128]{2,1,0:T(8,128)(2,1)S(1)}, u32[]{:S(2)}, u32[]{:S(2)}) async-start(bf16[8,416,128]{2,1,0:T(8,128)(2,1)} %get-tuple-element.25), calls=%async_computation | async-start | bytes 1703936 | tf_op jit(solution)/shard_map/all_to_all | solution.py:307
  12.8 1.3 collective-permute-start
  14.1 1.5 collective-permute-start.1
  16.8 1.5 collective-permute-start.3
  18.3 1.5 collective-permute-start.4
  20.6 3.4 %collective-permute-done.4.q3 = bf16[256,128]{1,0:T(8,128)(2,1)S(1)} collective-permute-done((bf16[256,128]{1,0:T(8,128)(2,1)}, bf16[256,128]{1,0:T(8,128)(2,1)S(1)}, u32[]{:S(2)}, u32[]{:S(2)}) %collective-permute-start.4) | collective-permute-done | bytes 65568 | tf_op jit(solution)/shard_map/ppermute | solution.py:285
  24.9 2.3 %collective-permute-start.5 = (bf16[4,256,128]{2,1,0:T(8,128)(2,1)S(1)}, bf16[4,256,128]{2,1,0:T(8,128)(2,1)S(1)}, u32[]{:S(2)}, u32[]{:S(2)}) collective-permute-start(bf16[4,256,128]{2,1,0:T(8,128)(2,1)S(1)} %pad_maximum_fusion.1), channel_id=1, source_target_pairs={{0,4},{4,0},{1,5},{5,1},{2,6},{6,2},{3,7},{7,3},{8,12},{12,8},{9,1... | collective-permute-start | bytes 786440 | tf_op jit(solution)/shard_map/ppermute | solution.py:285
  27.2 5.3 %collective-permute-done.w1 = bf16[192,2048]{1,0:T(8,128)(2,1)S(1)} collective-permute-done((bf16[192,2048]{1,0:T(8,128)(2,1)}, bf16[192,2048]{1,0:T(8,128)(2,1)S(1)}, u32[]{:S(2)}, u32[]{:S(2)}) %collective-permute-start) | collective-permute-done | bytes 786464 | tf_op jit(solution)/shard_map/ppermute | solution.py:285
  32.5 5.3 %all-to-all-done.kv_ref = bf16[8,416,128]{2,1,0:T(8,128)(2,1)S(1)} async-done(((bf16[8,416,128]{2,1,0:T(8,128)(2,1)}), bf16[8,416,128]{2,1,0:T(8,128)(2,1)S(1)}, u32[]{:S(2)}, u32[]{:S(2)}) %all-to-all-start) | async-done | bytes 852000 | tf_op jit(solution)/shard_map/all_to_all | solution.py:307
  37.8 4.7 %shard_map.191 = bf16[8,4,64,128]{3,2,1,0:T(8,128)(2,1)} custom-call(s32[4]{0:T(128)S(1)} %copy-done.7, bf16[8,416,128]{2,1,0:T(8,128)(2,1)S(1)} %all-to-all-done.kv_ref, bf16[256,128]{1,0:T(8,128)(2,1)S(1)} %copy-done.4, bf16[256,128]{1,0:T(8,128)(2,1)S(1)} %collective-permute-done.2.q1, bf16[256,128]{1,0:T(8,128)(2,1)S(1)} %collective-permute-done.3.q2, ...), custom_call_target="tpu_custom_call" | custom-call | flops 3000000000 | tf_op jit(solution)/shard_map/pallas_call | solution.py:333
  42.5 7.6 %all-to-all-start.1 = ((bf16[32,64,128]{2,1,0:T(8,128)(2,1)}), bf16[32,64,128]{2,1,0:T(8,128)(2,1)S(1)}, u32[]{:S(2)}, u32[]{:S(2)}) async-start(bf16[32,64,128]{2,1,0:T(8,128)(2,1)} %bitcast.14), calls=%async_computation.1 | async-start | bytes 1048576 | tf_op jit(solution)/shard_map/all_to_all | solution.py:334
  51.1 1.4 collective-permute-start.6
  53.6 1.6 collective-permute-start.7
  55.2 12.9 %collective-permute-done.6.w2a = bf16[96,2048]{1,0:T(8,128)(2,1)S(1)} collective-permute-done((bf16[96,2048]{1,0:T(8,128)(2,1)S(1)}, bf16[96,2048]{1,0:T(8,128)(2,1)S(1)}, u32[]{:S(2)}, u32[]{:S(2)}) %collective-permute-start.6) | collective-permute-done | bytes 393248 | tf_op jit(solution)/shard_map/ppermute | solution.py:285
  69.0 4.7 %shard_map.192 = (bf16[128,2048]{1,0:T(8,128)(2,1)}, bf16[32,2048]{1,0:T(8,128)(2,1)}, bf16[2,32,128]{2,1,0:T(8,128)(2,1)}) custom-call(s32[4]{0:T(128)} %pad_add_fusion.place_ref, bf16[8,4,64,128]{3,2,1,0:T(8,128)(2,1)} %bitcast.30, bf16[192,2048]{1,0:T(8,128)(2,1)} %get-tuple-element.26.w0, bf16[192,2048]{1,0:T(8,128)(2,1)} %copy-done.9, ...), custom_call_target="tpu_custom_call" | custom-call | flops 2000000000 | tf_op jit(solution)/shard_map/pallas_call | solution.py:338
  73.8 1.5 reshape.21
  75.3 23.6 %all_to_all.24 = bf16[64,2,2048]{2,1,0:T(2,128)(2,1)S(1)} all-to-all(bf16[64,2,2048]{2,1,0:T(2,128)(2,1)S(1)} %reshape.21), channel_id=1, replica_groups=mesh['z'=8,'x'=4,'c'=2,'y'=4] {'z','x','c'}, dimensions={0} | all-to-all | bytes 1048576 | tf_op jit(solution)/shard_map/all_to_all | solution.py:347
  99.6 2.7 %collective-permute-start.11 = (bf16[64,2048]{1,0:T(8,128)(2,1)S(1)}, bf16[64,2048]{1,0:T(8,128)(2,1)S(1)}, u32[]{:S(2)}, u32[]{:S(2)}) collective-permute-start(bf16[64,2048]{1,0:T(8,128)(2,1)S(1)} %slice.23.refs_1_), channel_id=1, source_target_pairs={{0,3},{1,0},{2,1},{3,2},{4,7},{5,4},{6,5},{7,6},{8,11},{9,8},{10,9... | collective-permute-start | bytes 786440 | tf_op jit(solution)/shard_map/ppermute | solution.py:285
  102.3 5.8 %collective-permute-done.8.refs_2_ = bf16[64,2048]{1,0:T(8,128)(2,1)S(1)} collective-permute-done((bf16[64,2048]{1,0:T(8,128)(2,1)S(1)}, bf16[64,2048]{1,0:T(8,128)(2,1)S(1)}, u32[]{:S(2)}, u32[]{:S(2)}) %collective-permute-start.8) | collective-permute-done | bytes 262176 | tf_op jit(solution)/shard_map/ppermute | solution.py:285
  108.1 2.7 %collective-permute-start.13 = (bf16[64,2048]{1,0:T(8,128)(2,1)S(1)}, bf16[64,2048]{1,0:T(8,128)(2,1)S(1)}, u32[]{:S(2)}, u32[]{:S(2)}) collective-permute-start(bf16[64,2048]{1,0:T(8,128)(2,1)S(1)} %collective-permute-done.11.refs_5_), channel_id=1, source_target_pairs={{0,3},{1,0},{2,1},{3,2},{4,7},{5,4},{6,5},{7,6},{8,11},{9,8},{10,9... | collective-permute-start | bytes 786440 | tf_op jit(solution)/shard_map/ppermute | solution.py:285
  110.8 1.6 copy-done.1
  112.4 1.6 copy-done.2
  114.6 1.5 collective-permute-start.9
  117.2 3.5 %collective-permute-done.10.refs_4_ = bf16[64,2048]{1,0:T(8,128)(2,1)S(1)} collective-permute-done((bf16[64,2048]{1,0:T(8,128)(2,1)S(1)}, bf16[64,2048]{1,0:T(8,128)(2,1)S(1)}, u32[]{:S(2)}, u32[]{:S(2)}) %collective-permute-start.10) | collective-permute-done | bytes 262176 | tf_op jit(solution)/shard_map/ppermute | solution.py:285
  121.9 2.7 %shard_map.194 = (bf16[64,2048]{1,0:T(8,128)(2,1)S(1)}, bf16[64,2048]{1,0:T(8,128)(2,1)S(1)}, bf16[64,2048]{1,0:T(8,128)(2,1)S(1)}, bf16[64,2048]{1,0:T(8,128)(2...) custom-call(bf16[64,2048]{1,0:T(8,128)(2,1)S(1)} %slice.21.refs_0_, ...), custom_call_target="tpu_custom_call" | custom-call | flops 3000000000 | tf_op jit(solution)/shard_map/pallas_call | solution.py:362
  124.6 2.5 %collective-permute-start.16 = (bf16[64,2048]{1,0:T(8,128)(2,1)S(1)}, bf16[64,2048]{1,0:T(8,128)(2,1)S(1)}, u32[]{:S(2)}, u32[]{:S(2)}) collective-permute-start(bf16[64,2048]{1,0:T(8,128)(2,1)S(1)} %get-tuple-element.40), channel_id=1, source_target_pairs={{0,3},{1,0},{2,1},{3,2},{4,7},{5,4},{6,5},{7,6},{8,11},{9,8},{10,9... | collective-permute-start | bytes 786440 | tf_op jit(solution)/shard_map/ppermute | solution.py:285
  127.1 2.7 %collective-permute-start.18 = (bf16[64,2048]{1,0:T(8,128)(2,1)S(1)}, bf16[64,2048]{1,0:T(8,128)(2,1)S(1)}, u32[]{:S(2)}, u32[]{:S(2)}) collective-permute-start(bf16[64,2048]{1,0:T(8,128)(2,1)S(1)} %get-tuple-element.44), channel_id=1, source_target_pairs={{0,3},{1,0},{2,1},{3,2},{4,7},{5,4},{6,5},{7,6},{8,11},{9,8},{10,9... | collective-permute-start | bytes 786440 | tf_op jit(solution)/shard_map/ppermute | solution.py:285
  129.9 6.0 %collective-permute-done.18 = bf16[64,2048]{1,0:T(8,128)(2,1)S(1)} collective-permute-done((bf16[64,2048]{1,0:T(8,128)(2,1)S(1)}, bf16[64,2048]{1,0:T(8,128)(2,1)S(1)}, u32[]{:S(2)}, u32[]{:S(2)}) %collective-permute-start.18) | collective-permute-done | bytes 262176 | tf_op jit(solution)/shard_map/ppermute | solution.py:285
  136.0 3.5 %collective-permute-start.19 = (bf16[64,2048]{1,0:T(8,128)(2,1)S(1)}, bf16[64,2048]{1,0:T(8,128)(2,1)S(1)}, u32[]{:S(2)}, u32[]{:S(2)}) collective-permute-start(bf16[64,2048]{1,0:T(8,128)(2,1)S(1)} %add_convert_fusion.1), channel_id=1, source_target_pairs={{0,3},{1,0},{2,1},{3,2},{4,7},{5,4},{6,5},{7,6},{8,11},{9,8},{10,9... | collective-permute-start | bytes 786440 | tf_op jit(solution)/shard_map/ppermute | solution.py:285
  139.6 3.2 %collective-permute-done.19 = bf16[64,2048]{1,0:T(8,128)(2,1)S(1)} collective-permute-done((bf16[64,2048]{1,0:T(8,128)(2,1)S(1)}, bf16[64,2048]{1,0:T(8,128)(2,1)S(1)}, u32[]{:S(2)}, u32[]{:S(2)}) %collective-permute-start.19) | collective-permute-done | bytes 262176 | tf_op jit(solution)/shard_map/ppermute | solution.py:285
  143.3 26.7 %all_to_all.25 = bf16[64,2,2048]{2,1,0:T(2,128)(2,1)S(1)} all-to-all(bf16[64,2,2048]{2,1,0:T(2,128)(2,1)S(1)} %convert_element_type.53), channel_id=1, replica_groups=mesh['z'=8,'x'=4,'c'=2,'y'=4] {'z','x','c'}, dimensions={0} | all-to-all | bytes 1048576 | tf_op jit(solution)/shard_map/all_to_all | solution.py:394
  (58 shorter events, 12.0 us)
Async XLA Ops:
  0.6 37.2 %copy-start.7 = (s32[4]{0:T(128)S(1)}, s32[4]{0:T(128)}, u32[]{:S(2)}) copy-start(s32[4]{0:T(128)} %pad_add_fusion.place_ref) | copy-start | bytes 52
  3.7 34.1 %copy-start.4 = (bf16[256,128]{1,0:T(8,128)(2,1)S(1)}, bf16[256,128]{1,0:T(8,128)(2,1)}, u32[]{:S(2)}) copy-start(bf16[256,128]{1,0:T(8,128)(2,1)} %get-tuple-element.28.q0) | copy-start | bytes 196612
  3.7 34.1 %all-to-all-start = ((bf16[8,416,128]{2,1,0:T(8,128)(2,1)}), bf16[8,416,128]{2,1,0:T(8,128)(2,1)S(1)}, u32[]{:S(2)}, u32[]{:S(2)}) async-start(bf16[8,416,128]{2,1,0:T(8,128)(2,1)} %get-tuple-element.25), calls=%async_computation | async-start | bytes 1703936 | tf_op jit(solution)/shard_map/all_to_all | solution.py:307
  12.8 19.7 %collective-permute-start = (bf16[192,2048]{1,0:T(8,128)(2,1)}, bf16[192,2048]{1,0:T(8,128)(2,1)S(1)}, u32[]{:S(2)}, u32[]{:S(2)}) collective-permute-start(bf16[192,2048]{1,0:T(8,128)(2,1)} %get-tuple-element.26.w0), channel_id=1, source_target_pairs={{0,1},{1,2},{2,3},{3,0},{4,5},{5,6},{6,7},{7,4},{8,9},{9,10},{10,1... | collective-permute-start | bytes 2359304 | tf_op jit(solution)/shard_map/ppermute | solution.py:285
  14.1 18.4 %collective-permute-start.1 = (bf16[192,2048]{1,0:T(8,128)(2,1)}, bf16[192,2048]{1,0:T(8,128)(2,1)}, u32[]{:S(2)}, u32[]{:S(2)}) collective-permute-start(bf16[192,2048]{1,0:T(8,128)(2,1)} %get-tuple-element.26.w0), channel_id=1, source_target_pairs={{0,3},{1,0},{2,1},{3,2},{4,7},{5,4},{6,5},{7,6},{8,11},{9,8},{10,9... | collective-permute-start | bytes 2359304 | tf_op jit(solution)/shard_map/ppermute | solution.py:285
  15.6 4.8 %collective-permute-start.2 = (bf16[256,128]{1,0:T(8,128)(2,1)}, bf16[256,128]{1,0:T(8,128)(2,1)S(1)}, u32[]{:S(2)}, u32[]{:S(2)}) collective-permute-start(bf16[256,128]{1,0:T(8,128)(2,1)} %get-tuple-element.28.q0), channel_id=1, source_target_pairs={{0,8},{8,16},{16,24},{24,0},{1,9},{9,17},{17,25},{25,1},{2,10},{10... | collective-permute-start | bytes 196616 | tf_op jit(solution)/shard_map/ppermute | solution.py:285
  16.8 3.7 %collective-permute-start.3 = (bf16[256,128]{1,0:T(8,128)(2,1)}, bf16[256,128]{1,0:T(8,128)(2,1)S(1)}, u32[]{:S(2)}, u32[]{:S(2)}) collective-permute-start(bf16[256,128]{1,0:T(8,128)(2,1)} %get-tuple-element.28.q0), channel_id=1, source_target_pairs={{0,24},{8,0},{16,8},{24,16},{1,25},{9,1},{17,9},{25,17},{2,26},{10... | collective-permute-start | bytes 196616 | tf_op jit(solution)/shard_map/ppermute | solution.py:285
  18.3 5.7 %collective-permute-start.4 = (bf16[256,128]{1,0:T(8,128)(2,1)}, bf16[256,128]{1,0:T(8,128)(2,1)S(1)}, u32[]{:S(2)}, u32[]{:S(2)}) collective-permute-start(bf16[256,128]{1,0:T(8,128)(2,1)} %get-tuple-element.28.q0), channel_id=1, source_target_pairs={{0,16},{8,24},{16,0},{24,8},{1,17},{9,25},{17,1},{25,9},{2,18},{10... | collective-permute-start | bytes 196616 | tf_op jit(solution)/shard_map/ppermute | solution.py:285
  24.9 12.9 %collective-permute-start.5 = (bf16[4,256,128]{2,1,0:T(8,128)(2,1)S(1)}, bf16[4,256,128]{2,1,0:T(8,128)(2,1)S(1)}, u32[]{:S(2)}, u32[]{:S(2)}) collective-permute-start(bf16[4,256,128]{2,1,0:T(8,128)(2,1)S(1)} %pad_maximum_fusion.1), channel_id=1, source_target_pairs={{0,4},{4,0},{1,5},{5,1},{2,6},{6,2},{3,7},{7,3},{8,12},{12,8},{9,1... | collective-permute-start | bytes 786440 | tf_op jit(solution)/shard_map/ppermute | solution.py:285
  32.5 5.3 %copy-start.9 = (bf16[192,2048]{1,0:T(8,128)(2,1)}, bf16[192,2048]{1,0:T(8,128)(2,1)S(1)}, u32[]{:S(2)}) copy-start(bf16[192,2048]{1,0:T(8,128)(2,1)S(1)} %collective-permute-done.w1) | copy-start | bytes 2359300
  42.5 25.6 %all-to-all-start.1 = ((bf16[32,64,128]{2,1,0:T(8,128)(2,1)}), bf16[32,64,128]{2,1,0:T(8,128)(2,1)S(1)}, u32[]{:S(2)}, u32[]{:S(2)}) async-start(bf16[32,64,128]{2,1,0:T(8,128)(2,1)} %bitcast.14), calls=%async_computation.1 | async-start | bytes 1048576 | tf_op jit(solution)/shard_map/all_to_all | solution.py:334
  51.1 16.9 %collective-permute-start.6 = (bf16[96,2048]{1,0:T(8,128)(2,1)S(1)}, bf16[96,2048]{1,0:T(8,128)(2,1)S(1)}, u32[]{:S(2)}, u32[]{:S(2)}) collective-permute-start(bf16[96,2048]{1,0:T(8,128)(2,1)S(1)} %slice.18), channel_id=1, source_target_pairs={{0,1},{1,2},{2,3},{3,0},{4,5},{5,6},{6,7},{7,4},{8,9},{9,10},{10,1... | collective-permute-start | bytes 1179656 | tf_op jit(solution)/shard_map/ppermute | solution.py:285
  53.6 14.5 %collective-permute-start.7 = (bf16[96,2048]{1,0:T(8,128)(2,1)S(1)}, bf16[96,2048]{1,0:T(8,128)(2,1)}, u32[]{:S(2)}, u32[]{:S(2)}) collective-permute-start(bf16[96,2048]{1,0:T(8,128)(2,1)S(1)} %slice.19), channel_id=1, source_target_pairs={{0,3},{1,0},{2,1},{3,2},{4,7},{5,4},{6,5},{7,6},{8,11},{9,8},{10,9... | collective-permute-start | bytes 1179656 | tf_op jit(solution)/shard_map/ppermute | solution.py:285
  68.1 0.9 copy-start.8
  73.8 37.1 %copy-start = (bf16[1,2048,512]{2,1,0:T(8,128)(2,1)S(1)}, bf16[1,2048,512]{2,1,0:T(8,128)(2,1)}, u32[]{:S(2)}) copy-start(bf16[1,2048,512]{2,1,0:T(8,128)(2,1)} %param.33) | copy-start | bytes 6291460
  99.4 8.8 %collective-permute-start.8 = (bf16[64,2048]{1,0:T(8,128)(2,1)S(1)}, bf16[64,2048]{1,0:T(8,128)(2,1)S(1)}, u32[]{:S(2)}, u32[]{:S(2)}) collective-permute-start(bf16[64,2048]{1,0:T(8,128)(2,1)S(1)} %slice.21.refs_0_), channel_id=1, source_target_pairs={{0,1},{1,2},{2,3},{3,0},{4,5},{5,6},{6,7},{7,4},{8,9},{9,10},{10,1... | collective-permute-start | bytes 786440 | tf_op jit(solution)/shard_map/ppermute | solution.py:285
  99.6 8.6 %collective-permute-start.11 = (bf16[64,2048]{1,0:T(8,128)(2,1)S(1)}, bf16[64,2048]{1,0:T(8,128)(2,1)S(1)}, u32[]{:S(2)}, u32[]{:S(2)}) collective-permute-start(bf16[64,2048]{1,0:T(8,128)(2,1)S(1)} %slice.23.refs_1_), channel_id=1, source_target_pairs={{0,3},{1,0},{2,1},{3,2},{4,7},{5,4},{6,5},{7,6},{8,11},{9,8},{10,9... | collective-permute-start | bytes 786440 | tf_op jit(solution)/shard_map/ppermute | solution.py:285
  108.1 7.9 %collective-permute-start.12 = (bf16[64,2048]{1,0:T(8,128)(2,1)S(1)}, bf16[64,2048]{1,0:T(8,128)(2,1)S(1)}, u32[]{:S(2)}, u32[]{:S(2)}) collective-permute-start(bf16[64,2048]{1,0:T(8,128)(2,1)S(1)} %collective-permute-done.8.refs_2_), channel_id=1, source_target_pairs={{0,1},{1,2},{2,3},{3,0},{4,5},{5,6},{6,7},{7,4},{8,9},{9,10},{10,1... | collective-permute-start | bytes 786440 | tf_op jit(solution)/shard_map/ppermute | solution.py:285
  108.1 7.9 %collective-permute-start.13 = (bf16[64,2048]{1,0:T(8,128)(2,1)S(1)}, bf16[64,2048]{1,0:T(8,128)(2,1)S(1)}, u32[]{:S(2)}, u32[]{:S(2)}) collective-permute-start(bf16[64,2048]{1,0:T(8,128)(2,1)S(1)} %collective-permute-done.11.refs_5_), channel_id=1, source_target_pairs={{0,3},{1,0},{2,1},{3,2},{4,7},{5,4},{6,5},{7,6},{8,11},{9,8},{10,9... | collective-permute-start | bytes 786440 | tf_op jit(solution)/shard_map/ppermute | solution.py:285
  110.8 1.6 copy-start.1
  112.4 1.6 copy-start.2
  114.5 6.2 %collective-permute-start.10 = (bf16[64,2048]{1,0:T(8,128)(2,1)S(1)}, bf16[64,2048]{1,0:T(8,128)(2,1)S(1)}, u32[]{:S(2)}, u32[]{:S(2)}) collective-permute-start(bf16[64,2048]{1,0:T(8,128)(2,1)S(1)} %slice.21.refs_0_), channel_id=1, source_target_pairs={{0,3},{1,0},{2,1},{3,2},{4,7},{5,4},{6,5},{7,6},{8,11},{9,8},{10,9... | collective-permute-start | bytes 786440 | tf_op jit(solution)/shard_map/ppermute | solution.py:285
  114.6 7.3 %collective-permute-start.9 = (bf16[64,2048]{1,0:T(8,128)(2,1)S(1)}, bf16[64,2048]{1,0:T(8,128)(2,1)S(1)}, u32[]{:S(2)}, u32[]{:S(2)}) collective-permute-start(bf16[64,2048]{1,0:T(8,128)(2,1)S(1)} %slice.23.refs_1_), channel_id=1, source_target_pairs={{0,1},{1,2},{2,3},{3,0},{4,5},{5,6},{6,7},{7,4},{8,9},{9,10},{10,1... | collective-permute-start | bytes 786440 | tf_op jit(solution)/shard_map/ppermute | solution.py:285
  117.1 12.6 %collective-permute-start.14 = (bf16[64,2048]{1,0:T(8,128)(2,1)S(1)}, bf16[64,2048]{1,0:T(8,128)(2,1)S(1)}, u32[]{:S(2)}, u32[]{:S(2)}) collective-permute-start(bf16[64,2048]{1,0:T(8,128)(2,1)S(1)} %get-tuple-element.39), channel_id=1, source_target_pairs={{0,1},{1,2},{2,3},{3,0},{4,5},{5,6},{6,7},{7,4},{8,9},{9,10},{10,1... | collective-permute-start | bytes 786440 | tf_op jit(solution)/shard_map/ppermute | solution.py:285
  124.6 14.9 %collective-permute-start.16 = (bf16[64,2048]{1,0:T(8,128)(2,1)S(1)}, bf16[64,2048]{1,0:T(8,128)(2,1)S(1)}, u32[]{:S(2)}, u32[]{:S(2)}) collective-permute-start(bf16[64,2048]{1,0:T(8,128)(2,1)S(1)} %get-tuple-element.40), channel_id=1, source_target_pairs={{0,3},{1,0},{2,1},{3,2},{4,7},{5,4},{6,5},{7,6},{8,11},{9,8},{10,9... | collective-permute-start | bytes 786440 | tf_op jit(solution)/shard_map/ppermute | solution.py:285
  127.1 12.5 %collective-permute-start.17 = (bf16[64,2048]{1,0:T(8,128)(2,1)S(1)}, bf16[64,2048]{1,0:T(8,128)(2,1)S(1)}, u32[]{:S(2)}, u32[]{:S(2)}) collective-permute-start(bf16[64,2048]{1,0:T(8,128)(2,1)S(1)} %get-tuple-element.42), channel_id=1, source_target_pairs={{0,1},{1,2},{2,3},{3,0},{4,5},{5,6},{6,7},{7,4},{8,9},{9,10},{10,1... | collective-permute-start | bytes 786440 | tf_op jit(solution)/shard_map/ppermute | solution.py:285
  127.1 8.8 %collective-permute-start.18 = (bf16[64,2048]{1,0:T(8,128)(2,1)S(1)}, bf16[64,2048]{1,0:T(8,128)(2,1)S(1)}, u32[]{:S(2)}, u32[]{:S(2)}) collective-permute-start(bf16[64,2048]{1,0:T(8,128)(2,1)S(1)} %get-tuple-element.44), channel_id=1, source_target_pairs={{0,3},{1,0},{2,1},{3,2},{4,7},{5,4},{6,5},{7,6},{8,11},{9,8},{10,9... | collective-permute-start | bytes 786440 | tf_op jit(solution)/shard_map/ppermute | solution.py:285
  129.8 9.6 %collective-permute-start.15 = (bf16[64,2048]{1,0:T(8,128)(2,1)S(1)}, bf16[64,2048]{1,0:T(8,128)(2,1)S(1)}, u32[]{:S(2)}, u32[]{:S(2)}) collective-permute-start(bf16[64,2048]{1,0:T(8,128)(2,1)S(1)} %add_convert_fusion.3), channel_id=1, source_target_pairs={{0,1},{1,2},{2,3},{3,0},{4,5},{5,6},{6,7},{7,4},{8,9},{9,10},{10,1... | collective-permute-start | bytes 786440 | tf_op jit(solution)/shard_map/ppermute | solution.py:285
  136.0 6.8 %collective-permute-start.19 = (bf16[64,2048]{1,0:T(8,128)(2,1)S(1)}, bf16[64,2048]{1,0:T(8,128)(2,1)S(1)}, u32[]{:S(2)}, u32[]{:S(2)}) collective-permute-start(bf16[64,2048]{1,0:T(8,128)(2,1)S(1)} %add_convert_fusion.1), channel_id=1, source_target_pairs={{0,3},{1,0},{2,1},{3,2},{4,7},{5,4},{6,5},{7,6},{8,11},{9,8},{10,9... | collective-permute-start | bytes 786440 | tf_op jit(solution)/shard_map/ppermute | solution.py:285
  142.9 27.3 %copy-start.3 = (bf16[32,2048]{1,0:T(8,128)(2,1)S(1)}, bf16[32,2048]{1,0:T(8,128)(2,1)}, u32[]{:S(2)}) copy-start(bf16[32,2048]{1,0:T(8,128)(2,1)} %get-tuple-element.31.mid_ref) | copy-start | bytes 393220
  142.9 27.3 %copy-start.5 = (bf16[2,32,128]{2,1,0:T(8,128)(2,1)S(1)}, bf16[2,32,128]{2,1,0:T(8,128)(2,1)}, u32[]{:S(2)}) copy-start(bf16[2,32,128]{2,1,0:T(8,128)(2,1)} %get-tuple-element.32.pick_ref) | copy-start | bytes 49156
  142.9 27.3 %copy-start.6 = (f32[32,2]{0,1:T(2,128)S(1)}, f32[32,2]{0,1:T(2,128)}, u32[]{:S(2)}) copy-start(f32[32,2]{0,1:T(2,128)} %param.37) | copy-start | bytes 772
  (1 other events, 0.8 us)

commit v3 on v2

--- a/solution.py
+++ b/solution.py
@@ -30,6 +30,7 @@
 SCALE_S = (NOPE_S + ROPE) ** -0.5 * LOG2E
 SCALE_L = (NOPE_L + ROPE) ** -0.5 * LOG2E
 
+
 f32 = jnp.float32
 bf16 = jnp.bfloat16
 
@@ -63,7 +64,7 @@
 
 def pre_kernel(
     place_ref, lat_ref, gain_ref, rk_ref, qs_ref, ql_ref, ks_w, vs_w, kl_w, vl_w,
-    base_ref, row_ref, lo_ref, so_ref, kv_ref, q_ref, wo_ref,
+    base_ref, row_ref, lo_ref, so_ref, kv_ref, q_ref, top_ref, low_ref,
 ):
     block = (place_ref[0] * NX + place_ref[1]) * NC + place_ref[2]
     base = column(base_ref[pl.ds(block, 1), :])
@@ -101,11 +102,13 @@
         axis=0,
     )
     q_ref[128:256, :] = mixed.T.astype(bf16)
-    wo_ref[0:128, :] = lo_ref[...]
-    wo_ref[128:192, :] = so_ref[...]
-
-
-def attn_kernel(place_ref, kv_ref, q0, q1, q2, q3, r_ref, out_ref, kl, ks, vl, vs):
+    top_ref[...] = lo_ref[0:96, :]
+    low_ref[0:32, :] = lo_ref[96:128, :]
+    low_ref[32:96, :] = so_ref[...]
+
+
+def attn_kernel(other, place_ref, kv_ref, *refs):
+    queries, (out_ref, kl, ks, vl, vs) = refs[:-5], refs[-5:]
     z, x, c = place_ref[0], place_ref[1], place_ref[2]
     kl[128:192, :] = jnp.zeros((64, 1024), bf16)
     kl[224:256, :] = jnp.zeros((32, 1024), bf16)
@@ -125,19 +128,17 @@
     kpos = (key // ROWS) * (NXC * ROWS) + (x * NC + c) * ROWS + lax.rem(key, ROWS)
     row = lax.broadcasted_iota(jnp.int32, (2 * ROWS, 1), 0)
     lanes = lax.broadcasted_iota(jnp.int32, (2 * ROWS, 128), 1)
-    for d, (shift, mine) in enumerate(((0, q0), (1, q1), (3, q2), (2, q3))):
-        xq = lax.rem(x + (NX - shift), NX)
-        b_mine = xq * NC + c
-        b_other = xq * NC + (1 - c)
+    core = 1 - c if other else c
+    for d in (0, 2):
+        block = [queries[0][d + i] if other else queries[d + i][...] for i in range(2)]
+        xq = [lax.rem(x + (NX - s), NX) for s in ((0, 1) if d == 0 else (3, 2))]
         q = jnp.concatenate(
-            [
-                jnp.concatenate([mine[0:128, :], mine[128:256, :]], axis=1),
-                jnp.concatenate([r_ref[d, 0:128, :], r_ref[d, 128:256, :]], axis=1),
-            ],
-            axis=0,
+            [jnp.concatenate([b[0:128, :], b[128:256, :]], axis=1) for b in block], axis=0
         )
         qpos = z * (NXC * ROWS) + jnp.where(
-            row < ROWS, b_mine * ROWS + row, b_other * ROWS + row - ROWS
+            row < ROWS,
+            (xq[0] * NC + core) * ROWS + row,
+            (xq[1] * NC + core) * ROWS + row - ROWS,
         )
         allowed = kpos <= qpos
 
@@ -160,23 +161,54 @@
             o_s = jnp.where(lanes == i, v, o_s)
         o_l = o_l.astype(bf16)
         o_s = o_s.astype(bf16)
-        for half, b in ((0, b_mine), (1, b_other)):
+        for half in range(2):
             for y in range(NY):
                 lo = half * ROWS + y * TOK
-                out_ref[b, y, 0:TOK, :] = o_l[lo : lo + TOK]
-                out_ref[b, y, TOK : 2 * TOK, :] = o_s[lo : lo + TOK]
+                out_ref[xq[half], y, 0:TOK, :] = o_l[lo : lo + TOK]
+                out_ref[xq[half], y, TOK : 2 * TOK, :] = o_s[lo : lo + TOK]
+
+
+def merge_kernel(a_ref, b_ref, out_ref):
+    rows = NX * NY * TOK
+    ref = [r[...].astype(f32) for r in (a_ref, b_ref)]
+    large = [r[:, :TOK].reshape(rows, 128) for r in ref]
+    small = [r[:, TOK:].reshape(rows, 128) for r in ref]
+    lanes = lax.broadcasted_iota(jnp.int32, (rows, 128), 1)
+    outs = []
+    stats = []
+    for at, scale, values in ((0, SCALE_L, large), (3, SCALE_S, small)):
+        tops = [s[:, at : at + 1] for s in small]
+        top = jnp.maximum(tops[0], tops[1])
+        ws = [
+            (s[:, at + 1 : at + 2] + s[:, at + 2 : at + 3]) * jnp.exp2((t - top) * scale)
+            for s, t in zip(small, tops)
+        ]
+        total = ws[0] + ws[1]
+        outs.append(values[0] * (ws[0] / total) + values[1] * (ws[1] / total))
+        high = total.astype(bf16).astype(f32)
+        stats += [top, high, total - high]
+    for i, v in enumerate(stats):
+        outs[1] = jnp.where(lanes == i, v, outs[1])
+    out_ref[:, :TOK] = outs[0].astype(bf16).reshape(NX * NY, TOK, 128)
+    out_ref[:, TOK:] = outs[1].astype(bf16).reshape(NX * NY, TOK, 128)
 
 
 def mid_kernel(
-    place_ref, parts_ref, w0, w1, w3, w2a, w2b, res_ref, gain_ref, routing_ref,
-    disp_ref, mid_ref, pick_ref,
+    place_ref, parts_ref, res_ref, gain_ref, routing_ref, *refs
 ):
+    sources, (disp_ref, mid_ref, pick_ref, w_ref, sems) = refs[:8], refs[8:]
+    copies = [
+        pltpu.make_async_copy(src, w_ref.at[i // 2, pl.ds(96 * (i % 2), 96)], sems.at[i])
+        for i, src in enumerate(sources)
+    ]
+    for copy in copies:
+        copy.start()
     y = place_ref[3]
     total = jnp.zeros((TOK, D), f32)
-    for shift, weights in ((0, (w0, w0, 96)), (1, (w1, w1, 96)), (3, (w3, w3, 96)), (2, (w2a, w2b, 0))):
+    for n, shift in enumerate((0, 1, 3, 2)):
         ya = lax.rem(y + (NY - shift), NY)
-        larges = [parts_ref[i, ya, 0:TOK, :].astype(f32) for i in range(NXC)]
-        smalls = [parts_ref[i, ya, TOK : 2 * TOK, :].astype(f32) for i in range(NXC)]
+        larges = [parts_ref[i, ya, 0:TOK, :].astype(f32) for i in range(NX)]
+        smalls = [parts_ref[i, ya, TOK : 2 * TOK, :].astype(f32) for i in range(NX)]
 
         def mixed(values, at, scale):
             tops = [s[:, at : at + 1] for s in smalls]
@@ -191,11 +223,9 @@
         large = mixed(larges, 0, SCALE_L).astype(bf16)
         small = mixed(smalls, 3, SCALE_S)[:, 64:128].astype(bf16)
         heads = jnp.concatenate([large, small], axis=1)
-        first, second, at = weights
-        partial = jnp.dot(heads[:, :96], first[0:96, :], preferred_element_type=f32)
-        partial = partial + jnp.dot(
-            heads[:, 96:192], second[at : at + 96, :], preferred_element_type=f32
-        )
+        copies[2 * n].wait()
+        copies[2 * n + 1].wait()
+        partial = jnp.dot(heads, w_ref[n], preferred_element_type=f32)
         total = total + partial.astype(bf16).astype(f32)
     attention = total.astype(bf16).astype(f32)
     middle = (res_ref[...].astype(f32) + attention).astype(bf16)
@@ -222,9 +252,11 @@
         pick = jnp.where(lane == r[k] * CAP + slot.astype(jnp.int32), 1.0, 0.0)
         pick_ref[k] = pick.astype(bf16)
         send = send + pick
-    disp_ref[...] = lax.dot_general(
+    disp = lax.dot_general(
         send.astype(bf16), normed, (((0,), (0,)), ((), ())), preferred_element_type=f32
     ).astype(bf16)
+    for e in range(EXPERTS):
+        disp_ref[e] = disp[CAP * e : CAP * e + CAP]
 
 
 def load_kernel(a, b, c, out_a, out_b, out_c, sems):
@@ -292,10 +324,10 @@
 ):
     place = jnp.stack([lax.axis_index(a) for a in ("z", "x", "c", "y")]).astype(jnp.int32)
     base, row = rope_parts()
-    kv, q, wo = call(
+    kv, q, top, low = call(
         pre_kernel,
         [smem()] + vmem(13),
-        [((NZ, 416, 128), bf16), ((256, 128), bf16), ((192, D), bf16)],
+        [((NZ, 416, 128), bf16), ((256, 128), bf16), ((96, D), bf16), ((96, D), bf16)],
         flops=10**9,
         mib=63,
     )(
@@ -311,40 +343,52 @@
         qx.append(shifted(q, "x", NX, by))
     qc = shifted(jnp.stack(qx), "c", NC, 1)
 
-    wo_p = shifted(wo, "y", NY, 1)
-    wo_m = shifted(wo, "y", NY, -1)
-    kvs, wo_p, wo_m = lax.optimization_barrier((kvs, wo_p, wo_m))
-    wo_a = shifted(wo_p[:96], "y", NY, 1)
-    wo_b = shifted(wo_m[96:], "y", NY, -1)
-
-    attend = call(
-        attn_kernel,
-        [smem()] + vmem(6),
-        [((NXC, NY, 2 * TOK, 128), bf16)],
-        scratch=[
-            pltpu.VMEM((256, 1024), bf16),
-            pltpu.VMEM((128, 1024), bf16),
-            pltpu.VMEM((1024, 256), bf16),
-            pltpu.VMEM((128, 1024), bf16),
-        ],
-        flops=3 * 10**9,
-        mib=24,
-    )
-    parts = attend(place, kvs, *qx, qc)
+    top_p = shifted(top, "y", NY, 1)
+    low_m = shifted(low, "y", NY, -1)
+    low_p = shifted(low, "y", NY, 1)
+    top_m = shifted(top, "y", NY, -1)
+    top_o = shifted(top_p, "y", NY, 1)
+    low_o = shifted(low_m, "y", NY, -1)
+
+    def attend(other, *queries):
+        return call(
+            functools.partial(attn_kernel, other),
+            [smem()] + vmem(1 + len(queries)),
+            [((NX, NY, 2 * TOK, 128), bf16)],
+            scratch=[
+                pltpu.VMEM((256, 1024), bf16),
+                pltpu.VMEM((128, 1024), bf16),
+                pltpu.VMEM((1024, 256), bf16),
+                pltpu.VMEM((128, 1024), bf16),
+            ],
+            flops=2 * 10**9,
+            mib=20,
+        )(place, kvs, *queries).reshape(NX * NY, 2 * TOK, 128)
+
+    theirs = attend(True, qc)
+    theirs = shifted(theirs, "c", NC, 1)
+    ours = attend(False, *qx)
+    parts = call(merge_kernel, vmem(2), [((NX * NY, 2 * TOK, 128), bf16)], flops=5 * 10**8)(
+        ours, theirs
+    )
     parts = lax.all_to_all(
-        parts.reshape(NXC * NY * 2 * TOK, 128), ("x", "c", "y"), 0, 0, tiled=True
-    ).reshape(NXC, NY, 2 * TOK, 128)
+        parts.reshape(NX * NY * 2 * TOK, 128), ("x", "y"), 0, 0, tiled=True
+    ).reshape(NX, NY, 2 * TOK, 128)
 
     disp, middle, pick = call(
         mid_kernel,
-        [smem()] + vmem(9),
-        [((SLOTS, D), bf16), ((TOK, D), bf16), ((2, TOK, SLOTS), bf16)],
+        [smem()] + vmem(4) + [pl.BlockSpec(memory_space=pltpu.HBM) for _ in range(8)],
+        [((EXPERTS, CAP, D), bf16), ((TOK, D), bf16), ((2, TOK, SLOTS), bf16)],
+        scratch=[pltpu.VMEM((NY, 192, D), bf16), pltpu.SemaphoreType.DMA((8,))],
         flops=2 * 10**9,
         mib=63,
-    )(place, parts, wo, wo_p, wo_m, wo_a, wo_b, residual, ffn_gain[None, :], routing.T)
+    )(
+        place, parts, residual, ffn_gain[None, :], routing.T,
+        top, low, top_p, low_p, top_m, low_m, top_o, low_o,
+    )
 
     sp = ("z", "x", "c")
-    mine = lax.all_to_all(disp.reshape(EXPERTS, CAP, D), sp, 0, 0, tiled=True)
+    mine = lax.all_to_all(disp, sp, 0, 0, tiled=True)
     mine = mine.reshape(SLOTS, D)
 
     half = SLOTS // 2

time: 172 us -> 167 us (0.971)
  waiting for transfers between devices: 47.4 us -> 40.3 us
  local copies, waits for them, and re-layouts: 8.82 us -> 5.02 us
  starting transfers between devices: 44.9 us -> 47.3 us
  Pallas kernels: 17.6 us -> 19.6 us
    ppermute x20 -> x23, waiting for transfers between devices: 42.1 us -> 27 us  [shifted(): return lax.ppermute(a, axis, [(i, (i + by) % size) for i in range(size)])]
    all_to_all x1, waiting for transfers between devices: 5.27 us -> 11.1 us  [layer(): kvs = lax.all_to_all(kv, 'z', 0, 0, tiled=True)]
    ppermute x20 -> x23, starting transfers between devices: 28.2 us -> 31.6 us  [shifted(): return lax.ppermute(a, axis, [(i, (i + by) % size) for i in range(size)])]
    all_to_all x1, waiting for transfers between devices: 0.01 us -> 2.2 us  [layer(): lax.all_to_all(parts.reshape(NX * NY * 2 * TOK, 128), ('x', 'y'), 0, 0, t...]
    slice x2 -> x0, local copies, waits for them, and re-layouts: 2.04 us -> none  [the longest x1 1.02 us: layer(): wo_a = shifted(wo_p[:96], 'y', NY, 1)]
    pallas_call x2 -> x4, Pallas kernels: 9.43 us -> 11.4 us  [the longest x2 5.06 us: attend(): call(functools.partial(attn_kernel, other), [smem()] + vmem(1 + len(queri...]
  transfers between devices with their start and end apart: 22 -> 25, of which waited for: 11 -> 10; matrix products, arithmetic and copies ran while one was open for 2% -> 1% of each run, Pallas kernels for 2% -> 7%
where the time goes in v3:
time: 167 us; the launch traced here: 166 us
  blocking collectives  51.9 us (31%)
  starting transfers between devices  47.3 us (28%)
  waiting for transfers between devices  40.3 us (24%)
  Pallas kernels  19.6 us (12%)
  local copies, waits for them, and re-layouts  5.02 us (3%)
  other arithmetic  1.86 us (1%)
    ppermute x23, starting transfers between devices, shifted(): return lax.ppermute(a, axis, [(i, (i + by) % size) for i in range(size)])  31.6 us
    all_to_all x1, blocking collectives, layer(): ret = lax.all_to_all(done.reshape(EXPERTS, CAP, D), sp, 0, 0, tiled=True)  27.2 us
    ppermute x23, waiting for transfers between devices, shifted(): return lax.ppermute(a, axis, [(i, (i + by) % size) for i in range(size)])  27 us
    all_to_all x1, blocking collectives, layer(): mine = lax.all_to_all(disp, sp, 0, 0, tiled=True)  24.7 us
    all_to_all x1, waiting for transfers between devices, layer(): kvs = lax.all_to_all(kv, 'z', 0, 0, tiled=True)  11.1 us
    all_to_all x1, starting transfers between devices, layer(): kvs = lax.all_to_all(kv, 'z', 0, 0, tiled=True)  9.15 us
    all_to_all x1, starting transfers between devices, layer(): lax.all_to_all(parts.reshape(NX * NY * 2 * TOK, 128), ('x', 'y'), 0, 0, t...  6.52 us
    pallas_call x2, Pallas kernels, attend(): call(functools.partial(attn_kernel, other), [smem()] + vmem(1 + len(queri...  5.06 us
  transfers between devices with their start and end apart: 25, of which 10 were waited for; matrix products, arithmetic and copies ran while one was open for 1% of the time, Pallas kernels for 7%

profile of v3, /device:TPU:1, one launch (start us, length us, event | category | flops | bytes accessed | tf_op | source)
XLA Modules:
  0.0 166.2 jit_solution(1171250185895401967)
XLA Ops:
  0.6 3.0 %shard_map.190 = (bf16[8,416,128]{2,1,0:T(8,128)(2,1)}, bf16[256,128]{1,0:T(8,128)(2,1)}, bf16[96,2048]{1,0:T(8,128)(2,1)}, bf16[96,2048]{1,0:T(8,128)(2,1)}) custom-call(s32[4]{0:T(128)} %pad_add_fusion.place_ref, bf16[128,512]{1,0:T(8,128)(2,1)} %lat_ref.1, f32[1,512]{1,0:T(1,128)} %bitcast.40, bf16[32,128]{1,0:T(8,128)(2,1)} %bitcast.38, ...), custom_call_target="tpu_custom_call" | custom-call | flops 1000000000 | tf_op jit(solution)/shard_map/pallas_call | solution.py:327
  3.6 9.2 %all-to-all-start = ((bf16[8,416,128]{2,1,0:T(8,128)(2,1)}), bf16[8,416,128]{2,1,0:T(8,128)(2,1)S(1)}, u32[]{:S(2)}, u32[]{:S(2)}) async-start(bf16[8,416,128]{2,1,0:T(8,128)(2,1)} %get-tuple-element.23), calls=%async_computation | async-start | bytes 1703936 | tf_op jit(solution)/shard_map/all_to_all | solution.py:339
  14.0 1.5 collective-permute-start.1
  15.5 1.5 collective-permute-start.2
  17.6 2.8 %collective-permute-done.2.refs_3_ = bf16[256,128]{1,0:T(8,128)(2,1)S(1)} collective-permute-done((bf16[256,128]{1,0:T(8,128)(2,1)}, bf16[256,128]{1,0:T(8,128)(2,1)S(1)}, u32[]{:S(2)}, u32[]{:S(2)}) %collective-permute-start.2) | collective-permute-done | bytes 65568 | tf_op jit(solution)/shard_map/ppermute | solution.py:317
  21.3 2.6 %collective-permute-start.3 = (bf16[4,256,128]{2,1,0:T(8,128)(2,1)S(1)}, bf16[4,256,128]{2,1,0:T(8,128)(2,1)S(1)}, u32[]{:S(2)}, u32[]{:S(2)}) collective-permute-start(bf16[4,256,128]{2,1,0:T(8,128)(2,1)S(1)} %pad_maximum_fusion.1), channel_id=1, source_target_pairs={{0,4},{4,0},{1,5},{5,1},{2,6},{6,2},{3,7},{7,3},{8,12},{12,8},{9,1... | collective-permute-start | bytes 786440 | tf_op jit(solution)/shard_map/ppermute | solution.py:317
  23.9 2.7 %collective-permute-start.8 = (bf16[96,2048]{1,0:T(8,128)(2,1)S(1)}, bf16[96,2048]{1,0:T(8,128)(2,1)}, u32[]{:S(2)}, u32[]{:S(2)}) collective-permute-start(bf16[96,2048]{1,0:T(8,128)(2,1)S(1)} %copy-done.10), channel_id=1, source_target_pairs={{0,3},{1,0},{2,1},{3,2},{4,7},{5,4},{6,5},{7,6},{8,11},{9,8},{10,9... | collective-permute-start | bytes 1179656 | tf_op jit(solution)/shard_map/ppermute | solution.py:317
  26.7 11.1 %all-to-all-done.kv_ref = bf16[8,416,128]{2,1,0:T(8,128)(2,1)S(1)} async-done(((bf16[8,416,128]{2,1,0:T(8,128)(2,1)}), bf16[8,416,128]{2,1,0:T(8,128)(2,1)S(1)}, u32[]{:S(2)}, u32[]{:S(2)}) %all-to-all-start) | async-done | bytes 852000 | tf_op jit(solution)/shard_map/all_to_all | solution.py:339
  37.8 2.5 %shard_map.192 = bf16[4,4,64,128]{3,2,1,0:T(8,128)(2,1)S(1)} custom-call(s32[4]{0:T(128)S(1)} %copy-done.7, bf16[8,416,128]{2,1,0:T(8,128)(2,1)S(1)} %all-to-all-done.kv_ref, bf16[4,256,128]{2,1,0:T(8,128)(2,1)S(1)} %collective-permute-done.3.refs_0_), custom_call_target="tpu_custom_call" | custom-call | flops 2000000000 | tf_op jit(solution)/shard_map/pallas_call | solution.py:354
  42.2 1.4 collective-permute-start.7
  43.6 1.5 collective-permute-start.10
  45.1 2.5 %shard_map.191 = bf16[4,4,64,128]{3,2,1,0:T(8,128)(2,1)S(1)} custom-call(s32[4]{0:T(128)S(1)} %copy-done.7, bf16[8,416,128]{2,1,0:T(8,128)(2,1)S(1)} %all-to-all-done.kv_ref, bf16[256,128]{1,0:T(8,128)(2,1)S(1)} %copy-done.4, bf16[256,128]{1,0:T(8,128)(2,1)S(1)} %collective-permute-done.refs_1_, bf16[256,128]{1,0:T(8,128)(2,1)S(1)} %collective-permute-done.1.refs_2_, ...), custom_call_target="tpu_custom_call" | custom-call | flops 2000000000 | tf_op jit(solution)/shard_map/pallas_call | solution.py:354
  47.7 1.7 %shard_map.193 = bf16[16,64,128]{2,1,0:T(8,128)(2,1)} custom-call(bf16[16,64,128]{2,1,0:T(8,128)(2,1)S(1)} %bitcast.32, bf16[16,64,128]{2,1,0:T(8,128)(2,1)S(1)} %collective-permute-done.4.b_ref), custom_call_target="tpu_custom_call" | custom-call | flops 500000000 | tf_op jit(solution)/shard_map/pallas_call | solution.py:371
  49.4 6.5 %all-to-all-start.1 = ((bf16[16,64,128]{2,1,0:T(8,128)(2,1)}), bf16[16,64,128]{2,1,0:T(8,128)(2,1)S(1)}, u32[]{:S(2)}, u32[]{:S(2)}) async-start(bf16[16,64,128]{2,1,0:T(8,128)(2,1)} %shard_map.193), calls=%async_computation.1 | async-start | bytes 524288 | tf_op jit(solution)/shard_map/all_to_all | solution.py:374
  55.9 5.8 %collective-permute-done.10.refs_7_ = bf16[96,2048]{1,0:T(8,128)(2,1)} collective-permute-done((bf16[96,2048]{1,0:T(8,128)(2,1)}, bf16[96,2048]{1,0:T(8,128)(2,1)}, u32[]{:S(2)}, u32[]{:S(2)}) %collective-permute-start.10) | collective-permute-done | bytes 393248 | tf_op jit(solution)/shard_map/ppermute | solution.py:317
  61.7 2.2 %all-to-all-done.1 = bf16[16,64,128]{2,1,0:T(8,128)(2,1)S(1)} async-done(((bf16[16,64,128]{2,1,0:T(8,128)(2,1)}), bf16[16,64,128]{2,1,0:T(8,128)(2,1)S(1)}, u32[]{:S(2)}, u32[]{:S(2)}) %all-to-all-start.1) | async-done | bytes 262176 | tf_op jit(solution)/shard_map/all_to_all | solution.py:374
  64.6 4.6 %shard_map.194 = (bf16[64,2,2048]{2,1,0:T(2,128)(2,1)}, bf16[32,2048]{1,0:T(8,128)(2,1)}, bf16[2,32,128]{2,1,0:T(8,128)(2,1)}) custom-call(s32[4]{0:T(128)} %pad_add_fusion.place_ref, bf16[4,4,64,128]{3,2,1,0:T(8,128)(2,1)} %bitcast.33, bf16[32,2048]{1,0:T(8,128)(2,1)} %res_ref.1, f32[1,2048]{1,0:T(1,128)} %bitcast.39, s32[2,32]{1,0:T(2,128)} %bitcast.41, ...), custom_call_target="tpu_custom_call" | custom-call | flops 2000000000 | tf_op jit(solution)/shard_map/pallas_call | solution.py:378
  69.3 24.7 %all_to_all.21 = bf16[64,2,2048]{2,1,0:T(2,128)(2,1)S(1)} all-to-all(bf16[64,2,2048]{2,1,0:T(2,128)(2,1)} %get-tuple-element.29), channel_id=1, replica_groups=mesh['z'=8,'x'=4,'c'=2,'y'=4] {'z','x','c'}, dimensions={0} | all-to-all | bytes 1048576 | tf_op jit(solution)/shard_map/all_to_all | solution.py:391
  95.5 1.9 %collective-permute-start.14 = (bf16[64,2048]{1,0:T(8,128)(2,1)S(1)}, bf16[64,2048]{1,0:T(8,128)(2,1)S(1)}, u32[]{:S(2)}, u32[]{:S(2)}) collective-permute-start(bf16[64,2048]{1,0:T(8,128)(2,1)S(1)} %slice.15.refs_1_), channel_id=1, source_target_pairs={{0,3},{1,0},{2,1},{3,2},{4,7},{5,4},{6,5},{7,6},{8,11},{9,8},{10,9... | collective-permute-start | bytes 786440 | tf_op jit(solution)/shard_map/ppermute | solution.py:317
  97.4 5.8 %collective-permute-done.11.refs_2_ = bf16[64,2048]{1,0:T(8,128)(2,1)S(1)} collective-permute-done((bf16[64,2048]{1,0:T(8,128)(2,1)S(1)}, bf16[64,2048]{1,0:T(8,128)(2,1)S(1)}, u32[]{:S(2)}, u32[]{:S(2)}) %collective-permute-start.11) | collective-permute-done | bytes 262176 | tf_op jit(solution)/shard_map/ppermute | solution.py:317
  103.2 2.7 %collective-permute-start.16 = (bf16[64,2048]{1,0:T(8,128)(2,1)S(1)}, bf16[64,2048]{1,0:T(8,128)(2,1)S(1)}, u32[]{:S(2)}, u32[]{:S(2)}) collective-permute-start(bf16[64,2048]{1,0:T(8,128)(2,1)S(1)} %collective-permute-done.14.refs_5_), channel_id=1, source_target_pairs={{0,3},{1,0},{2,1},{3,2},{4,7},{5,4},{6,5},{7,6},{8,11},{9,8},{10,9... | collective-permute-start | bytes 786440 | tf_op jit(solution)/shard_map/ppermute | solution.py:317
  105.9 1.6 copy-done.1
  107.5 1.6 copy-done.2
  109.6 2.7 %collective-permute-start.13 = (bf16[64,2048]{1,0:T(8,128)(2,1)S(1)}, bf16[64,2048]{1,0:T(8,128)(2,1)S(1)}, u32[]{:S(2)}, u32[]{:S(2)}) collective-permute-start(bf16[64,2048]{1,0:T(8,128)(2,1)S(1)} %slice.13.refs_0_), channel_id=1, source_target_pairs={{0,3},{1,0},{2,1},{3,2},{4,7},{5,4},{6,5},{7,6},{8,11},{9,8},{10,9... | collective-permute-start | bytes 786440 | tf_op jit(solution)/shard_map/ppermute | solution.py:317
  113.7 3.2 %collective-permute-done.12.refs_3_ = bf16[64,2048]{1,0:T(8,128)(2,1)S(1)} collective-permute-done((bf16[64,2048]{1,0:T(8,128)(2,1)S(1)}, bf16[64,2048]{1,0:T(8,128)(2,1)S(1)}, u32[]{:S(2)}, u32[]{:S(2)}) %collective-permute-start.12) | collective-permute-done | bytes 262176 | tf_op jit(solution)/shard_map/ppermute | solution.py:317
  116.9 2.7 %shard_map.196 = (bf16[64,2048]{1,0:T(8,128)(2,1)S(1)}, bf16[64,2048]{1,0:T(8,128)(2,1)S(1)}, bf16[64,2048]{1,0:T(8,128)(2,1)S(1)}, bf16[64,2048]{1,0:T(8,128)(2...) custom-call(bf16[64,2048]{1,0:T(8,128)(2,1)S(1)} %slice.13.refs_0_, ...), custom_call_target="tpu_custom_call" | custom-call | flops 3000000000 | tf_op jit(solution)/shard_map/pallas_call | solution.py:406
  119.6 2.5 %collective-permute-start.19 = (bf16[64,2048]{1,0:T(8,128)(2,1)S(1)}, bf16[64,2048]{1,0:T(8,128)(2,1)S(1)}, u32[]{:S(2)}, u32[]{:S(2)}) collective-permute-start(bf16[64,2048]{1,0:T(8,128)(2,1)S(1)} %get-tuple-element.36), channel_id=1, source_target_pairs={{0,3},{1,0},{2,1},{3,2},{4,7},{5,4},{6,5},{7,6},{8,11},{9,8},{10,9... | collective-permute-start | bytes 786440 | tf_op jit(solution)/shard_map/ppermute | solution.py:317
  122.0 2.7 %collective-permute-start.21 = (bf16[64,2048]{1,0:T(8,128)(2,1)S(1)}, bf16[64,2048]{1,0:T(8,128)(2,1)S(1)}, u32[]{:S(2)}, u32[]{:S(2)}) collective-permute-start(bf16[64,2048]{1,0:T(8,128)(2,1)S(1)} %get-tuple-element.40), channel_id=1, source_target_pairs={{0,3},{1,0},{2,1},{3,2},{4,7},{5,4},{6,5},{7,6},{8,11},{9,8},{10,9... | collective-permute-start | bytes 786440 | tf_op jit(solution)/shard_map/ppermute | solution.py:317
  124.9 5.5 %collective-permute-done.21 = bf16[64,2048]{1,0:T(8,128)(2,1)S(1)} collective-permute-done((bf16[64,2048]{1,0:T(8,128)(2,1)S(1)}, bf16[64,2048]{1,0:T(8,128)(2,1)S(1)}, u32[]{:S(2)}, u32[]{:S(2)}) %collective-permute-start.21) | collective-permute-done | bytes 262176 | tf_op jit(solution)/shard_map/ppermute | solution.py:317
  130.5 3.5 %collective-permute-start.22 = (bf16[64,2048]{1,0:T(8,128)(2,1)S(1)}, bf16[64,2048]{1,0:T(8,128)(2,1)S(1)}, u32[]{:S(2)}, u32[]{:S(2)}) collective-permute-start(bf16[64,2048]{1,0:T(8,128)(2,1)S(1)} %add_convert_fusion.1), channel_id=1, source_target_pairs={{0,3},{1,0},{2,1},{3,2},{4,7},{5,4},{6,5},{7,6},{8,11},{9,8},{10,9... | collective-permute-start | bytes 786440 | tf_op jit(solution)/shard_map/ppermute | solution.py:317
  134.1 3.2 %collective-permute-done.22 = bf16[64,2048]{1,0:T(8,128)(2,1)S(1)} collective-permute-done((bf16[64,2048]{1,0:T(8,128)(2,1)S(1)}, bf16[64,2048]{1,0:T(8,128)(2,1)S(1)}, u32[]{:S(2)}, u32[]{:S(2)}) %collective-permute-start.22) | collective-permute-done | bytes 262176 | tf_op jit(solution)/shard_map/ppermute | solution.py:317
  137.8 27.2 %all_to_all.22 = bf16[64,2,2048]{2,1,0:T(2,128)(2,1)S(1)} all-to-all(bf16[64,2,2048]{2,1,0:T(2,128)(2,1)S(1)} %convert_element_type.53), channel_id=1, replica_groups=mesh['z'=8,'x'=4,'c'=2,'y'=4] {'z','x','c'}, dimensions={0} | all-to-all | bytes 1048576 | tf_op jit(solution)/shard_map/all_to_all | solution.py:438
  (63 shorter events, 11.3 us)
Async XLA Ops:
  0.6 37.2 %copy-start.7 = (s32[4]{0:T(128)S(1)}, s32[4]{0:T(128)}, u32[]{:S(2)}) copy-start(s32[4]{0:T(128)} %pad_add_fusion.place_ref) | copy-start | bytes 52
  3.6 20.3 %copy-start.10 = (bf16[96,2048]{1,0:T(8,128)(2,1)S(1)}, bf16[96,2048]{1,0:T(8,128)(2,1)}, u32[]{:S(2)}) copy-start(bf16[96,2048]{1,0:T(8,128)(2,1)} %get-tuple-element.26.refs_1_) | copy-start | bytes 1179652
  3.6 23.0 %copy-start.9 = (bf16[96,2048]{1,0:T(8,128)(2,1)S(1)}, bf16[96,2048]{1,0:T(8,128)(2,1)}, u32[]{:S(2)}) copy-start(bf16[96,2048]{1,0:T(8,128)(2,1)} %get-tuple-element.25.refs_0_) | copy-start | bytes 1179652
  3.6 34.1 %all-to-all-start = ((bf16[8,416,128]{2,1,0:T(8,128)(2,1)}), bf16[8,416,128]{2,1,0:T(8,128)(2,1)S(1)}, u32[]{:S(2)}, u32[]{:S(2)}) async-start(bf16[8,416,128]{2,1,0:T(8,128)(2,1)} %get-tuple-element.23), calls=%async_computation | async-start | bytes 1703936 | tf_op jit(solution)/shard_map/all_to_all | solution.py:339
  12.8 4.5 %collective-permute-start = (bf16[256,128]{1,0:T(8,128)(2,1)}, bf16[256,128]{1,0:T(8,128)(2,1)S(1)}, u32[]{:S(2)}, u32[]{:S(2)}) collective-permute-start(bf16[256,128]{1,0:T(8,128)(2,1)} %get-tuple-element.24.refs_0_), channel_id=1, source_target_pairs={{0,8},{8,16},{16,24},{24,0},{1,9},{9,17},{17,25},{25,1},{2,10},{10... | collective-permute-start | bytes 196616 | tf_op jit(solution)/shard_map/ppermute | solution.py:317
  14.0 3.6 %collective-permute-start.1 = (bf16[256,128]{1,0:T(8,128)(2,1)}, bf16[256,128]{1,0:T(8,128)(2,1)S(1)}, u32[]{:S(2)}, u32[]{:S(2)}) collective-permute-start(bf16[256,128]{1,0:T(8,128)(2,1)} %get-tuple-element.24.refs_0_), channel_id=1, source_target_pairs={{0,24},{8,0},{16,8},{24,16},{1,25},{9,1},{17,9},{25,17},{2,26},{10... | collective-permute-start | bytes 196616 | tf_op jit(solution)/shard_map/ppermute | solution.py:317
  15.5 5.0 %collective-permute-start.2 = (bf16[256,128]{1,0:T(8,128)(2,1)}, bf16[256,128]{1,0:T(8,128)(2,1)S(1)}, u32[]{:S(2)}, u32[]{:S(2)}) collective-permute-start(bf16[256,128]{1,0:T(8,128)(2,1)} %get-tuple-element.24.refs_0_), channel_id=1, source_target_pairs={{0,16},{8,24},{16,0},{24,8},{1,17},{9,25},{17,1},{25,9},{2,18},{10... | collective-permute-start | bytes 196616 | tf_op jit(solution)/shard_map/ppermute | solution.py:317
  21.3 5.4 %collective-permute-start.3 = (bf16[4,256,128]{2,1,0:T(8,128)(2,1)S(1)}, bf16[4,256,128]{2,1,0:T(8,128)(2,1)S(1)}, u32[]{:S(2)}, u32[]{:S(2)}) collective-permute-start(bf16[4,256,128]{2,1,0:T(8,128)(2,1)S(1)} %pad_maximum_fusion.1), channel_id=1, source_target_pairs={{0,4},{4,0},{1,5},{5,1},{2,6},{6,2},{3,7},{7,3},{8,12},{12,8},{9,1... | collective-permute-start | bytes 786440 | tf_op jit(solution)/shard_map/ppermute | solution.py:317
  23.9 19.7 %collective-permute-start.8 = (bf16[96,2048]{1,0:T(8,128)(2,1)S(1)}, bf16[96,2048]{1,0:T(8,128)(2,1)}, u32[]{:S(2)}, u32[]{:S(2)}) collective-permute-start(bf16[96,2048]{1,0:T(8,128)(2,1)S(1)} %copy-done.10), channel_id=1, source_target_pairs={{0,3},{1,0},{2,1},{3,2},{4,7},{5,4},{6,5},{7,6},{8,11},{9,8},{10,9... | collective-permute-start | bytes 1179656 | tf_op jit(solution)/shard_map/ppermute | solution.py:317
  26.7 18.4 %collective-permute-start.5 = (bf16[96,2048]{1,0:T(8,128)(2,1)S(1)}, bf16[96,2048]{1,0:T(8,128)(2,1)}, u32[]{:S(2)}, u32[]{:S(2)}) collective-permute-start(bf16[96,2048]{1,0:T(8,128)(2,1)S(1)} %copy-done.9), channel_id=1, source_target_pairs={{0,1},{1,2},{2,3},{3,0},{4,5},{5,6},{6,7},{7,4},{8,9},{9,10},{10,1... | collective-permute-start | bytes 1179656 | tf_op jit(solution)/shard_map/ppermute | solution.py:317
  40.3 7.3 %collective-permute-start.4 = (bf16[16,64,128]{2,1,0:T(8,128)(2,1)S(1)}, bf16[16,64,128]{2,1,0:T(8,128)(2,1)S(1)}, u32[]{:S(2)}, u32[]{:S(2)}) collective-permute-start(bf16[16,64,128]{2,1,0:T(8,128)(2,1)S(1)} %bitcast.31), channel_id=1, source_target_pairs={{0,4},{4,0},{1,5},{5,1},{2,6},{6,2},{3,7},{7,3},{8,12},{12,8},{9,1... | collective-permute-start | bytes 786440 | tf_op jit(solution)/shard_map/ppermute | solution.py:317
  40.9 15.0 %collective-permute-start.6 = (bf16[96,2048]{1,0:T(8,128)(2,1)S(1)}, bf16[96,2048]{1,0:T(8,128)(2,1)}, u32[]{:S(2)}, u32[]{:S(2)}) collective-permute-start(bf16[96,2048]{1,0:T(8,128)(2,1)S(1)} %copy-done.10), channel_id=1, source_target_pairs={{0,1},{1,2},{2,3},{3,0},{4,5},{5,6},{6,7},{7,4},{8,9},{9,10},{10,1... | collective-permute-start | bytes 1179656 | tf_op jit(solution)/shard_map/ppermute | solution.py:317
  42.2 13.7 %collective-permute-start.7 = (bf16[96,2048]{1,0:T(8,128)(2,1)S(1)}, bf16[96,2048]{1,0:T(8,128)(2,1)}, u32[]{:S(2)}, u32[]{:S(2)}) collective-permute-start(bf16[96,2048]{1,0:T(8,128)(2,1)S(1)} %copy-done.9), channel_id=1, source_target_pairs={{0,3},{1,0},{2,1},{3,2},{4,7},{5,4},{6,5},{7,6},{8,11},{9,8},{10,9... | collective-permute-start | bytes 1179656 | tf_op jit(solution)/shard_map/ppermute | solution.py:317
  43.6 18.1 %collective-permute-start.10 = (bf16[96,2048]{1,0:T(8,128)(2,1)}, bf16[96,2048]{1,0:T(8,128)(2,1)}, u32[]{:S(2)}, u32[]{:S(2)}) collective-permute-start(bf16[96,2048]{1,0:T(8,128)(2,1)} %collective-permute-done.8.refs_5_), channel_id=1, source_target_pairs={{0,3},{1,0},{2,1},{3,2},{4,7},{5,4},{6,5},{7,6},{8,11},{9,8},{10,9... | collective-permute-start | bytes 1179656 | tf_op jit(solution)/shard_map/ppermute | solution.py:317
  45.1 16.6 %collective-permute-start.9 = (bf16[96,2048]{1,0:T(8,128)(2,1)}, bf16[96,2048]{1,0:T(8,128)(2,1)}, u32[]{:S(2)}, u32[]{:S(2)}) collective-permute-start(bf16[96,2048]{1,0:T(8,128)(2,1)} %collective-permute-done.5.refs_2_), channel_id=1, source_target_pairs={{0,1},{1,2},{2,3},{3,0},{4,5},{5,6},{6,7},{7,4},{8,9},{9,10},{10,1... | collective-permute-start | bytes 1179656 | tf_op jit(solution)/shard_map/ppermute | solution.py:317
  49.4 14.6 %all-to-all-start.1 = ((bf16[16,64,128]{2,1,0:T(8,128)(2,1)}), bf16[16,64,128]{2,1,0:T(8,128)(2,1)S(1)}, u32[]{:S(2)}, u32[]{:S(2)}) async-start(bf16[16,64,128]{2,1,0:T(8,128)(2,1)} %shard_map.193), calls=%async_computation.1 | async-start | bytes 524288 | tf_op jit(solution)/shard_map/all_to_all | solution.py:374
  69.2 36.6 %copy-start = (bf16[1,2048,512]{2,1,0:T(8,128)(2,1)S(1)}, bf16[1,2048,512]{2,1,0:T(8,128)(2,1)}, u32[]{:S(2)}) copy-start(bf16[1,2048,512]{2,1,0:T(8,128)(2,1)} %param.33) | copy-start | bytes 6291460
  94.4 8.8 %collective-permute-start.11 = (bf16[64,2048]{1,0:T(8,128)(2,1)S(1)}, bf16[64,2048]{1,0:T(8,128)(2,1)S(1)}, u32[]{:S(2)}, u32[]{:S(2)}) collective-permute-start(bf16[64,2048]{1,0:T(8,128)(2,1)S(1)} %slice.13.refs_0_), channel_id=1, source_target_pairs={{0,1},{1,2},{2,3},{3,0},{4,5},{5,6},{6,7},{7,4},{8,9},{9,10},{10,1... | collective-permute-start | bytes 786440 | tf_op jit(solution)/shard_map/ppermute | solution.py:317
  95.5 7.7 %collective-permute-start.14 = (bf16[64,2048]{1,0:T(8,128)(2,1)S(1)}, bf16[64,2048]{1,0:T(8,128)(2,1)S(1)}, u32[]{:S(2)}, u32[]{:S(2)}) collective-permute-start(bf16[64,2048]{1,0:T(8,128)(2,1)S(1)} %slice.15.refs_1_), channel_id=1, source_target_pairs={{0,3},{1,0},{2,1},{3,2},{4,7},{5,4},{6,5},{7,6},{8,11},{9,8},{10,9... | collective-permute-start | bytes 786440 | tf_op jit(solution)/shard_map/ppermute | solution.py:317
  103.2 9.1 %collective-permute-start.15 = (bf16[64,2048]{1,0:T(8,128)(2,1)S(1)}, bf16[64,2048]{1,0:T(8,128)(2,1)S(1)}, u32[]{:S(2)}, u32[]{:S(2)}) collective-permute-start(bf16[64,2048]{1,0:T(8,128)(2,1)S(1)} %collective-permute-done.11.refs_2_), channel_id=1, source_target_pairs={{0,1},{1,2},{2,3},{3,0},{4,5},{5,6},{6,7},{7,4},{8,9},{9,10},{10,1... | collective-permute-start | bytes 786440 | tf_op jit(solution)/shard_map/ppermute | solution.py:317
  103.2 9.1 %collective-permute-start.16 = (bf16[64,2048]{1,0:T(8,128)(2,1)S(1)}, bf16[64,2048]{1,0:T(8,128)(2,1)S(1)}, u32[]{:S(2)}, u32[]{:S(2)}) collective-permute-start(bf16[64,2048]{1,0:T(8,128)(2,1)S(1)} %collective-permute-done.14.refs_5_), channel_id=1, source_target_pairs={{0,3},{1,0},{2,1},{3,2},{4,7},{5,4},{6,5},{7,6},{8,11},{9,8},{10,9... | collective-permute-start | bytes 786440 | tf_op jit(solution)/shard_map/ppermute | solution.py:317
  109.5 7.3 %collective-permute-start.12 = (bf16[64,2048]{1,0:T(8,128)(2,1)S(1)}, bf16[64,2048]{1,0:T(8,128)(2,1)S(1)}, u32[]{:S(2)}, u32[]{:S(2)}) collective-permute-start(bf16[64,2048]{1,0:T(8,128)(2,1)S(1)} %slice.15.refs_1_), channel_id=1, source_target_pairs={{0,1},{1,2},{2,3},{3,0},{4,5},{5,6},{6,7},{7,4},{8,9},{9,10},{10,1... | collective-permute-start | bytes 786440 | tf_op jit(solution)/shard_map/ppermute | solution.py:317
  109.6 7.3 %collective-permute-start.13 = (bf16[64,2048]{1,0:T(8,128)(2,1)S(1)}, bf16[64,2048]{1,0:T(8,128)(2,1)S(1)}, u32[]{:S(2)}, u32[]{:S(2)}) collective-permute-start(bf16[64,2048]{1,0:T(8,128)(2,1)S(1)} %slice.13.refs_0_), channel_id=1, source_target_pairs={{0,3},{1,0},{2,1},{3,2},{4,7},{5,4},{6,5},{7,6},{8,11},{9,8},{10,9... | collective-permute-start | bytes 786440 | tf_op jit(solution)/shard_map/ppermute | solution.py:317
  113.4 11.3 %collective-permute-start.17 = (bf16[64,2048]{1,0:T(8,128)(2,1)S(1)}, bf16[64,2048]{1,0:T(8,128)(2,1)S(1)}, u32[]{:S(2)}, u32[]{:S(2)}) collective-permute-start(bf16[64,2048]{1,0:T(8,128)(2,1)S(1)} %get-tuple-element.35), channel_id=1, source_target_pairs={{0,1},{1,2},{2,3},{3,0},{4,5},{5,6},{6,7},{7,4},{8,9},{9,10},{10,1... | collective-permute-start | bytes 786440 | tf_op jit(solution)/shard_map/ppermute | solution.py:317
  119.6 14.4 %collective-permute-start.19 = (bf16[64,2048]{1,0:T(8,128)(2,1)S(1)}, bf16[64,2048]{1,0:T(8,128)(2,1)S(1)}, u32[]{:S(2)}, u32[]{:S(2)}) collective-permute-start(bf16[64,2048]{1,0:T(8,128)(2,1)S(1)} %get-tuple-element.36), channel_id=1, source_target_pairs={{0,3},{1,0},{2,1},{3,2},{4,7},{5,4},{6,5},{7,6},{8,11},{9,8},{10,9... | collective-permute-start | bytes 786440 | tf_op jit(solution)/shard_map/ppermute | solution.py:317
  122.0 12.0 %collective-permute-start.20 = (bf16[64,2048]{1,0:T(8,128)(2,1)S(1)}, bf16[64,2048]{1,0:T(8,128)(2,1)S(1)}, u32[]{:S(2)}, u32[]{:S(2)}) collective-permute-start(bf16[64,2048]{1,0:T(8,128)(2,1)S(1)} %get-tuple-element.38), channel_id=1, source_target_pairs={{0,1},{1,2},{2,3},{3,0},{4,5},{5,6},{6,7},{7,4},{8,9},{9,10},{10,1... | collective-permute-start | bytes 786440 | tf_op jit(solution)/shard_map/ppermute | solution.py:317
  122.0 8.3 %collective-permute-start.21 = (bf16[64,2048]{1,0:T(8,128)(2,1)S(1)}, bf16[64,2048]{1,0:T(8,128)(2,1)S(1)}, u32[]{:S(2)}, u32[]{:S(2)}) collective-permute-start(bf16[64,2048]{1,0:T(8,128)(2,1)S(1)} %get-tuple-element.40), channel_id=1, source_target_pairs={{0,3},{1,0},{2,1},{3,2},{4,7},{5,4},{6,5},{7,6},{8,11},{9,8},{10,9... | collective-permute-start | bytes 786440 | tf_op jit(solution)/shard_map/ppermute | solution.py:317
  124.8 9.2 %collective-permute-start.18 = (bf16[64,2048]{1,0:T(8,128)(2,1)S(1)}, bf16[64,2048]{1,0:T(8,128)(2,1)S(1)}, u32[]{:S(2)}, u32[]{:S(2)}) collective-permute-start(bf16[64,2048]{1,0:T(8,128)(2,1)S(1)} %add_convert_fusion.3), channel_id=1, source_target_pairs={{0,1},{1,2},{2,3},{3,0},{4,5},{5,6},{6,7},{7,4},{8,9},{9,10},{10,1... | collective-permute-start | bytes 786440 | tf_op jit(solution)/shard_map/ppermute | solution.py:317
  130.5 6.8 %collective-permute-start.22 = (bf16[64,2048]{1,0:T(8,128)(2,1)S(1)}, bf16[64,2048]{1,0:T(8,128)(2,1)S(1)}, u32[]{:S(2)}, u32[]{:S(2)}) collective-permute-start(bf16[64,2048]{1,0:T(8,128)(2,1)S(1)} %add_convert_fusion.1), channel_id=1, source_target_pairs={{0,3},{1,0},{2,1},{3,2},{4,7},{5,4},{6,5},{7,6},{8,11},{9,8},{10,9... | collective-permute-start | bytes 786440 | tf_op jit(solution)/shard_map/ppermute | solution.py:317
  137.4 27.8 %copy-start.3 = (bf16[32,2048]{1,0:T(8,128)(2,1)S(1)}, bf16[32,2048]{1,0:T(8,128)(2,1)}, u32[]{:S(2)}) copy-start(bf16[32,2048]{1,0:T(8,128)(2,1)} %get-tuple-element.27.mid_ref) | copy-start | bytes 393220
  137.4 27.8 %copy-start.5 = (bf16[2,32,128]{2,1,0:T(8,128)(2,1)S(1)}, bf16[2,32,128]{2,1,0:T(8,128)(2,1)}, u32[]{:S(2)}) copy-start(bf16[2,32,128]{2,1,0:T(8,128)(2,1)} %get-tuple-element.28.pick_ref) | copy-start | bytes 49156
  137.4 27.8 %copy-start.6 = (f32[32,2]{0,1:T(2,128)S(1)}, f32[32,2]{0,1:T(2,128)}, u32[]{:S(2)}) copy-start(f32[32,2]{0,1:T(2,128)} %param.37) | copy-start | bytes 772
  (4 other events, 22.3 us)

commit v4 on v3

--- a/solution.py
+++ b/solution.py
@@ -50,10 +50,6 @@
     return [pl.BlockSpec(memory_space=pltpu.VMEM) for _ in range(n)]
 
 
-def smem():
-    return pl.BlockSpec(memory_space=pltpu.SMEM)
-
-
 def column(row):
     n = row.shape[1]
     same = lax.broadcasted_iota(jnp.int32, (n, n), 0) == lax.broadcasted_iota(
@@ -63,10 +59,10 @@
 
 
 def pre_kernel(
-    place_ref, lat_ref, gain_ref, rk_ref, qs_ref, ql_ref, ks_w, vs_w, kl_w, vl_w,
-    base_ref, row_ref, lo_ref, so_ref, kv_ref, q_ref, top_ref, low_ref,
+    lat_ref, gain_ref, rk_ref, qs_ref, ql_ref, ks_w, vs_w, kl_w, vl_w,
+    base_ref, row_ref, kv_ref, q_ref,
 ):
-    block = (place_ref[0] * NX + place_ref[1]) * NC + place_ref[2]
+    block = (lax.axis_index("z") * NX + lax.axis_index("x")) * NC + lax.axis_index("c")
     base = column(base_ref[pl.ds(block, 1), :])
     cb, sb = base[:ROPE], base[ROPE:]
     cr, sr = row_ref[:ROPE], row_ref[ROPE:]
@@ -102,14 +98,11 @@
         axis=0,
     )
     q_ref[128:256, :] = mixed.T.astype(bf16)
-    top_ref[...] = lo_ref[0:96, :]
-    low_ref[0:32, :] = lo_ref[96:128, :]
-    low_ref[32:96, :] = so_ref[...]
-
-
-def attn_kernel(other, place_ref, kv_ref, *refs):
+
+
+def attn_kernel(other, kv_ref, *refs):
     queries, (out_ref, kl, ks, vl, vs) = refs[:-5], refs[-5:]
-    z, x, c = place_ref[0], place_ref[1], place_ref[2]
+    z, x, c = (lax.axis_index(a) for a in ("z", "x", "c"))
     kl[128:192, :] = jnp.zeros((64, 1024), bf16)
     kl[224:256, :] = jnp.zeros((32, 1024), bf16)
     ks[64:96, :] = jnp.zeros((32, 1024), bf16)
@@ -193,17 +186,24 @@
     out_ref[:, TOK:] = outs[1].astype(bf16).reshape(NX * NY, TOK, 128)
 
 
-def mid_kernel(
-    place_ref, parts_ref, res_ref, gain_ref, routing_ref, *refs
-):
-    sources, (disp_ref, mid_ref, pick_ref, w_ref, sems) = refs[:8], refs[8:]
+def gather_kernel(*refs):
+    sources, (out_ref, sems) = refs[:8], refs[8:]
     copies = [
-        pltpu.make_async_copy(src, w_ref.at[i // 2, pl.ds(96 * (i % 2), 96)], sems.at[i])
+        pltpu.make_async_copy(
+            src, out_ref.at[i // 2, pl.ds(128 * (i % 2), 128 - 64 * (i % 2))], sems.at[i]
+        )
         for i, src in enumerate(sources)
     ]
     for copy in copies:
         copy.start()
-    y = place_ref[3]
+    for copy in copies:
+        copy.wait()
+
+
+def mid_kernel(
+    parts_ref, res_ref, gain_ref, routing_ref, w_ref, disp_ref, mid_ref, pick_ref
+):
+    y = lax.axis_index("y")
     total = jnp.zeros((TOK, D), f32)
     for n, shift in enumerate((0, 1, 3, 2)):
         ya = lax.rem(y + (NY - shift), NY)
@@ -223,8 +223,6 @@
         large = mixed(larges, 0, SCALE_L).astype(bf16)
         small = mixed(smalls, 3, SCALE_S)[:, 64:128].astype(bf16)
         heads = jnp.concatenate([large, small], axis=1)
-        copies[2 * n].wait()
-        copies[2 * n + 1].wait()
         partial = jnp.dot(heads, w_ref[n], preferred_element_type=f32)
         total = total + partial.astype(bf16).astype(f32)
     attention = total.astype(bf16).astype(f32)
@@ -322,18 +320,16 @@
     small_keys, small_values, large_keys, large_values, small_output, large_output,
     ffn_gain, gate_weights, up_weights, down_weights, routing, route_weight,
 ):
-    place = jnp.stack([lax.axis_index(a) for a in ("z", "x", "c", "y")]).astype(jnp.int32)
     base, row = rope_parts()
-    kv, q, top, low = call(
+    kv, q = call(
         pre_kernel,
-        [smem()] + vmem(13),
-        [((NZ, 416, 128), bf16), ((256, 128), bf16), ((96, D), bf16), ((96, D), bf16)],
+        vmem(11),
+        [((NZ, 416, 128), bf16), ((256, 128), bf16)],
         flops=10**9,
         mib=63,
     )(
-        place, latent, latent_gain[None, :], rotary_key.T, query_small.T, query_large.T,
+        latent, latent_gain[None, :], rotary_key.T, query_small.T, query_large.T,
         small_keys.T, small_values.T, large_keys, large_values, base, row,
-        large_output, small_output,
     )
 
     kvs = lax.all_to_all(kv, "z", 0, 0, tiled=True)
@@ -343,6 +339,7 @@
         qx.append(shifted(q, "x", NX, by))
     qc = shifted(jnp.stack(qx), "c", NC, 1)
 
+    top, low = large_output, small_output
     top_p = shifted(top, "y", NY, 1)
     low_m = shifted(low, "y", NY, -1)
     low_p = shifted(low, "y", NY, 1)
@@ -353,7 +350,7 @@
     def attend(other, *queries):
         return call(
             functools.partial(attn_kernel, other),
-            [smem()] + vmem(1 + len(queries)),
+            vmem(1 + len(queries)),
             [((NX, NY, 2 * TOK, 128), bf16)],
             scratch=[
                 pltpu.VMEM((256, 1024), bf16),
@@ -363,7 +360,7 @@
             ],
             flops=2 * 10**9,
             mib=20,
-        )(place, kvs, *queries).reshape(NX * NY, 2 * TOK, 128)
+        )(kvs, *queries).reshape(NX * NY, 2 * TOK, 128)
 
     theirs = attend(True, qc)
     theirs = shifted(theirs, "c", NC, 1)
@@ -374,18 +371,21 @@
     parts = lax.all_to_all(
         parts.reshape(NX * NY * 2 * TOK, 128), ("x", "y"), 0, 0, tiled=True
     ).reshape(NX, NY, 2 * TOK, 128)
+    projection = call(
+        gather_kernel,
+        [pl.BlockSpec(memory_space=pltpu.HBM) for _ in range(8)],
+        [((NY, 192, D), bf16)],
+        scratch=[pltpu.SemaphoreType.DMA((8,))],
+        flops=10**9,
+        mib=8,
+    )(top, low, top_p, low_p, top_m, low_m, top_o, low_o)
 
     disp, middle, pick = call(
         mid_kernel,
-        [smem()] + vmem(4) + [pl.BlockSpec(memory_space=pltpu.HBM) for _ in range(8)],
+        vmem(5),
         [((EXPERTS, CAP, D), bf16), ((TOK, D), bf16), ((2, TOK, SLOTS), bf16)],
-        scratch=[pltpu.VMEM((NY, 192, D), bf16), pltpu.SemaphoreType.DMA((8,))],
         flops=2 * 10**9,
-        mib=63,
-    )(
-        place, parts, residual, ffn_gain[None, :], routing.T,
-        top, low, top_p, low_p, top_m, low_m, top_o, low_o,
-    )
+    )(parts, residual, ffn_gain[None, :], routing.T, projection)
 
     sp = ("z", "x", "c")
     mine = lax.all_to_all(disp, sp, 0, 0, tiled=True)

time: 167 us -> 166 us (level)
  waiting for transfers between devices: 40.3 us -> 31 us
  local copies, waits for them, and re-layouts: 5.02 us -> 11.8 us
  blocking collectives: 51.9 us -> 56.6 us
  Pallas kernels: 19.6 us -> 17.2 us
    unnamed x22 -> x38, local copies, waits for them, and re-layouts: 3.92 us -> 10.7 us
    ppermute x23, waiting for transfers between devices: 27 us -> 21.8 us  [shifted(): return lax.ppermute(a, axis, [(i, (i + by) % size) for i in range(size)])]
    all_to_all x1, blocking collectives: 24.7 us -> 29.4 us  [layer(): mine = lax.all_to_all(disp, sp, 0, 0, tiled=True)]
    pallas_call x4 -> x5, Pallas kernels: 12.7 us -> 10.3 us  [the longest x2 3.98 us: attend(): call(functools.partial(attn_kernel, other), vmem(1 + len(queries)), [((NX...]
    all_to_all x1, waiting for transfers between devices: 11.1 us -> 8.98 us  [layer(): kvs = lax.all_to_all(kv, 'z', 0, 0, tiled=True)]
    ppermute x23, starting transfers between devices: 31.6 us -> 33.6 us  [shifted(): return lax.ppermute(a, axis, [(i, (i + by) % size) for i in range(size)])]
    all_to_all x1, waiting for transfers between devices: 2.2 us -> 0.28 us  [layer(): lax.all_to_all(parts.reshape(NX * NY * 2 * TOK, 128), ('x', 'y'), 0, 0, t...]
    all_to_all x1, starting transfers between devices: 6.52 us -> 4.73 us  [layer(): lax.all_to_all(parts.reshape(NX * NY * 2 * TOK, 128), ('x', 'y'), 0, 0, t...]
  transfers between devices with their start and end apart: 25 -> 25, of which waited for: 10 -> 8; matrix products, arithmetic and copies ran while one was open for 1% -> 1% of each run, Pallas kernels for 7% -> 7%
where the time goes in v4:
time: 166 us; the launch traced here: 165 us
  blocking collectives  56.6 us (34%)
  starting transfers between devices  47.4 us (29%)
  waiting for transfers between devices  31 us (19%)
  Pallas kernels  17.2 us (10%)
  local copies, waits for them, and re-layouts  11.8 us (7%)
    ppermute x23, starting transfers between devices, shifted(): return lax.ppermute(a, axis, [(i, (i + by) % size) for i in range(size)])  33.6 us
    all_to_all x1, blocking collectives, layer(): mine = lax.all_to_all(disp, sp, 0, 0, tiled=True)  29.4 us
    all_to_all x1, blocking collectives, layer(): ret = lax.all_to_all(done.reshape(EXPERTS, CAP, D), sp, 0, 0, tiled=True)  27.2 us
    ppermute x23, waiting for transfers between devices, shifted(): return lax.ppermute(a, axis, [(i, (i + by) % size) for i in range(size)])  21.8 us
    unnamed x38, local copies, waits for them, and re-layouts  10.7 us
    all_to_all x1, starting transfers between devices, layer(): kvs = lax.all_to_all(kv, 'z', 0, 0, tiled=True)  9 us
    all_to_all x1, waiting for transfers between devices, layer(): kvs = lax.all_to_all(kv, 'z', 0, 0, tiled=True)  8.98 us
    all_to_all x1, starting transfers between devices, layer(): lax.all_to_all(parts.reshape(NX * NY * 2 * TOK, 128), ('x', 'y'), 0, 0, t...  4.73 us
  transfers between devices with their start and end apart: 25, of which 8 were waited for; matrix products, arithmetic and copies ran while one was open for 1% of the time, Pallas kernels for 7%

profile of v4, /device:TPU:1, one launch (start us, length us, event | category | flops | bytes accessed | tf_op | source)
XLA Modules:
  0.0 165.4 jit_solution(1044761543658066837)
XLA Ops:
  0.0 2.6 %shard_map.190 = (bf16[8,416,128]{2,1,0:T(8,128)(2,1)}, bf16[256,128]{1,0:T(8,128)(2,1)}) custom-call(bf16[128,512]{1,0:T(8,128)(2,1)} %lat_ref.1, f32[1,512]{1,0:T(1,128)} %bitcast.36, bf16[32,128]{1,0:T(8,128)(2,1)} %bitcast.35, bf16[96,128]{1,0:T(8,128)(2,1)} %bitcast.34, bf16[160,128]{1,0:T(8,128)(2,1)} %bitcast.33, bf16[64,512]{1,0:T(8,128)(2,1)} %bitcast.31, ...), custom_call_target="tpu_custom_call" | custom-call | flops 1000000000 | tf_op jit(solution)/shard_map/pallas_call | solution.py:324
  2.6 9.0 %all-to-all-start = ((bf16[8,416,128]{2,1,0:T(8,128)(2,1)}), bf16[8,416,128]{2,1,0:T(8,128)(2,1)S(1)}, u32[]{:S(2)}, u32[]{:S(2)}) async-start(bf16[8,416,128]{2,1,0:T(8,128)(2,1)} %get-tuple-element.21), calls=%async_computation | async-start | bytes 1703936 | tf_op jit(solution)/shard_map/all_to_all | solution.py:335
  11.6 1.4 collective-permute-start.5
  12.9 2.7 %collective-permute-start.2 = (bf16[256,128]{1,0:T(8,128)(2,1)}, bf16[256,128]{1,0:T(8,128)(2,1)S(1)}, u32[]{:S(2)}, u32[]{:S(2)}) collective-permute-start(bf16[256,128]{1,0:T(8,128)(2,1)} %get-tuple-element.22.refs_0_), channel_id=1, source_target_pairs={{0,16},{8,24},{16,0},{24,8},{1,17},{9,25},{17,1},{25,9},{2,18},{10... | collective-permute-start | bytes 196616 | tf_op jit(solution)/shard_map/ppermute | solution.py:315
  16.0 2.4 %collective-permute-start.1 = (bf16[256,128]{1,0:T(8,128)(2,1)}, bf16[256,128]{1,0:T(8,128)(2,1)S(1)}, u32[]{:S(2)}, u32[]{:S(2)}) collective-permute-start(bf16[256,128]{1,0:T(8,128)(2,1)} %get-tuple-element.22.refs_0_), channel_id=1, source_target_pairs={{0,24},{8,0},{16,8},{24,16},{1,25},{9,1},{17,9},{25,17},{2,26},{10... | collective-permute-start | bytes 196616 | tf_op jit(solution)/shard_map/ppermute | solution.py:315
  18.4 2.4 %collective-permute-done.refs_1_ = bf16[256,128]{1,0:T(8,128)(2,1)S(1)} collective-permute-done((bf16[256,128]{1,0:T(8,128)(2,1)}, bf16[256,128]{1,0:T(8,128)(2,1)S(1)}, u32[]{:S(2)}, u32[]{:S(2)}) %collective-permute-start) | collective-permute-done | bytes 65568 | tf_op jit(solution)/shard_map/ppermute | solution.py:315
  21.7 2.2 %collective-permute-start.3 = (bf16[4,256,128]{2,1,0:T(8,128)(2,1)S(1)}, bf16[4,256,128]{2,1,0:T(8,128)(2,1)S(1)}, u32[]{:S(2)}, u32[]{:S(2)}) collective-permute-start(bf16[4,256,128]{2,1,0:T(8,128)(2,1)S(1)} %pad_maximum_fusion.1), channel_id=1, source_target_pairs={{0,4},{4,0},{1,5},{5,1},{2,6},{6,2},{3,7},{7,3},{8,12},{12,8},{9,1... | collective-permute-start | bytes 786440 | tf_op jit(solution)/shard_map/ppermute | solution.py:315
  23.9 1.4 collective-permute-start.7
  25.3 1.5 collective-permute-start.8
  27.6 9.0 %all-to-all-done.kv_ref = bf16[8,416,128]{2,1,0:T(8,128)(2,1)S(1)} async-done(((bf16[8,416,128]{2,1,0:T(8,128)(2,1)}), bf16[8,416,128]{2,1,0:T(8,128)(2,1)S(1)}, u32[]{:S(2)}, u32[]{:S(2)}) %all-to-all-start) | async-done | bytes 852000 | tf_op jit(solution)/shard_map/all_to_all | solution.py:335
  37.5 2.0 %shard_map.192 = bf16[4,4,64,128]{3,2,1,0:T(8,128)(2,1)S(1)} custom-call(bf16[8,416,128]{2,1,0:T(8,128)(2,1)S(1)} %all-to-all-done.kv_ref, bf16[4,256,128]{2,1,0:T(8,128)(2,1)S(1)} %copy-done.15), custom_call_target="tpu_custom_call" | custom-call | flops 2000000000 | tf_op jit(solution)/shard_map/pallas_call | solution.py:351
  41.4 1.6 collective-permute-done.8.refs_5_
  43.0 2.6 %collective-permute-start.10 = (bf16[64,2048]{1,0:T(8,128)(2,1)}, bf16[64,2048]{1,0:T(8,128)(2,1)}, u32[]{:S(2)}, u32[]{:S(2)}) collective-permute-start(bf16[64,2048]{1,0:T(8,128)(2,1)} %collective-permute-done.8.refs_5_), channel_id=1, source_target_pairs={{0,3},{1,0},{2,1},{3,2},{4,7},{5,4},{6,5},{7,6},{8,11},{9,8},{10,9... | collective-permute-start | bytes 786440 | tf_op jit(solution)/shard_map/ppermute | solution.py:315
  45.6 2.0 %shard_map.191 = bf16[4,4,64,128]{3,2,1,0:T(8,128)(2,1)S(1)} custom-call(bf16[8,416,128]{2,1,0:T(8,128)(2,1)S(1)} %all-to-all-done.kv_ref, bf16[256,128]{1,0:T(8,128)(2,1)S(1)} %copy-done.12, bf16[256,128]{1,0:T(8,128)(2,1)S(1)} %collective-permute-done.refs_1_, bf16[256,128]{1,0:T(8,128)(2,1)S(1)} %collective-permute-done.1.refs_2_, ...), custom_call_target="tpu_custom_call" | custom-call | flops 2000000000 | tf_op jit(solution)/shard_map/pallas_call | solution.py:351
  47.6 1.7 %shard_map.193 = bf16[16,64,128]{2,1,0:T(8,128)(2,1)} custom-call(bf16[16,64,128]{2,1,0:T(8,128)(2,1)S(1)} %bitcast.30, bf16[16,64,128]{2,1,0:T(8,128)(2,1)S(1)} %collective-permute-done.4.b_ref), custom_call_target="tpu_custom_call" | custom-call | flops 500000000 | tf_op jit(solution)/shard_map/pallas_call | solution.py:368
  49.3 4.7 %all-to-all-start.1 = ((bf16[16,64,128]{2,1,0:T(8,128)(2,1)}), bf16[16,64,128]{2,1,0:T(8,128)(2,1)}, u32[]{:S(2)}, u32[]{:S(2)}) async-start(bf16[16,64,128]{2,1,0:T(8,128)(2,1)} %shard_map.193), calls=%async_computation.1 | async-start | bytes 524288 | tf_op jit(solution)/shard_map/all_to_all | solution.py:371
  61.4 2.5 %shard_map.195 = (bf16[64,2,2048]{2,1,0:T(2,128)(2,1)S(1)}, bf16[32,2048]{1,0:T(8,128)(2,1)S(1)}, bf16[2,32,128]{2,1,0:T(8,128)(2,1)S(1)}) custom-call(bf16[4,4,64,128]{3,2,1,0:T(8,128)(2,1)} %bitcast.12.parts_ref, bf16[32,2048]{1,0:T(8,128)(2,1)S(1)} %copy-done.16, f32[1,2048]{1,0:T(1,128)S(1)} %bitcast.28, s32[2,32]{1,0:T(2,128)S(1)} %bitcast.29, ...), custom_call_target="tpu_custom_call" | custom-call | flops 2000000000 | tf_op jit(solution)/shard_map/pallas_call | solution.py:383
  63.9 29.4 %all_to_all.21 = bf16[64,2,2048]{2,1,0:T(2,128)(2,1)S(1)} all-to-all(bf16[64,2,2048]{2,1,0:T(2,128)(2,1)S(1)} %get-tuple-element.25), channel_id=1, replica_groups=mesh['z'=8,'x'=4,'c'=2,'y'=4] {'z','x','c'}, dimensions={0} | all-to-all | bytes 1048576 | tf_op jit(solution)/shard_map/all_to_all | solution.py:391
  95.1 1.6 collective-permute-start.14
  96.7 5.8 %collective-permute-done.11.refs_2_ = bf16[64,2048]{1,0:T(8,128)(2,1)S(1)} collective-permute-done((bf16[64,2048]{1,0:T(8,128)(2,1)S(1)}, bf16[64,2048]{1,0:T(8,128)(2,1)S(1)}, u32[]{:S(2)}, u32[]{:S(2)}) %collective-permute-start.11) | collective-permute-done | bytes 262176 | tf_op jit(solution)/shard_map/ppermute | solution.py:315
  102.5 2.7 %collective-permute-start.16 = (bf16[64,2048]{1,0:T(8,128)(2,1)S(1)}, bf16[64,2048]{1,0:T(8,128)(2,1)S(1)}, u32[]{:S(2)}, u32[]{:S(2)}) collective-permute-start(bf16[64,2048]{1,0:T(8,128)(2,1)S(1)} %collective-permute-done.14.refs_5_), channel_id=1, source_target_pairs={{0,3},{1,0},{2,1},{3,2},{4,7},{5,4},{6,5},{7,6},{8,11},{9,8},{10,9... | collective-permute-start | bytes 786440 | tf_op jit(solution)/shard_map/ppermute | solution.py:315
  105.2 1.6 copy-done.1
  106.8 1.6 copy-done.2
  108.9 2.7 %collective-permute-start.13 = (bf16[64,2048]{1,0:T(8,128)(2,1)S(1)}, bf16[64,2048]{1,0:T(8,128)(2,1)S(1)}, u32[]{:S(2)}, u32[]{:S(2)}) collective-permute-start(bf16[64,2048]{1,0:T(8,128)(2,1)S(1)} %slice.13.refs_0_), channel_id=1, source_target_pairs={{0,3},{1,0},{2,1},{3,2},{4,7},{5,4},{6,5},{7,6},{8,11},{9,8},{10,9... | collective-permute-start | bytes 786440 | tf_op jit(solution)/shard_map/ppermute | solution.py:315
  113.0 3.2 %collective-permute-done.12.refs_3_ = bf16[64,2048]{1,0:T(8,128)(2,1)S(1)} collective-permute-done((bf16[64,2048]{1,0:T(8,128)(2,1)S(1)}, bf16[64,2048]{1,0:T(8,128)(2,1)S(1)}, u32[]{:S(2)}, u32[]{:S(2)}) %collective-permute-start.12) | collective-permute-done | bytes 262176 | tf_op jit(solution)/shard_map/ppermute | solution.py:315
  116.2 2.7 %shard_map.197 = (bf16[64,2048]{1,0:T(8,128)(2,1)S(1)}, bf16[64,2048]{1,0:T(8,128)(2,1)S(1)}, bf16[64,2048]{1,0:T(8,128)(2,1)S(1)}, bf16[64,2048]{1,0:T(8,128)(2...) custom-call(bf16[64,2048]{1,0:T(8,128)(2,1)S(1)} %slice.13.refs_0_, ...), custom_call_target="tpu_custom_call" | custom-call | flops 3000000000 | tf_op jit(solution)/shard_map/pallas_call | solution.py:406
  118.9 2.5 %collective-permute-start.19 = (bf16[64,2048]{1,0:T(8,128)(2,1)S(1)}, bf16[64,2048]{1,0:T(8,128)(2,1)S(1)}, u32[]{:S(2)}, u32[]{:S(2)}) collective-permute-start(bf16[64,2048]{1,0:T(8,128)(2,1)S(1)} %get-tuple-element.32), channel_id=1, source_target_pairs={{0,3},{1,0},{2,1},{3,2},{4,7},{5,4},{6,5},{7,6},{8,11},{9,8},{10,9... | collective-permute-start | bytes 786440 | tf_op jit(solution)/shard_map/ppermute | solution.py:315
  121.4 2.7 %collective-permute-start.21 = (bf16[64,2048]{1,0:T(8,128)(2,1)S(1)}, bf16[64,2048]{1,0:T(8,128)(2,1)S(1)}, u32[]{:S(2)}, u32[]{:S(2)}) collective-permute-start(bf16[64,2048]{1,0:T(8,128)(2,1)S(1)} %get-tuple-element.36), channel_id=1, source_target_pairs={{0,3},{1,0},{2,1},{3,2},{4,7},{5,4},{6,5},{7,6},{8,11},{9,8},{10,9... | collective-permute-start | bytes 786440 | tf_op jit(solution)/shard_map/ppermute | solution.py:315
  124.2 5.5 %collective-permute-done.21 = bf16[64,2048]{1,0:T(8,128)(2,1)S(1)} collective-permute-done((bf16[64,2048]{1,0:T(8,128)(2,1)S(1)}, bf16[64,2048]{1,0:T(8,128)(2,1)S(1)}, u32[]{:S(2)}, u32[]{:S(2)}) %collective-permute-start.21) | collective-permute-done | bytes 262176 | tf_op jit(solution)/shard_map/ppermute | solution.py:315
  129.8 3.5 %collective-permute-start.22 = (bf16[64,2048]{1,0:T(8,128)(2,1)S(1)}, bf16[64,2048]{1,0:T(8,128)(2,1)S(1)}, u32[]{:S(2)}, u32[]{:S(2)}) collective-permute-start(bf16[64,2048]{1,0:T(8,128)(2,1)S(1)} %add_convert_fusion.1), channel_id=1, source_target_pairs={{0,3},{1,0},{2,1},{3,2},{4,7},{5,4},{6,5},{7,6},{8,11},{9,8},{10,9... | collective-permute-start | bytes 786440 | tf_op jit(solution)/shard_map/ppermute | solution.py:315
  133.4 3.2 %collective-permute-done.22 = bf16[64,2048]{1,0:T(8,128)(2,1)S(1)} collective-permute-done((bf16[64,2048]{1,0:T(8,128)(2,1)S(1)}, bf16[64,2048]{1,0:T(8,128)(2,1)S(1)}, u32[]{:S(2)}, u32[]{:S(2)}) %collective-permute-start.22) | collective-permute-done | bytes 262176 | tf_op jit(solution)/shard_map/ppermute | solution.py:315
  137.1 27.2 %all_to_all.22 = bf16[64,2,2048]{2,1,0:T(2,128)(2,1)S(1)} all-to-all(bf16[64,2,2048]{2,1,0:T(2,128)(2,1)S(1)} %convert_element_type.53), channel_id=1, replica_groups=mesh['z'=8,'x'=4,'c'=2,'y'=4] {'z','x','c'}, dimensions={0} | all-to-all | bytes 1048576 | tf_op jit(solution)/shard_map/all_to_all | solution.py:438
  (79 shorter events, 17.9 us)
Async XLA Ops:
  0.0 25.3 %copy-start.11 = (bf16[64,2048]{1,0:T(8,128)(2,1)S(1)}, bf16[64,2048]{1,0:T(8,128)(2,1)}, u32[]{:S(2)}) copy-start(bf16[64,2048]{1,0:T(8,128)(2,1)} %refs_1_.1) | copy-start | bytes 786436
  2.6 34.0 %all-to-all-start = ((bf16[8,416,128]{2,1,0:T(8,128)(2,1)}), bf16[8,416,128]{2,1,0:T(8,128)(2,1)S(1)}, u32[]{:S(2)}, u32[]{:S(2)}) async-start(bf16[8,416,128]{2,1,0:T(8,128)(2,1)} %get-tuple-element.21), calls=%async_computation | async-start | bytes 1703936 | tf_op jit(solution)/shard_map/all_to_all | solution.py:335
  11.6 15.2 %collective-permute-start.5 = (bf16[128,2048]{1,0:T(8,128)(2,1)S(1)}, bf16[128,2048]{1,0:T(8,128)(2,1)S(1)}, u32[]{:S(2)}, u32[]{:S(2)}) collective-permute-start(bf16[128,2048]{1,0:T(8,128)(2,1)S(1)} %copy-done.3), channel_id=1, source_target_pairs={{0,1},{1,2},{2,3},{3,0},{4,5},{5,6},{6,7},{7,4},{8,9},{9,10},{10,1... | collective-permute-start | bytes 1572872 | tf_op jit(solution)/shard_map/ppermute | solution.py:315
  12.9 5.4 %collective-permute-start.2 = (bf16[256,128]{1,0:T(8,128)(2,1)}, bf16[256,128]{1,0:T(8,128)(2,1)S(1)}, u32[]{:S(2)}, u32[]{:S(2)}) collective-permute-start(bf16[256,128]{1,0:T(8,128)(2,1)} %get-tuple-element.22.refs_0_), channel_id=1, source_target_pairs={{0,16},{8,24},{16,0},{24,8},{1,17},{9,25},{17,1},{25,9},{2,18},{10... | collective-permute-start | bytes 196616 | tf_op jit(solution)/shard_map/ppermute | solution.py:315
  15.7 5.1 %collective-permute-start = (bf16[256,128]{1,0:T(8,128)(2,1)}, bf16[256,128]{1,0:T(8,128)(2,1)S(1)}, u32[]{:S(2)}, u32[]{:S(2)}) collective-permute-start(bf16[256,128]{1,0:T(8,128)(2,1)} %get-tuple-element.22.refs_0_), channel_id=1, source_target_pairs={{0,8},{8,16},{16,24},{24,0},{1,9},{9,17},{17,25},{25,1},{2,10},{10... | collective-permute-start | bytes 196616 | tf_op jit(solution)/shard_map/ppermute | solution.py:315
  16.0 4.8 %collective-permute-start.1 = (bf16[256,128]{1,0:T(8,128)(2,1)}, bf16[256,128]{1,0:T(8,128)(2,1)S(1)}, u32[]{:S(2)}, u32[]{:S(2)}) collective-permute-start(bf16[256,128]{1,0:T(8,128)(2,1)} %get-tuple-element.22.refs_0_), channel_id=1, source_target_pairs={{0,24},{8,0},{16,8},{24,16},{1,25},{9,1},{17,9},{25,17},{2,26},{10... | collective-permute-start | bytes 196616 | tf_op jit(solution)/shard_map/ppermute | solution.py:315
  21.7 23.9 %copy-start.12 = (bf16[256,128]{1,0:T(8,128)(2,1)S(1)}, bf16[256,128]{1,0:T(8,128)(2,1)}, u32[]{:S(2)}) copy-start(bf16[256,128]{1,0:T(8,128)(2,1)} %get-tuple-element.22.refs_0_) | copy-start | bytes 196612
  21.7 5.1 %collective-permute-start.3 = (bf16[4,256,128]{2,1,0:T(8,128)(2,1)S(1)}, bf16[4,256,128]{2,1,0:T(8,128)(2,1)S(1)}, u32[]{:S(2)}, u32[]{:S(2)}) collective-permute-start(bf16[4,256,128]{2,1,0:T(8,128)(2,1)S(1)} %pad_maximum_fusion.1), channel_id=1, source_target_pairs={{0,4},{4,0},{1,5},{5,1},{2,6},{6,2},{3,7},{7,3},{8,12},{12,8},{9,1... | collective-permute-start | bytes 786440 | tf_op jit(solution)/shard_map/ppermute | solution.py:315
  23.9 30.2 %collective-permute-start.7 = (bf16[128,2048]{1,0:T(8,128)(2,1)S(1)}, bf16[128,2048]{1,0:T(8,128)(2,1)S(1)}, u32[]{:S(2)}, u32[]{:S(2)}) collective-permute-start(bf16[128,2048]{1,0:T(8,128)(2,1)S(1)} %copy-done.3), channel_id=1, source_target_pairs={{0,3},{1,0},{2,1},{3,2},{4,7},{5,4},{6,5},{7,6},{8,11},{9,8},{10,9... | collective-permute-start | bytes 1572872 | tf_op jit(solution)/shard_map/ppermute | solution.py:315
  25.3 17.7 %collective-permute-start.8 = (bf16[64,2048]{1,0:T(8,128)(2,1)S(1)}, bf16[64,2048]{1,0:T(8,128)(2,1)}, u32[]{:S(2)}, u32[]{:S(2)}) collective-permute-start(bf16[64,2048]{1,0:T(8,128)(2,1)S(1)} %copy-done.11), channel_id=1, source_target_pairs={{0,3},{1,0},{2,1},{3,2},{4,7},{5,4},{6,5},{7,6},{8,11},{9,8},{10,9... | collective-permute-start | bytes 786440 | tf_op jit(solution)/shard_map/ppermute | solution.py:315
  26.8 12.7 %copy-start.5 = (bf16[128,2048]{1,0:T(8,128)(2,1)}, bf16[128,2048]{1,0:T(8,128)(2,1)S(1)}, u32[]{:S(2)}) copy-start(bf16[128,2048]{1,0:T(8,128)(2,1)S(1)} %collective-permute-done.5.refs_2_) | copy-start | bytes 1572868
  26.8 28.1 %collective-permute-start.9 = (bf16[128,2048]{1,0:T(8,128)(2,1)S(1)}, bf16[128,2048]{1,0:T(8,128)(2,1)S(1)}, u32[]{:S(2)}, u32[]{:S(2)}) collective-permute-start(bf16[128,2048]{1,0:T(8,128)(2,1)S(1)} %collective-permute-done.5.refs_2_), channel_id=1, source_target_pairs={{0,1},{1,2},{2,3},{3,0},{4,5},{5,6},{6,7},{7,4},{8,9},{9,10},{10,1... | collective-permute-start | bytes 1572872 | tf_op jit(solution)/shard_map/ppermute | solution.py:315
  39.5 8.1 %collective-permute-start.4 = (bf16[16,64,128]{2,1,0:T(8,128)(2,1)S(1)}, bf16[16,64,128]{2,1,0:T(8,128)(2,1)S(1)}, u32[]{:S(2)}, u32[]{:S(2)}) collective-permute-start(bf16[16,64,128]{2,1,0:T(8,128)(2,1)S(1)} %bitcast.27), channel_id=1, source_target_pairs={{0,4},{4,0},{1,5},{5,1},{2,6},{6,2},{3,7},{7,3},{8,12},{12,8},{9,1... | collective-permute-start | bytes 786440 | tf_op jit(solution)/shard_map/ppermute | solution.py:315
  40.1 14.0 %collective-permute-start.6 = (bf16[64,2048]{1,0:T(8,128)(2,1)S(1)}, bf16[64,2048]{1,0:T(8,128)(2,1)}, u32[]{:S(2)}, u32[]{:S(2)}) collective-permute-start(bf16[64,2048]{1,0:T(8,128)(2,1)S(1)} %copy-done.11), channel_id=1, source_target_pairs={{0,1},{1,2},{2,3},{3,0},{4,5},{5,6},{6,7},{7,4},{8,9},{9,10},{10,1... | collective-permute-start | bytes 786440 | tf_op jit(solution)/shard_map/ppermute | solution.py:315
  43.0 11.0 %collective-permute-start.10 = (bf16[64,2048]{1,0:T(8,128)(2,1)}, bf16[64,2048]{1,0:T(8,128)(2,1)}, u32[]{:S(2)}, u32[]{:S(2)}) collective-permute-start(bf16[64,2048]{1,0:T(8,128)(2,1)} %collective-permute-done.8.refs_5_), channel_id=1, source_target_pairs={{0,3},{1,0},{2,1},{3,2},{4,7},{5,4},{6,5},{7,6},{8,11},{9,8},{10,9... | collective-permute-start | bytes 786440 | tf_op jit(solution)/shard_map/ppermute | solution.py:315
  49.3 12.1 %copy-start.17 = (f32[2048]{0:T(1024)S(1)}, f32[2048]{0:T(1024)}, u32[]{:S(2)}) copy-start(f32[2048]{0:T(1024)} %param.32) | copy-start | bytes 24580
  49.3 12.1 %copy-start.18 = (s32[32,2]{0,1:T(2,128)S(1)}, s32[32,2]{0,1:T(2,128)}, u32[]{:S(2)}) copy-start(s32[32,2]{0,1:T(2,128)} %param.36) | copy-start | bytes 772
  49.3 12.1 %all-to-all-start.1 = ((bf16[16,64,128]{2,1,0:T(8,128)(2,1)}), bf16[16,64,128]{2,1,0:T(8,128)(2,1)}, u32[]{:S(2)}, u32[]{:S(2)}) async-start(bf16[16,64,128]{2,1,0:T(8,128)(2,1)} %shard_map.193), calls=%async_computation.1 | async-start | bytes 524288 | tf_op jit(solution)/shard_map/all_to_all | solution.py:371
  63.9 41.3 %copy-start = (bf16[1,2048,512]{2,1,0:T(8,128)(2,1)S(1)}, bf16[1,2048,512]{2,1,0:T(8,128)(2,1)}, u32[]{:S(2)}) copy-start(bf16[1,2048,512]{2,1,0:T(8,128)(2,1)} %param.33) | copy-start | bytes 6291460
  93.8 8.8 %collective-permute-start.11 = (bf16[64,2048]{1,0:T(8,128)(2,1)S(1)}, bf16[64,2048]{1,0:T(8,128)(2,1)S(1)}, u32[]{:S(2)}, u32[]{:S(2)}) collective-permute-start(bf16[64,2048]{1,0:T(8,128)(2,1)S(1)} %slice.13.refs_0_), channel_id=1, source_target_pairs={{0,1},{1,2},{2,3},{3,0},{4,5},{5,6},{6,7},{7,4},{8,9},{9,10},{10,1... | collective-permute-start | bytes 786440 | tf_op jit(solution)/shard_map/ppermute | solution.py:315
  95.1 7.4 %collective-permute-start.14 = (bf16[64,2048]{1,0:T(8,128)(2,1)S(1)}, bf16[64,2048]{1,0:T(8,128)(2,1)S(1)}, u32[]{:S(2)}, u32[]{:S(2)}) collective-permute-start(bf16[64,2048]{1,0:T(8,128)(2,1)S(1)} %slice.15.refs_1_), channel_id=1, source_target_pairs={{0,3},{1,0},{2,1},{3,2},{4,7},{5,4},{6,5},{7,6},{8,11},{9,8},{10,9... | collective-permute-start | bytes 786440 | tf_op jit(solution)/shard_map/ppermute | solution.py:315
  102.5 9.1 %collective-permute-start.15 = (bf16[64,2048]{1,0:T(8,128)(2,1)S(1)}, bf16[64,2048]{1,0:T(8,128)(2,1)S(1)}, u32[]{:S(2)}, u32[]{:S(2)}) collective-permute-start(bf16[64,2048]{1,0:T(8,128)(2,1)S(1)} %collective-permute-done.11.refs_2_), channel_id=1, source_target_pairs={{0,1},{1,2},{2,3},{3,0},{4,5},{5,6},{6,7},{7,4},{8,9},{9,10},{10,1... | collective-permute-start | bytes 786440 | tf_op jit(solution)/shard_map/ppermute | solution.py:315
  102.5 9.1 %collective-permute-start.16 = (bf16[64,2048]{1,0:T(8,128)(2,1)S(1)}, bf16[64,2048]{1,0:T(8,128)(2,1)S(1)}, u32[]{:S(2)}, u32[]{:S(2)}) collective-permute-start(bf16[64,2048]{1,0:T(8,128)(2,1)S(1)} %collective-permute-done.14.refs_5_), channel_id=1, source_target_pairs={{0,3},{1,0},{2,1},{3,2},{4,7},{5,4},{6,5},{7,6},{8,11},{9,8},{10,9... | collective-permute-start | bytes 786440 | tf_op jit(solution)/shard_map/ppermute | solution.py:315
  108.8 7.3 %collective-permute-start.12 = (bf16[64,2048]{1,0:T(8,128)(2,1)S(1)}, bf16[64,2048]{1,0:T(8,128)(2,1)S(1)}, u32[]{:S(2)}, u32[]{:S(2)}) collective-permute-start(bf16[64,2048]{1,0:T(8,128)(2,1)S(1)} %slice.15.refs_1_), channel_id=1, source_target_pairs={{0,1},{1,2},{2,3},{3,0},{4,5},{5,6},{6,7},{7,4},{8,9},{9,10},{10,1... | collective-permute-start | bytes 786440 | tf_op jit(solution)/shard_map/ppermute | solution.py:315
  108.9 7.3 %collective-permute-start.13 = (bf16[64,2048]{1,0:T(8,128)(2,1)S(1)}, bf16[64,2048]{1,0:T(8,128)(2,1)S(1)}, u32[]{:S(2)}, u32[]{:S(2)}) collective-permute-start(bf16[64,2048]{1,0:T(8,128)(2,1)S(1)} %slice.13.refs_0_), channel_id=1, source_target_pairs={{0,3},{1,0},{2,1},{3,2},{4,7},{5,4},{6,5},{7,6},{8,11},{9,8},{10,9... | collective-permute-start | bytes 786440 | tf_op jit(solution)/shard_map/ppermute | solution.py:315
  112.7 11.3 %collective-permute-start.17 = (bf16[64,2048]{1,0:T(8,128)(2,1)S(1)}, bf16[64,2048]{1,0:T(8,128)(2,1)S(1)}, u32[]{:S(2)}, u32[]{:S(2)}) collective-permute-start(bf16[64,2048]{1,0:T(8,128)(2,1)S(1)} %get-tuple-element.31), channel_id=1, source_target_pairs={{0,1},{1,2},{2,3},{3,0},{4,5},{5,6},{6,7},{7,4},{8,9},{9,10},{10,1... | collective-permute-start | bytes 786440 | tf_op jit(solution)/shard_map/ppermute | solution.py:315
  118.9 14.4 %collective-permute-start.19 = (bf16[64,2048]{1,0:T(8,128)(2,1)S(1)}, bf16[64,2048]{1,0:T(8,128)(2,1)S(1)}, u32[]{:S(2)}, u32[]{:S(2)}) collective-permute-start(bf16[64,2048]{1,0:T(8,128)(2,1)S(1)} %get-tuple-element.32), channel_id=1, source_target_pairs={{0,3},{1,0},{2,1},{3,2},{4,7},{5,4},{6,5},{7,6},{8,11},{9,8},{10,9... | collective-permute-start | bytes 786440 | tf_op jit(solution)/shard_map/ppermute | solution.py:315
  121.4 12.0 %collective-permute-start.20 = (bf16[64,2048]{1,0:T(8,128)(2,1)S(1)}, bf16[64,2048]{1,0:T(8,128)(2,1)S(1)}, u32[]{:S(2)}, u32[]{:S(2)}) collective-permute-start(bf16[64,2048]{1,0:T(8,128)(2,1)S(1)} %get-tuple-element.34), channel_id=1, source_target_pairs={{0,1},{1,2},{2,3},{3,0},{4,5},{5,6},{6,7},{7,4},{8,9},{9,10},{10,1... | collective-permute-start | bytes 786440 | tf_op jit(solution)/shard_map/ppermute | solution.py:315
  121.4 8.3 %collective-permute-start.21 = (bf16[64,2048]{1,0:T(8,128)(2,1)S(1)}, bf16[64,2048]{1,0:T(8,128)(2,1)S(1)}, u32[]{:S(2)}, u32[]{:S(2)}) collective-permute-start(bf16[64,2048]{1,0:T(8,128)(2,1)S(1)} %get-tuple-element.36), channel_id=1, source_target_pairs={{0,3},{1,0},{2,1},{3,2},{4,7},{5,4},{6,5},{7,6},{8,11},{9,8},{10,9... | collective-permute-start | bytes 786440 | tf_op jit(solution)/shard_map/ppermute | solution.py:315
  124.1 9.2 %collective-permute-start.18 = (bf16[64,2048]{1,0:T(8,128)(2,1)S(1)}, bf16[64,2048]{1,0:T(8,128)(2,1)S(1)}, u32[]{:S(2)}, u32[]{:S(2)}) collective-permute-start(bf16[64,2048]{1,0:T(8,128)(2,1)S(1)} %add_convert_fusion.3), channel_id=1, source_target_pairs={{0,1},{1,2},{2,3},{3,0},{4,5},{5,6},{6,7},{7,4},{8,9},{9,10},{10,1... | collective-permute-start | bytes 786440 | tf_op jit(solution)/shard_map/ppermute | solution.py:315
  129.8 6.8 %collective-permute-start.22 = (bf16[64,2048]{1,0:T(8,128)(2,1)S(1)}, bf16[64,2048]{1,0:T(8,128)(2,1)S(1)}, u32[]{:S(2)}, u32[]{:S(2)}) collective-permute-start(bf16[64,2048]{1,0:T(8,128)(2,1)S(1)} %add_convert_fusion.1), channel_id=1, source_target_pairs={{0,3},{1,0},{2,1},{3,2},{4,7},{5,4},{6,5},{7,6},{8,11},{9,8},{10,9... | collective-permute-start | bytes 786440 | tf_op jit(solution)/shard_map/ppermute | solution.py:315
  136.7 27.8 %copy-start.13 = (f32[32,2]{0,1:T(2,128)S(1)}, f32[32,2]{0,1:T(2,128)}, u32[]{:S(2)}) copy-start(f32[32,2]{0,1:T(2,128)} %param.37) | copy-start | bytes 772
  (12 other events, 34.3 us)

commit v5 on v4

--- a/solution.py
+++ b/solution.py
@@ -58,10 +58,7 @@
     return jnp.sum(jnp.where(same, row, 0.0), axis=1, keepdims=True)
 
 
-def pre_kernel(
-    lat_ref, gain_ref, rk_ref, qs_ref, ql_ref, ks_w, vs_w, kl_w, vl_w,
-    base_ref, row_ref, kv_ref, q_ref,
-):
+def turner(base_ref, row_ref):
     block = (lax.axis_index("z") * NX + lax.axis_index("x")) * NC + lax.axis_index("c")
     base = column(base_ref[pl.ds(block, 1), :])
     cb, sb = base[:ROPE], base[ROPE:]
@@ -76,6 +73,13 @@
         swapped = jnp.concatenate([v[ROPE // 2 :], v[: ROPE // 2]], axis=0)
         return v * cos + swapped * sin
 
+    return turned
+
+
+def key_kernel(
+    lat_ref, gain_ref, rk_ref, ks_w, vs_w, kl_w, vl_w, base_ref, row_ref, kv_ref
+):
+    turned = turner(base_ref, row_ref)
     lat = lat_ref[...].astype(f32)
     scale = lax.rsqrt(jnp.mean(lat * lat, axis=1, keepdims=True) + EPS)
     normed = (lat * scale * gain_ref[...]).astype(bf16)
@@ -92,6 +96,10 @@
     ).astype(bf16)
     for j in range(1, NZ):
         kv_ref[j] = kv_ref[0]
+
+
+def query_kernel(qs_ref, ql_ref, base_ref, row_ref, q_ref):
+    turned = turner(base_ref, row_ref)
     q_ref[0:128, :] = ql_ref[0:NOPE_L, :].astype(f32).T.astype(bf16)
     mixed = jnp.concatenate(
         [qs_ref[0:NOPE_S, :].astype(f32), turned(ql_ref[NOPE_L:, :]), turned(qs_ref[NOPE_S:, :])],
@@ -161,29 +169,34 @@
                 out_ref[xq[half], y, TOK : 2 * TOK, :] = o_s[lo : lo + TOK]
 
 
+def merged(large, small):
+    lane = lax.broadcasted_iota(jnp.int32, small[0].shape, 1)
+    scale = jnp.where(lane < 3, SCALE_L, SCALE_S)
+    top = functools.reduce(jnp.maximum, small)
+    ws = [
+        (pltpu.roll(s, 127, 1) + pltpu.roll(s, 126, 1)) * jnp.exp2((s - top) * scale)
+        for s in small
+    ]
+    total = functools.reduce(jnp.add, ws)
+    ws = [w / total for w in ws]
+    out_l = functools.reduce(jnp.add, [v * w[:, 0:1] for v, w in zip(large, ws)])
+    out_s = functools.reduce(jnp.add, [v * w[:, 3:4] for v, w in zip(small, ws)])
+    return out_l, out_s, top, total, lane
+
+
 def merge_kernel(a_ref, b_ref, out_ref):
     rows = NX * NY * TOK
     ref = [r[...].astype(f32) for r in (a_ref, b_ref)]
-    large = [r[:, :TOK].reshape(rows, 128) for r in ref]
-    small = [r[:, TOK:].reshape(rows, 128) for r in ref]
-    lanes = lax.broadcasted_iota(jnp.int32, (rows, 128), 1)
-    outs = []
-    stats = []
-    for at, scale, values in ((0, SCALE_L, large), (3, SCALE_S, small)):
-        tops = [s[:, at : at + 1] for s in small]
-        top = jnp.maximum(tops[0], tops[1])
-        ws = [
-            (s[:, at + 1 : at + 2] + s[:, at + 2 : at + 3]) * jnp.exp2((t - top) * scale)
-            for s, t in zip(small, tops)
-        ]
-        total = ws[0] + ws[1]
-        outs.append(values[0] * (ws[0] / total) + values[1] * (ws[1] / total))
-        high = total.astype(bf16).astype(f32)
-        stats += [top, high, total - high]
-    for i, v in enumerate(stats):
-        outs[1] = jnp.where(lanes == i, v, outs[1])
-    out_ref[:, :TOK] = outs[0].astype(bf16).reshape(NX * NY, TOK, 128)
-    out_ref[:, TOK:] = outs[1].astype(bf16).reshape(NX * NY, TOK, 128)
+    out_l, out_s, top, total, lane = merged(
+        [r[:, :TOK].reshape(rows, 128) for r in ref],
+        [r[:, TOK:].reshape(rows, 128) for r in ref],
+    )
+    high = total.astype(bf16).astype(f32)
+    out_s = jnp.where((lane == 0) | (lane == 3), top, out_s)
+    out_s = jnp.where((lane == 1) | (lane == 4), pltpu.roll(high, 1, 1), out_s)
+    out_s = jnp.where((lane == 2) | (lane == 5), pltpu.roll(total - high, 2, 1), out_s)
+    out_ref[:, :TOK] = out_l.astype(bf16).reshape(NX * NY, TOK, 128)
+    out_ref[:, TOK:] = out_s.astype(bf16).reshape(NX * NY, TOK, 128)
 
 
 def gather_kernel(*refs):
@@ -210,18 +223,9 @@
         larges = [parts_ref[i, ya, 0:TOK, :].astype(f32) for i in range(NX)]
         smalls = [parts_ref[i, ya, TOK : 2 * TOK, :].astype(f32) for i in range(NX)]
 
-        def mixed(values, at, scale):
-            tops = [s[:, at : at + 1] for s in smalls]
-            top = functools.reduce(jnp.maximum, tops)
-            ws = [
-                (s[:, at + 1 : at + 2] + s[:, at + 2 : at + 3]) * jnp.exp2((t - top) * scale)
-                for s, t in zip(smalls, tops)
-            ]
-            inv = 1.0 / functools.reduce(jnp.add, ws)
-            return functools.reduce(jnp.add, [v * (w * inv) for v, w in zip(values, ws)])
-
-        large = mixed(larges, 0, SCALE_L).astype(bf16)
-        small = mixed(smalls, 3, SCALE_S)[:, 64:128].astype(bf16)
+        out_l, out_s, _, _, _ = merged(larges, smalls)
+        large = out_l.astype(bf16)
+        small = out_s[:, 64:128].astype(bf16)
         heads = jnp.concatenate([large, small], axis=1)
         partial = jnp.dot(heads, w_ref[n], preferred_element_type=f32)
         total = total + partial.astype(bf16).astype(f32)
@@ -321,18 +325,16 @@
     ffn_gain, gate_weights, up_weights, down_weights, routing, route_weight,
 ):
     base, row = rope_parts()
-    kv, q = call(
-        pre_kernel,
-        vmem(11),
-        [((NZ, 416, 128), bf16), ((256, 128), bf16)],
-        flops=10**9,
-        mib=63,
-    )(
-        latent, latent_gain[None, :], rotary_key.T, query_small.T, query_large.T,
-        small_keys.T, small_values.T, large_keys, large_values, base, row,
+    kv = call(key_kernel, vmem(9), [((NZ, 416, 128), bf16)], flops=10**9, mib=63)(
+        latent, latent_gain[None, :], rotary_key.T, small_keys.T, small_values.T,
+        large_keys, large_values, base, row,
     )
 
     kvs = lax.all_to_all(kv, "z", 0, 0, tiled=True)
+
+    q = call(query_kernel, vmem(4), [((256, 128), bf16)], flops=10**8, mib=63)(
+        query_small.T, query_large.T, base, row
+    )
 
     qx = [q]
     for by in (1, -1, 2):

time: 166 us -> 169 us (1.018)
  waiting for transfers between devices: 31 us -> 32.7 us
    ppermute x23, waiting for transfers between devices: 21.8 us -> 24.5 us  [shifted(): return lax.ppermute(a, axis, [(i, (i + by) % size) for i in range(size)])]
    pallas_call x1 -> x2, Pallas kernels: 2.57 us -> 4.12 us  [the longest x1 2.51 us: layer(): call(key_kernel, vmem(9), [((NZ, 416, 128), bf16)], flops=10 ** 9, mib=63)]
  transfers between devices with their start and end apart: 25 -> 25, of which waited for: 8 -> 7; matrix products, arithmetic and copies ran while one was open for 1% -> 1% of each run, Pallas kernels for 7% -> 7%
where the time goes in v5:
time: 169 us; the launch traced here: 168 us
  blocking collectives  56.9 us (34%)
  starting transfers between devices  47.2 us (28%)
  waiting for transfers between devices  32.7 us (19%)
  Pallas kernels  18.3 us (11%)
  local copies, waits for them, and re-layouts  11.6 us (7%)
    ppermute x23, starting transfers between devices, shifted(): return lax.ppermute(a, axis, [(i, (i + by) % size) for i in range(size)])  33.5 us
    all_to_all x1, blocking collectives, layer(): mine = lax.all_to_all(disp, sp, 0, 0, tiled=True)  29.7 us
    all_to_all x1, blocking collectives, layer(): ret = lax.all_to_all(done.reshape(EXPERTS, CAP, D), sp, 0, 0, tiled=True)  27.2 us
    ppermute x23, waiting for transfers between devices, shifted(): return lax.ppermute(a, axis, [(i, (i + by) % size) for i in range(size)])  24.5 us
    unnamed x38, local copies, waits for them, and re-layouts  10.5 us
    all_to_all x1, starting transfers between devices, layer(): kvs = lax.all_to_all(kv, 'z', 0, 0, tiled=True)  9.01 us
    all_to_all x1, waiting for transfers between devices, layer(): kvs = lax.all_to_all(kv, 'z', 0, 0, tiled=True)  8.21 us
    all_to_all x1, starting transfers between devices, layer(): lax.all_to_all(parts.reshape(NX * NY * 2 * TOK, 128), ('x', 'y'), 0, 0, t...  4.73 us
  transfers between devices with their start and end apart: 25, of which 7 were waited for; matrix products, arithmetic and copies ran while one was open for 1% of the time, Pallas kernels for 7%

profile of v5, /device:TPU:1, one launch (start us, length us, event | category | flops | bytes accessed | tf_op | source)
XLA Modules:
  0.0 168.2 jit_solution(566263329888710575)
XLA Ops:
  0.0 2.5 %shard_map.190 = bf16[8,416,128]{2,1,0:T(8,128)(2,1)} custom-call(bf16[128,512]{1,0:T(8,128)(2,1)} %lat_ref.1, f32[1,512]{1,0:T(1,128)} %bitcast.36, bf16[32,128]{1,0:T(8,128)(2,1)} %bitcast.35, bf16[64,512]{1,0:T(8,128)(2,1)} %bitcast.31, bf16[64,512]{1,0:T(8,128)(2,1)} %bitcast.32, bf16[512,128]{1,0:T(8,128)(2,1)} %kl_w.1, bf16[512,128]{1,0:T(8,128)(2,1)} %vl_w.1, ...), custom_call_target="tpu_custom_call" | custom-call | flops 1000000000 | tf_op jit(solution)/shard_map/pallas_call | solution.py:328
  2.5 9.0 %all-to-all-start = ((bf16[8,416,128]{2,1,0:T(8,128)(2,1)}), bf16[8,416,128]{2,1,0:T(8,128)(2,1)S(1)}, u32[]{:S(2)}, u32[]{:S(2)}) async-start(bf16[8,416,128]{2,1,0:T(8,128)(2,1)} %shard_map.190), calls=%async_computation | async-start | bytes 1703936 | tf_op jit(solution)/shard_map/all_to_all | solution.py:333
  12.8 1.6 shard_map.191.refs_0_
  14.4 2.7 %collective-permute-start.2 = (bf16[256,128]{1,0:T(8,128)(2,1)}, bf16[256,128]{1,0:T(8,128)(2,1)S(1)}, u32[]{:S(2)}, u32[]{:S(2)}) collective-permute-start(bf16[256,128]{1,0:T(8,128)(2,1)} %shard_map.191.refs_0_), channel_id=1, source_target_pairs={{0,16},{8,24},{16,0},{24,8},{1,17},{9,25},{17,1},{25,9},{2,18},{10... | collective-permute-start | bytes 196616 | tf_op jit(solution)/shard_map/ppermute | solution.py:319
  17.5 2.4 %collective-permute-start.1 = (bf16[256,128]{1,0:T(8,128)(2,1)}, bf16[256,128]{1,0:T(8,128)(2,1)S(1)}, u32[]{:S(2)}, u32[]{:S(2)}) collective-permute-start(bf16[256,128]{1,0:T(8,128)(2,1)} %shard_map.191.refs_0_), channel_id=1, source_target_pairs={{0,24},{8,0},{16,8},{24,16},{1,25},{9,1},{17,9},{25,17},{2,26},{10... | collective-permute-start | bytes 196616 | tf_op jit(solution)/shard_map/ppermute | solution.py:319
  19.9 2.5 %collective-permute-done.refs_1_ = bf16[256,128]{1,0:T(8,128)(2,1)S(1)} collective-permute-done((bf16[256,128]{1,0:T(8,128)(2,1)}, bf16[256,128]{1,0:T(8,128)(2,1)S(1)}, u32[]{:S(2)}, u32[]{:S(2)}) %collective-permute-start) | collective-permute-done | bytes 65568 | tf_op jit(solution)/shard_map/ppermute | solution.py:319
  23.3 2.1 %collective-permute-start.3 = (bf16[4,256,128]{2,1,0:T(8,128)(2,1)S(1)}, bf16[4,256,128]{2,1,0:T(8,128)(2,1)S(1)}, u32[]{:S(2)}, u32[]{:S(2)}) collective-permute-start(bf16[4,256,128]{2,1,0:T(8,128)(2,1)S(1)} %pad_maximum_fusion.1), channel_id=1, source_target_pairs={{0,4},{4,0},{1,5},{5,1},{2,6},{6,2},{3,7},{7,3},{8,12},{12,8},{9,1... | collective-permute-start | bytes 786440 | tf_op jit(solution)/shard_map/ppermute | solution.py:319
  25.4 1.4 collective-permute-start.7
  26.7 1.5 collective-permute-start.8
  28.3 8.2 %all-to-all-done.kv_ref = bf16[8,416,128]{2,1,0:T(8,128)(2,1)S(1)} async-done(((bf16[8,416,128]{2,1,0:T(8,128)(2,1)}), bf16[8,416,128]{2,1,0:T(8,128)(2,1)S(1)}, u32[]{:S(2)}, u32[]{:S(2)}) %all-to-all-start) | async-done | bytes 852000 | tf_op jit(solution)/shard_map/all_to_all | solution.py:333
  36.5 2.0 %shard_map.193 = bf16[4,4,64,128]{3,2,1,0:T(8,128)(2,1)S(1)} custom-call(bf16[8,416,128]{2,1,0:T(8,128)(2,1)S(1)} %all-to-all-done.kv_ref, bf16[4,256,128]{2,1,0:T(8,128)(2,1)S(1)} %collective-permute-done.3.refs_0_), custom_call_target="tpu_custom_call" | custom-call | flops 2000000000 | tf_op jit(solution)/shard_map/pallas_call | solution.py:353
  40.4 4.2 %collective-permute-done.8.refs_5_ = bf16[64,2048]{1,0:T(8,128)(2,1)S(1)} collective-permute-done((bf16[64,2048]{1,0:T(8,128)(2,1)}, bf16[64,2048]{1,0:T(8,128)(2,1)S(1)}, u32[]{:S(2)}, u32[]{:S(2)}) %collective-permute-start.8) | collective-permute-done | bytes 262176 | tf_op jit(solution)/shard_map/ppermute | solution.py:319
  44.6 2.6 %collective-permute-start.10 = (bf16[64,2048]{1,0:T(8,128)(2,1)S(1)}, bf16[64,2048]{1,0:T(8,128)(2,1)}, u32[]{:S(2)}, u32[]{:S(2)}) collective-permute-start(bf16[64,2048]{1,0:T(8,128)(2,1)S(1)} %collective-permute-done.8.refs_5_), channel_id=1, source_target_pairs={{0,3},{1,0},{2,1},{3,2},{4,7},{5,4},{6,5},{7,6},{8,11},{9,8},{10,9... | collective-permute-start | bytes 786440 | tf_op jit(solution)/shard_map/ppermute | solution.py:319
  47.2 2.0 %shard_map.192 = bf16[4,4,64,128]{3,2,1,0:T(8,128)(2,1)S(1)} custom-call(bf16[8,416,128]{2,1,0:T(8,128)(2,1)S(1)} %all-to-all-done.kv_ref, bf16[256,128]{1,0:T(8,128)(2,1)S(1)} %copy-done.14, bf16[256,128]{1,0:T(8,128)(2,1)S(1)} %collective-permute-done.refs_1_, bf16[256,128]{1,0:T(8,128)(2,1)S(1)} %collective-permute-done.1.refs_2_, ...), custom_call_target="tpu_custom_call" | custom-call | flops 2000000000 | tf_op jit(solution)/shard_map/pallas_call | solution.py:353
  49.2 1.3 shard_map.194
  50.6 4.7 %all-to-all-start.1 = ((bf16[16,64,128]{2,1,0:T(8,128)(2,1)}), bf16[16,64,128]{2,1,0:T(8,128)(2,1)}, u32[]{:S(2)}, u32[]{:S(2)}) async-start(bf16[16,64,128]{2,1,0:T(8,128)(2,1)} %shard_map.194), calls=%async_computation.1 | async-start | bytes 524288 | tf_op jit(solution)/shard_map/all_to_all | solution.py:373
  64.0 2.4 %shard_map.196 = (bf16[64,2,2048]{2,1,0:T(2,128)(2,1)S(1)}, bf16[32,2048]{1,0:T(8,128)(2,1)S(1)}, bf16[2,32,128]{2,1,0:T(8,128)(2,1)S(1)}) custom-call(bf16[4,4,64,128]{3,2,1,0:T(8,128)(2,1)} %bitcast.12.parts_ref, bf16[32,2048]{1,0:T(8,128)(2,1)S(1)} %copy-done.16, f32[1,2048]{1,0:T(1,128)S(1)} %bitcast.28, s32[2,32]{1,0:T(2,128)S(1)} %bitcast.29, ...), custom_call_target="tpu_custom_call" | custom-call | flops 2000000000 | tf_op jit(solution)/shard_map/pallas_call | solution.py:385
  66.4 29.7 %all_to_all.21 = bf16[64,2,2048]{2,1,0:T(2,128)(2,1)S(1)} all-to-all(bf16[64,2,2048]{2,1,0:T(2,128)(2,1)S(1)} %get-tuple-element.21), channel_id=1, replica_groups=mesh['z'=8,'x'=4,'c'=2,'y'=4] {'z','x','c'}, dimensions={0} | all-to-all | bytes 1048576 | tf_op jit(solution)/shard_map/all_to_all | solution.py:393
  97.9 1.6 collective-permute-start.14
  99.5 5.8 %collective-permute-done.11.refs_2_ = bf16[64,2048]{1,0:T(8,128)(2,1)S(1)} collective-permute-done((bf16[64,2048]{1,0:T(8,128)(2,1)S(1)}, bf16[64,2048]{1,0:T(8,128)(2,1)S(1)}, u32[]{:S(2)}, u32[]{:S(2)}) %collective-permute-start.11) | collective-permute-done | bytes 262176 | tf_op jit(solution)/shard_map/ppermute | solution.py:319
  105.3 2.7 %collective-permute-start.16 = (bf16[64,2048]{1,0:T(8,128)(2,1)S(1)}, bf16[64,2048]{1,0:T(8,128)(2,1)S(1)}, u32[]{:S(2)}, u32[]{:S(2)}) collective-permute-start(bf16[64,2048]{1,0:T(8,128)(2,1)S(1)} %collective-permute-done.14.refs_5_), channel_id=1, source_target_pairs={{0,3},{1,0},{2,1},{3,2},{4,7},{5,4},{6,5},{7,6},{8,11},{9,8},{10,9... | collective-permute-start | bytes 786440 | tf_op jit(solution)/shard_map/ppermute | solution.py:319
  108.0 1.6 copy-done.1
  109.6 1.6 copy-done.2
  111.7 2.7 %collective-permute-start.13 = (bf16[64,2048]{1,0:T(8,128)(2,1)S(1)}, bf16[64,2048]{1,0:T(8,128)(2,1)S(1)}, u32[]{:S(2)}, u32[]{:S(2)}) collective-permute-start(bf16[64,2048]{1,0:T(8,128)(2,1)S(1)} %slice.13.refs_0_), channel_id=1, source_target_pairs={{0,3},{1,0},{2,1},{3,2},{4,7},{5,4},{6,5},{7,6},{8,11},{9,8},{10,9... | collective-permute-start | bytes 786440 | tf_op jit(solution)/shard_map/ppermute | solution.py:319
  115.8 3.2 %collective-permute-done.12.refs_3_ = bf16[64,2048]{1,0:T(8,128)(2,1)S(1)} collective-permute-done((bf16[64,2048]{1,0:T(8,128)(2,1)S(1)}, bf16[64,2048]{1,0:T(8,128)(2,1)S(1)}, u32[]{:S(2)}, u32[]{:S(2)}) %collective-permute-start.12) | collective-permute-done | bytes 262176 | tf_op jit(solution)/shard_map/ppermute | solution.py:319
  119.0 2.7 %shard_map.198 = (bf16[64,2048]{1,0:T(8,128)(2,1)S(1)}, bf16[64,2048]{1,0:T(8,128)(2,1)S(1)}, bf16[64,2048]{1,0:T(8,128)(2,1)S(1)}, bf16[64,2048]{1,0:T(8,128)(2...) custom-call(bf16[64,2048]{1,0:T(8,128)(2,1)S(1)} %slice.13.refs_0_, ...), custom_call_target="tpu_custom_call" | custom-call | flops 3000000000 | tf_op jit(solution)/shard_map/pallas_call | solution.py:408
  121.7 2.5 %collective-permute-start.19 = (bf16[64,2048]{1,0:T(8,128)(2,1)S(1)}, bf16[64,2048]{1,0:T(8,128)(2,1)S(1)}, u32[]{:S(2)}, u32[]{:S(2)}) collective-permute-start(bf16[64,2048]{1,0:T(8,128)(2,1)S(1)} %get-tuple-element.28), channel_id=1, source_target_pairs={{0,3},{1,0},{2,1},{3,2},{4,7},{5,4},{6,5},{7,6},{8,11},{9,8},{10,9... | collective-permute-start | bytes 786440 | tf_op jit(solution)/shard_map/ppermute | solution.py:319
  124.2 2.7 %collective-permute-start.21 = (bf16[64,2048]{1,0:T(8,128)(2,1)S(1)}, bf16[64,2048]{1,0:T(8,128)(2,1)S(1)}, u32[]{:S(2)}, u32[]{:S(2)}) collective-permute-start(bf16[64,2048]{1,0:T(8,128)(2,1)S(1)} %get-tuple-element.32), channel_id=1, source_target_pairs={{0,3},{1,0},{2,1},{3,2},{4,7},{5,4},{6,5},{7,6},{8,11},{9,8},{10,9... | collective-permute-start | bytes 786440 | tf_op jit(solution)/shard_map/ppermute | solution.py:319
  127.0 5.5 %collective-permute-done.21 = bf16[64,2048]{1,0:T(8,128)(2,1)S(1)} collective-permute-done((bf16[64,2048]{1,0:T(8,128)(2,1)S(1)}, bf16[64,2048]{1,0:T(8,128)(2,1)S(1)}, u32[]{:S(2)}, u32[]{:S(2)}) %collective-permute-start.21) | collective-permute-done | bytes 262176 | tf_op jit(solution)/shard_map/ppermute | solution.py:319
  132.6 3.5 %collective-permute-start.22 = (bf16[64,2048]{1,0:T(8,128)(2,1)S(1)}, bf16[64,2048]{1,0:T(8,128)(2,1)S(1)}, u32[]{:S(2)}, u32[]{:S(2)}) collective-permute-start(bf16[64,2048]{1,0:T(8,128)(2,1)S(1)} %add_convert_fusion.1), channel_id=1, source_target_pairs={{0,3},{1,0},{2,1},{3,2},{4,7},{5,4},{6,5},{7,6},{8,11},{9,8},{10,9... | collective-permute-start | bytes 786440 | tf_op jit(solution)/shard_map/ppermute | solution.py:319
  136.2 3.2 %collective-permute-done.22 = bf16[64,2048]{1,0:T(8,128)(2,1)S(1)} collective-permute-done((bf16[64,2048]{1,0:T(8,128)(2,1)S(1)}, bf16[64,2048]{1,0:T(8,128)(2,1)S(1)}, u32[]{:S(2)}, u32[]{:S(2)}) %collective-permute-start.22) | collective-permute-done | bytes 262176 | tf_op jit(solution)/shard_map/ppermute | solution.py:319
  139.9 27.2 %all_to_all.22 = bf16[64,2,2048]{2,1,0:T(2,128)(2,1)S(1)} all-to-all(bf16[64,2,2048]{2,1,0:T(2,128)(2,1)S(1)} %convert_element_type.53), channel_id=1, replica_groups=mesh['z'=8,'x'=4,'c'=2,'y'=4] {'z','x','c'}, dimensions={0} | all-to-all | bytes 1048576 | tf_op jit(solution)/shard_map/all_to_all | solution.py:440
  (80 shorter events, 18.7 us)
Async XLA Ops:
  2.5 34.0 %all-to-all-start = ((bf16[8,416,128]{2,1,0:T(8,128)(2,1)}), bf16[8,416,128]{2,1,0:T(8,128)(2,1)S(1)}, u32[]{:S(2)}, u32[]{:S(2)}) async-start(bf16[8,416,128]{2,1,0:T(8,128)(2,1)} %shard_map.190), calls=%async_computation | async-start | bytes 1703936 | tf_op jit(solution)/shard_map/all_to_all | solution.py:333
  11.5 16.8 %collective-permute-start.5 = (bf16[128,2048]{1,0:T(8,128)(2,1)}, bf16[128,2048]{1,0:T(8,128)(2,1)}, u32[]{:S(2)}, u32[]{:S(2)}) collective-permute-start(bf16[128,2048]{1,0:T(8,128)(2,1)} %refs_0_.1), channel_id=1, source_target_pairs={{0,1},{1,2},{2,3},{3,0},{4,5},{5,6},{6,7},{7,4},{8,9},{9,10},{10,1... | collective-permute-start | bytes 1572872 | tf_op jit(solution)/shard_map/ppermute | solution.py:319
  14.4 5.4 %collective-permute-start.2 = (bf16[256,128]{1,0:T(8,128)(2,1)}, bf16[256,128]{1,0:T(8,128)(2,1)S(1)}, u32[]{:S(2)}, u32[]{:S(2)}) collective-permute-start(bf16[256,128]{1,0:T(8,128)(2,1)} %shard_map.191.refs_0_), channel_id=1, source_target_pairs={{0,16},{8,24},{16,0},{24,8},{1,17},{9,25},{17,1},{25,9},{2,18},{10... | collective-permute-start | bytes 196616 | tf_op jit(solution)/shard_map/ppermute | solution.py:319
  17.2 5.2 %collective-permute-start = (bf16[256,128]{1,0:T(8,128)(2,1)}, bf16[256,128]{1,0:T(8,128)(2,1)S(1)}, u32[]{:S(2)}, u32[]{:S(2)}) collective-permute-start(bf16[256,128]{1,0:T(8,128)(2,1)} %shard_map.191.refs_0_), channel_id=1, source_target_pairs={{0,8},{8,16},{16,24},{24,0},{1,9},{9,17},{17,25},{25,1},{2,10},{10... | collective-permute-start | bytes 196616 | tf_op jit(solution)/shard_map/ppermute | solution.py:319
  17.5 4.9 %collective-permute-start.1 = (bf16[256,128]{1,0:T(8,128)(2,1)}, bf16[256,128]{1,0:T(8,128)(2,1)S(1)}, u32[]{:S(2)}, u32[]{:S(2)}) collective-permute-start(bf16[256,128]{1,0:T(8,128)(2,1)} %shard_map.191.refs_0_), channel_id=1, source_target_pairs={{0,24},{8,0},{16,8},{24,16},{1,25},{9,1},{17,9},{25,17},{2,26},{10... | collective-permute-start | bytes 196616 | tf_op jit(solution)/shard_map/ppermute | solution.py:319
  23.3 15.8 %copy-start.8 = (bf16[64,2048]{1,0:T(8,128)(2,1)S(1)}, bf16[64,2048]{1,0:T(8,128)(2,1)}, u32[]{:S(2)}) copy-start(bf16[64,2048]{1,0:T(8,128)(2,1)} %refs_1_.1) | copy-start | bytes 786436
  23.3 23.9 %copy-start.14 = (bf16[256,128]{1,0:T(8,128)(2,1)S(1)}, bf16[256,128]{1,0:T(8,128)(2,1)}, u32[]{:S(2)}) copy-start(bf16[256,128]{1,0:T(8,128)(2,1)} %shard_map.191.refs_0_) | copy-start | bytes 196612
  23.3 5.0 %collective-permute-start.3 = (bf16[4,256,128]{2,1,0:T(8,128)(2,1)S(1)}, bf16[4,256,128]{2,1,0:T(8,128)(2,1)S(1)}, u32[]{:S(2)}, u32[]{:S(2)}) collective-permute-start(bf16[4,256,128]{2,1,0:T(8,128)(2,1)S(1)} %pad_maximum_fusion.1), channel_id=1, source_target_pairs={{0,4},{4,0},{1,5},{5,1},{2,6},{6,2},{3,7},{7,3},{8,12},{12,8},{9,1... | collective-permute-start | bytes 786440 | tf_op jit(solution)/shard_map/ppermute | solution.py:319
  25.4 30.7 %collective-permute-start.7 = (bf16[128,2048]{1,0:T(8,128)(2,1)}, bf16[128,2048]{1,0:T(8,128)(2,1)S(1)}, u32[]{:S(2)}, u32[]{:S(2)}) collective-permute-start(bf16[128,2048]{1,0:T(8,128)(2,1)} %refs_0_.1), channel_id=1, source_target_pairs={{0,3},{1,0},{2,1},{3,2},{4,7},{5,4},{6,5},{7,6},{8,11},{9,8},{10,9... | collective-permute-start | bytes 1572872 | tf_op jit(solution)/shard_map/ppermute | solution.py:319
  26.7 17.8 %collective-permute-start.8 = (bf16[64,2048]{1,0:T(8,128)(2,1)}, bf16[64,2048]{1,0:T(8,128)(2,1)S(1)}, u32[]{:S(2)}, u32[]{:S(2)}) collective-permute-start(bf16[64,2048]{1,0:T(8,128)(2,1)} %refs_1_.1), channel_id=1, source_target_pairs={{0,3},{1,0},{2,1},{3,2},{4,7},{5,4},{6,5},{7,6},{8,11},{9,8},{10,9... | collective-permute-start | bytes 786440 | tf_op jit(solution)/shard_map/ppermute | solution.py:319
  28.3 28.5 %collective-permute-start.9 = (bf16[128,2048]{1,0:T(8,128)(2,1)}, bf16[128,2048]{1,0:T(8,128)(2,1)S(1)}, u32[]{:S(2)}, u32[]{:S(2)}) collective-permute-start(bf16[128,2048]{1,0:T(8,128)(2,1)} %collective-permute-done.5.refs_2_), channel_id=1, source_target_pairs={{0,1},{1,2},{2,3},{3,0},{4,5},{5,6},{6,7},{7,4},{8,9},{9,10},{10,1... | collective-permute-start | bytes 1572872 | tf_op jit(solution)/shard_map/ppermute | solution.py:319
  38.5 10.7 %collective-permute-start.4 = (bf16[16,64,128]{2,1,0:T(8,128)(2,1)S(1)}, bf16[16,64,128]{2,1,0:T(8,128)(2,1)S(1)}, u32[]{:S(2)}, u32[]{:S(2)}) collective-permute-start(bf16[16,64,128]{2,1,0:T(8,128)(2,1)S(1)} %bitcast.27), channel_id=1, source_target_pairs={{0,4},{4,0},{1,5},{5,1},{2,6},{6,2},{3,7},{7,3},{8,12},{12,8},{9,1... | collective-permute-start | bytes 786440 | tf_op jit(solution)/shard_map/ppermute | solution.py:319
  39.1 16.2 %collective-permute-start.6 = (bf16[64,2048]{1,0:T(8,128)(2,1)S(1)}, bf16[64,2048]{1,0:T(8,128)(2,1)S(1)}, u32[]{:S(2)}, u32[]{:S(2)}) collective-permute-start(bf16[64,2048]{1,0:T(8,128)(2,1)S(1)} %copy-done.8), channel_id=1, source_target_pairs={{0,1},{1,2},{2,3},{3,0},{4,5},{5,6},{6,7},{7,4},{8,9},{9,10},{10,1... | collective-permute-start | bytes 786440 | tf_op jit(solution)/shard_map/ppermute | solution.py:319
  44.6 11.4 %collective-permute-start.10 = (bf16[64,2048]{1,0:T(8,128)(2,1)S(1)}, bf16[64,2048]{1,0:T(8,128)(2,1)}, u32[]{:S(2)}, u32[]{:S(2)}) collective-permute-start(bf16[64,2048]{1,0:T(8,128)(2,1)S(1)} %collective-permute-done.8.refs_5_), channel_id=1, source_target_pairs={{0,3},{1,0},{2,1},{3,2},{4,7},{5,4},{6,5},{7,6},{8,11},{9,8},{10,9... | collective-permute-start | bytes 786440 | tf_op jit(solution)/shard_map/ppermute | solution.py:319
  50.5 13.4 %copy-start.16 = (bf16[32,2048]{1,0:T(8,128)(2,1)S(1)}, bf16[32,2048]{1,0:T(8,128)(2,1)}, u32[]{:S(2)}) copy-start(bf16[32,2048]{1,0:T(8,128)(2,1)} %res_ref.1) | copy-start | bytes 393220
  50.5 13.4 %copy-start.17 = (f32[2048]{0:T(1024)S(1)}, f32[2048]{0:T(1024)}, u32[]{:S(2)}) copy-start(f32[2048]{0:T(1024)} %param.32) | copy-start | bytes 24580
  50.6 13.4 %copy-start.18 = (s32[32,2]{0,1:T(2,128)S(1)}, s32[32,2]{0,1:T(2,128)}, u32[]{:S(2)}) copy-start(s32[32,2]{0,1:T(2,128)} %param.36) | copy-start | bytes 772
  50.6 13.4 %all-to-all-start.1 = ((bf16[16,64,128]{2,1,0:T(8,128)(2,1)}), bf16[16,64,128]{2,1,0:T(8,128)(2,1)}, u32[]{:S(2)}, u32[]{:S(2)}) async-start(bf16[16,64,128]{2,1,0:T(8,128)(2,1)} %shard_map.194), calls=%async_computation.1 | async-start | bytes 524288 | tf_op jit(solution)/shard_map/all_to_all | solution.py:373
  66.4 41.6 %copy-start = (bf16[1,2048,512]{2,1,0:T(8,128)(2,1)S(1)}, bf16[1,2048,512]{2,1,0:T(8,128)(2,1)}, u32[]{:S(2)}) copy-start(bf16[1,2048,512]{2,1,0:T(8,128)(2,1)} %param.33) | copy-start | bytes 6291460
  96.6 8.8 %collective-permute-start.11 = (bf16[64,2048]{1,0:T(8,128)(2,1)S(1)}, bf16[64,2048]{1,0:T(8,128)(2,1)S(1)}, u32[]{:S(2)}, u32[]{:S(2)}) collective-permute-start(bf16[64,2048]{1,0:T(8,128)(2,1)S(1)} %slice.13.refs_0_), channel_id=1, source_target_pairs={{0,1},{1,2},{2,3},{3,0},{4,5},{5,6},{6,7},{7,4},{8,9},{9,10},{10,1... | collective-permute-start | bytes 786440 | tf_op jit(solution)/shard_map/ppermute | solution.py:319
  97.9 7.4 %collective-permute-start.14 = (bf16[64,2048]{1,0:T(8,128)(2,1)S(1)}, bf16[64,2048]{1,0:T(8,128)(2,1)S(1)}, u32[]{:S(2)}, u32[]{:S(2)}) collective-permute-start(bf16[64,2048]{1,0:T(8,128)(2,1)S(1)} %slice.15.refs_1_), channel_id=1, source_target_pairs={{0,3},{1,0},{2,1},{3,2},{4,7},{5,4},{6,5},{7,6},{8,11},{9,8},{10,9... | collective-permute-start | bytes 786440 | tf_op jit(solution)/shard_map/ppermute | solution.py:319
  105.3 9.1 %collective-permute-start.15 = (bf16[64,2048]{1,0:T(8,128)(2,1)S(1)}, bf16[64,2048]{1,0:T(8,128)(2,1)S(1)}, u32[]{:S(2)}, u32[]{:S(2)}) collective-permute-start(bf16[64,2048]{1,0:T(8,128)(2,1)S(1)} %collective-permute-done.11.refs_2_), channel_id=1, source_target_pairs={{0,1},{1,2},{2,3},{3,0},{4,5},{5,6},{6,7},{7,4},{8,9},{9,10},{10,1... | collective-permute-start | bytes 786440 | tf_op jit(solution)/shard_map/ppermute | solution.py:319
  105.3 9.1 %collective-permute-start.16 = (bf16[64,2048]{1,0:T(8,128)(2,1)S(1)}, bf16[64,2048]{1,0:T(8,128)(2,1)S(1)}, u32[]{:S(2)}, u32[]{:S(2)}) collective-permute-start(bf16[64,2048]{1,0:T(8,128)(2,1)S(1)} %collective-permute-done.14.refs_5_), channel_id=1, source_target_pairs={{0,3},{1,0},{2,1},{3,2},{4,7},{5,4},{6,5},{7,6},{8,11},{9,8},{10,9... | collective-permute-start | bytes 786440 | tf_op jit(solution)/shard_map/ppermute | solution.py:319
  111.6 7.3 %collective-permute-start.12 = (bf16[64,2048]{1,0:T(8,128)(2,1)S(1)}, bf16[64,2048]{1,0:T(8,128)(2,1)S(1)}, u32[]{:S(2)}, u32[]{:S(2)}) collective-permute-start(bf16[64,2048]{1,0:T(8,128)(2,1)S(1)} %slice.15.refs_1_), channel_id=1, source_target_pairs={{0,1},{1,2},{2,3},{3,0},{4,5},{5,6},{6,7},{7,4},{8,9},{9,10},{10,1... | collective-permute-start | bytes 786440 | tf_op jit(solution)/shard_map/ppermute | solution.py:319
  111.7 7.3 %collective-permute-start.13 = (bf16[64,2048]{1,0:T(8,128)(2,1)S(1)}, bf16[64,2048]{1,0:T(8,128)(2,1)S(1)}, u32[]{:S(2)}, u32[]{:S(2)}) collective-permute-start(bf16[64,2048]{1,0:T(8,128)(2,1)S(1)} %slice.13.refs_0_), channel_id=1, source_target_pairs={{0,3},{1,0},{2,1},{3,2},{4,7},{5,4},{6,5},{7,6},{8,11},{9,8},{10,9... | collective-permute-start | bytes 786440 | tf_op jit(solution)/shard_map/ppermute | solution.py:319
  115.5 11.3 %collective-permute-start.17 = (bf16[64,2048]{1,0:T(8,128)(2,1)S(1)}, bf16[64,2048]{1,0:T(8,128)(2,1)S(1)}, u32[]{:S(2)}, u32[]{:S(2)}) collective-permute-start(bf16[64,2048]{1,0:T(8,128)(2,1)S(1)} %get-tuple-element.27), channel_id=1, source_target_pairs={{0,1},{1,2},{2,3},{3,0},{4,5},{5,6},{6,7},{7,4},{8,9},{9,10},{10,1... | collective-permute-start | bytes 786440 | tf_op jit(solution)/shard_map/ppermute | solution.py:319
  121.7 14.4 %collective-permute-start.19 = (bf16[64,2048]{1,0:T(8,128)(2,1)S(1)}, bf16[64,2048]{1,0:T(8,128)(2,1)S(1)}, u32[]{:S(2)}, u32[]{:S(2)}) collective-permute-start(bf16[64,2048]{1,0:T(8,128)(2,1)S(1)} %get-tuple-element.28), channel_id=1, source_target_pairs={{0,3},{1,0},{2,1},{3,2},{4,7},{5,4},{6,5},{7,6},{8,11},{9,8},{10,9... | collective-permute-start | bytes 786440 | tf_op jit(solution)/shard_map/ppermute | solution.py:319
  124.2 12.0 %collective-permute-start.20 = (bf16[64,2048]{1,0:T(8,128)(2,1)S(1)}, bf16[64,2048]{1,0:T(8,128)(2,1)S(1)}, u32[]{:S(2)}, u32[]{:S(2)}) collective-permute-start(bf16[64,2048]{1,0:T(8,128)(2,1)S(1)} %get-tuple-element.30), channel_id=1, source_target_pairs={{0,1},{1,2},{2,3},{3,0},{4,5},{5,6},{6,7},{7,4},{8,9},{9,10},{10,1... | collective-permute-start | bytes 786440 | tf_op jit(solution)/shard_map/ppermute | solution.py:319
  124.2 8.3 %collective-permute-start.21 = (bf16[64,2048]{1,0:T(8,128)(2,1)S(1)}, bf16[64,2048]{1,0:T(8,128)(2,1)S(1)}, u32[]{:S(2)}, u32[]{:S(2)}) collective-permute-start(bf16[64,2048]{1,0:T(8,128)(2,1)S(1)} %get-tuple-element.32), channel_id=1, source_target_pairs={{0,3},{1,0},{2,1},{3,2},{4,7},{5,4},{6,5},{7,6},{8,11},{9,8},{10,9... | collective-permute-start | bytes 786440 | tf_op jit(solution)/shard_map/ppermute | solution.py:319
  126.9 9.2 %collective-permute-start.18 = (bf16[64,2048]{1,0:T(8,128)(2,1)S(1)}, bf16[64,2048]{1,0:T(8,128)(2,1)S(1)}, u32[]{:S(2)}, u32[]{:S(2)}) collective-permute-start(bf16[64,2048]{1,0:T(8,128)(2,1)S(1)} %add_convert_fusion.3), channel_id=1, source_target_pairs={{0,1},{1,2},{2,3},{3,0},{4,5},{5,6},{6,7},{7,4},{8,9},{9,10},{10,1... | collective-permute-start | bytes 786440 | tf_op jit(solution)/shard_map/ppermute | solution.py:319
  132.6 6.8 %collective-permute-start.22 = (bf16[64,2048]{1,0:T(8,128)(2,1)S(1)}, bf16[64,2048]{1,0:T(8,128)(2,1)S(1)}, u32[]{:S(2)}, u32[]{:S(2)}) collective-permute-start(bf16[64,2048]{1,0:T(8,128)(2,1)S(1)} %add_convert_fusion.1), channel_id=1, source_target_pairs={{0,3},{1,0},{2,1},{3,2},{4,7},{5,4},{6,5},{7,6},{8,11},{9,8},{10,9... | collective-permute-start | bytes 786440 | tf_op jit(solution)/shard_map/ppermute | solution.py:319
  139.5 27.8 %copy-start.15 = (f32[32,2]{0,1:T(2,128)S(1)}, f32[32,2]{0,1:T(2,128)}, u32[]{:S(2)}) copy-start(f32[32,2]{0,1:T(2,128)} %param.37) | copy-start | bytes 772
  (12 other events, 23.5 us)
